TPU v7x, 512 devices: a whole 4x4x16 slice. The times are simulated.
512 devices in a mesh: sp: 128 (over z, x, core), tp: 4 (over y).
Axes of the slice: x: 4, y: 4, z: 16, core: 2. Of those that a mesh axis runs over, the one named last changes fastest.
Arguments:
- tokens: bfloat16 [65536, 2048], P(('sp', 'tp')), may hold values from -6 to 6
- input_norm_scale: bfloat16 [2048], replicated, may hold values from 0.099609375 to 1.8984375
- outer_gate_weight: bfloat16 [2048, 1024], P('sp', 'tp'), may hold values from -0.125 to 0.125
- inner_gate_weight: bfloat16 [2048, 1024], P('sp', 'tp'), may hold values from -0.125 to 0.125
- value_weight_matrix: bfloat16 [2048, 1024], P('sp', 'tp'), may hold values from -0.125 to 0.125
- output_gate_weight: bfloat16 [2048, 1024], P('sp', 'tp'), may hold values from -0.125 to 0.125
- state_input_weight: bfloat16 [2048, 1024], P('sp', 'tp'), may hold values from -0.125 to 0.125
- write_key_weight: bfloat16 [2048, 512], P('sp', 'tp'), may hold values from -0.125 to 0.125
- read_key_weight: bfloat16 [2048, 512], P('sp', 'tp'), may hold values from -0.125 to 0.125
- step_size_weight: bfloat16 [2048, 16], P(None, 'tp'), may hold values from -0.125 to 0.125
- gated_conv_weight: bfloat16 [3, 1024], P(None, 'tp'), may hold values from -3.5 to 3.5
- input_conv_weight: bfloat16 [4, 1024], P(None, 'tp'), may hold values from -3 to 3
- write_conv_weight: bfloat16 [4, 512], P(None, 'tp'), may hold values from -3 to 3
- read_conv_weight: bfloat16 [4, 512], P(None, 'tp'), may hold values from -3 to 3
- step_size_bias: float32 [16], P('tp'), may hold values from -1 to 0.5
- log_decay_rate: float32 [16], P('tp'), may hold values from -16 to -2.5, as said below
- decay_spikes: float32 [16, 65536], P('tp', 'sp'), may hold values from -1 to 0, as said below
- direct_path_weight: float32 [16], P('tp'), may hold values from 0.5 to 2
- head_norm_scale: bfloat16 [1024], P('tp'), may hold values from 0.099609375 to 1.8984375
- conv_output_weight: bfloat16 [1024, 2048], P('tp', 'sp'), may hold values from -0.125 to 0.125
- state_output_weight: bfloat16 [1024, 2048], P('tp', 'sp'), may hold values from -0.125 to 0.125
Outputs:
- mixed: bfloat16 [65536, 2048], P(('sp', 'tp'))
Inputs may be any that keep to these rules, and one draw needn't show every extreme that they name: `log_decay_rate`: one value a head. `decay_spikes`: never positive.
All inputs are finite; a program needn't handle non-finite values.
Results may differ from a plain program's by a relative error of at most 0.017.
Values may be sent and summed in bfloat16 or wider, within the bound.
No kernel may reach another device: no remote copies, remote signals or barrier semaphores. Data moves between devices by JAX's collectives and lax.ppermute only.
A program may use at most 128 MiB of HBM per device.

v0:
```python
import jax
import jax.numpy as jnp
from jax import lax
from jax.sharding import Mesh
from jax.sharding import PartitionSpec as P

HEAD_DIM = 64
STATE = 128
BLOCK = 64
SP = ("sp_0", "sp_1", "sp_2")
SP_TP = ("sp_0", "sp_1", "sp_2", "tp")


epsilon = 1e-05


def in_order(tiles, dim):
    tiles = jnp.moveaxis(tiles, 0, dim)
    dims = tiles.shape
    return tiles.reshape(*dims[:dim], dims[dim] * dims[dim + 1], *dims[dim + 2 :])


def copy_for_each(shard, axis):
    devices = lax.axis_size(axis)
    return lax.all_to_all(
        jnp.broadcast_to(shard[None], (devices, *shard.shape)), axis, 0, 0, tiled=True
    )


def gather_directly(shard, axis, dim):
    return in_order(copy_for_each(shard, axis), dim)


def side_by_side(arrays, axis, dim, along):
    widths = [a.shape[along] for a in arrays]
    both = jnp.concatenate(arrays, axis=along)
    whole = lax.all_gather(both, axis, axis=dim, tiled=True)
    return tuple(jnp.split(whole, [sum(widths[:k]) for k in range(1, len(widths))], axis=along))


def shifted(shard, axis, by):
    devices = lax.axis_size(axis)
    pairs = [(i, i + by) for i in range(devices) if 0 <= i + by < devices]
    return lax.ppermute(shard, axis, pairs)


def filled_with(shard, identity):
    return jax.tree.map(
        lambda a, e: jnp.broadcast_to(jnp.asarray(e, a.dtype), a.shape), shard, identity
    )


def prefix_by_axis(shard, axes, combine, identity):
    before = start = filled_with(shard, identity)
    subtotal = shard
    for axis in reversed(axes):
        devices, index = (lax.axis_size(axis), lax.axis_index(axis))
        pieces = jax.tree.map(
            lambda part, kind: lax.all_gather(part.astype(kind), axis),
            subtotal,
            (jnp.bfloat16, jnp.bfloat16),
        )
        inside, subtotal = (start, start)
        for k in range(devices):
            passed = k < index
            subtotal = combine(
                subtotal, jax.tree.map(lambda part, own: part[k].astype(own.dtype), pieces, shard)
            )
            inside = jax.tree.map(lambda new, old: jnp.where(passed, new, old), subtotal, inside)
        before = combine(inside, before)
    return before


def whole_of(shard, axes, dim):
    far, near = axes
    tiles = copy_for_each(copy_for_each(shard, far), near)
    return in_order(tiles.swapaxes(0, 1).reshape(-1, *shard.shape), dim)


def side_by_side_2(arrays, axis, dim, along):
    both = jnp.concatenate(arrays, axis=along)
    whole, at, outs = (whole_of(both, axis, dim), 0, [])
    for a in arrays:
        outs.append(lax.slice_in_dim(whole, at, at + a.shape[along], axis=along))
        at += a.shape[along]
    return tuple(outs)


def split_up(shard, dim, devices):
    dims = shard.shape
    tiles = shard.reshape(*dims[:dim], devices, dims[dim] // devices, *dims[dim + 1 :])
    return jnp.moveaxis(tiles, dim, 0)


def summed_on_arrival(shard, axis, dim):
    tiles = split_up(shard, dim, lax.axis_size(axis))
    arrived = lax.all_to_all(tiles, axis, split_axis=0, concat_axis=0, tiled=True)
    return arrived.astype(jnp.float32).sum(axis=0)


def causal_taps(values, rim_rows, tap_weights):
    tap_count = tap_weights.shape[0]
    length = values.shape[0]
    padded = jnp.concatenate([rim_rows, values], axis=0)
    running = tap_weights[0] * padded[0:length]
    for offset in range(1, tap_count):
        running = running + tap_weights[offset] * padded[offset : offset + length]
    return running


def combine_states(earlier, later):
    return (earlier[0] * later[0], earlier[1] * later[0][:, None, None] + later[1])


def per_device(
    tokens,
    input_norm_scale,
    outer_gate_weight,
    inner_gate_weight,
    value_weight_matrix,
    output_gate_weight,
    state_input_weight,
    write_key_weight,
    read_key_weight,
    step_size_weight,
    gated_conv_weight,
    input_conv_weight,
    write_conv_weight,
    read_conv_weight,
    step_size_bias,
    log_decay_rate,
    decay_spikes,
    direct_path_weight,
    head_norm_scale,
    conv_output_weight,
    state_output_weight,
):
    token_rows = tokens.astype(jnp.float32)
    scaled = token_rows * lax.rsqrt(
        jnp.mean(token_rows * token_rows, axis=1, keepdims=True) + epsilon
    )
    normed_own = (scaled * input_norm_scale.astype(jnp.float32)).astype(jnp.bfloat16)
    normed = gather_directly(normed_own, "tp", 0)
    length = normed.shape[0]
    pieces = side_by_side(
        (
            outer_gate_weight,
            inner_gate_weight,
            value_weight_matrix,
            output_gate_weight,
            state_input_weight,
            write_key_weight,
            read_key_weight,
        ),
        SP,
        0,
        1,
    )
    projected = tuple(
        (jnp.dot(normed, weight_rows, preferred_element_type=jnp.float32) for weight_rows in pieces)
    )
    outer_gate, inner_gate, conv_input, out_gate, state_input, write_keys, read_keys = [
        member.astype(jnp.bfloat16) for member in projected
    ]
    step_raw = jnp.dot(normed, step_size_weight, preferred_element_type=jnp.float32)
    short_rim = gated_conv_weight.shape[0] - 1
    state_rim = input_conv_weight.shape[0] - 1
    rim_rows = shifted(
        (
            inner_gate[length - short_rim :],
            conv_input[length - short_rim :],
            state_input[length - state_rim :],
            write_keys[length - state_rim :],
            read_keys[length - state_rim :],
        ),
        SP,
        1,
    )
    product = inner_gate.astype(jnp.float32) * conv_input.astype(jnp.float32)
    rim_product = rim_rows[0].astype(jnp.float32) * rim_rows[1].astype(jnp.float32)
    mixer_part = (
        outer_gate.astype(jnp.float32)
        * causal_taps(product, rim_product, gated_conv_weight.astype(jnp.float32))
    ).astype(jnp.bfloat16)
    seq_input = jax.nn.silu(
        causal_taps(
            state_input.astype(jnp.float32),
            rim_rows[2].astype(jnp.float32),
            input_conv_weight.astype(jnp.float32),
        )
    )
    seq_write = jax.nn.silu(
        causal_taps(
            write_keys.astype(jnp.float32),
            rim_rows[3].astype(jnp.float32),
            write_conv_weight.astype(jnp.float32),
        )
    )
    seq_read = jax.nn.silu(
        causal_taps(
            read_keys.astype(jnp.float32),
            rim_rows[4].astype(jnp.float32),
            read_conv_weight.astype(jnp.float32),
        )
    )
    discrete_step = jax.nn.softplus(step_raw + step_size_bias[None, :])
    step_logarithm = discrete_step * (-jnp.exp(log_decay_rate))[None, :] + decay_spikes.T
    heads_here = discrete_step.shape[1]
    groups_here = seq_write.shape[1] // STATE
    per_group = heads_here // groups_here
    blocks = length // BLOCK
    input_blocks = seq_input.reshape(blocks, BLOCK, heads_here, HEAD_DIM)
    weighted = input_blocks * discrete_step.reshape(blocks, BLOCK, heads_here, 1)
    write_blocks = jnp.repeat(
        seq_write.reshape(blocks, BLOCK, groups_here, STATE), per_group, axis=2
    )
    read_blocks = jnp.repeat(seq_read.reshape(blocks, BLOCK, groups_here, STATE), per_group, axis=2)
    cumulative = jnp.cumsum(step_logarithm.reshape(blocks, BLOCK, heads_here), axis=1)
    causal = lax.broadcasted_iota(jnp.int32, (BLOCK, BLOCK), 0) >= lax.broadcasted_iota(
        jnp.int32, (BLOCK, BLOCK), 1
    )
    scores = jnp.einsum("clhm,cshm->clsh", read_blocks, write_blocks)
    damping = jnp.exp(
        jnp.where(
            causal[None, :, :, None],
            cumulative[:, :, None, :] - cumulative[:, None, :, :],
            -jnp.inf,
        )
    )
    within_block = jnp.einsum("clsh,cshp->clhp", scores * damping, weighted)
    to_end = jnp.exp(cumulative[:, -1:, :] - cumulative)
    block_states = jnp.einsum("cshm,cshp->chpm", write_blocks * to_end[..., None], weighted)
    block_logs = cumulative[:, -1, :]

    def advance(carried_state, inputs):
        contribution, block_log = inputs
        return (carried_state * jnp.exp(block_log)[:, None, None] + contribution, carried_state)

    own_total, own_before = lax.scan(
        advance, jnp.zeros(block_states.shape[1:], jnp.float32), (block_states, block_logs)
    )
    total_log = jnp.sum(block_logs, axis=0)
    arriving = prefix_by_axis(
        (jnp.exp(total_log), own_total),
        SP,
        combine_states,
        (jnp.ones_like(total_log), jnp.zeros_like(own_total)),
    )[1]
    before_logs = jnp.cumsum(block_logs, axis=0) - block_logs
    entering = own_before + jnp.exp(before_logs)[:, :, None, None] * arriving[None]
    from_before = (
        jnp.einsum("clhm,chpm->clhp", read_blocks, entering) * jnp.exp(cumulative)[..., None]
    )
    head_out = within_block + from_before + direct_path_weight[None, None, :, None] * input_blocks
    head_out = head_out.reshape(length, heads_here * HEAD_DIM)
    gated_heads = (head_out * jax.nn.silu(out_gate.astype(jnp.float32))).reshape(
        length, heads_here, HEAD_DIM
    )
    normalized = gated_heads * lax.rsqrt(
        jnp.mean(gated_heads * gated_heads, axis=2, keepdims=True) + epsilon
    )
    state_part = (
        normalized.reshape(length, heads_here * HEAD_DIM) * head_norm_scale.astype(jnp.float32)
    ).astype(jnp.bfloat16)
    wide_mixer, wide_state = side_by_side_2(
        (conv_output_weight, state_output_weight), (("sp_0", "sp_1"), "sp_2"), 1, 0
    )
    summed = summed_on_arrival(
        (
            jnp.dot(mixer_part, wide_mixer, preferred_element_type=jnp.float32)
            + jnp.dot(state_part, wide_state, preferred_element_type=jnp.float32)
        ).astype(jnp.bfloat16),
        "tp",
        0,
    )
    return summed.astype(jnp.bfloat16)


def solution(mesh):
    torus = Mesh(mesh.devices.reshape(16, 4, 2, mesh.shape["tp"]), ("sp_0", "sp_1", "sp_2", "tp"))
    return jax.shard_map(
        per_device,
        mesh=torus,
        in_specs=(
            P(SP_TP, None),
            P(),
            P(SP, "tp"),
            P(SP, "tp"),
            P(SP, "tp"),
            P(SP, "tp"),
            P(SP, "tp"),
            P(SP, "tp"),
            P(SP, "tp"),
            P(None, "tp"),
            P(None, "tp"),
            P(None, "tp"),
            P(None, "tp"),
            P(None, "tp"),
            P("tp"),
            P("tp"),
            P("tp", SP),
            P("tp"),
            P("tp"),
            P("tp", SP),
            P("tp", SP),
        ),
        out_specs=P(SP_TP, None),
        check_vma=False,
    )
```

profile of v0, /device:TPU:2, one launch (start us, length us, event | category | flops | bytes accessed | tf_op | source)
XLA Modules:
  0.0 331.9 jit_solution(838444194159853852)
XLA Ops:
  12.8 1.2 fusion.11
  14.0 1.2 fusion.13
  15.2 1.7 broadcast_in_dim.23
  16.9 4.6 %all-to-all-start = ((bf16[4,128,2048]{2,1,0:T(8,128)(2,1)}), bf16[4,128,2048]{2,1,0:T(8,128)(2,1)S(1)}, u32[]{:S(2)}, u32[]{:S(2)}) async-start(bf16[4,128,2048]{2,1,0:T(8,128)(2,1)} %broadcast_in_dim.23), calls=%async_computation | async-start | bytes 4194304 | tf_op jit(solution)/shard_map/all_to_all | solution.py:25
  21.6 26.2 %all-to-all-done = bf16[4,128,2048]{2,1,0:T(8,128)(2,1)S(1)} async-done(((bf16[4,128,2048]{2,1,0:T(8,128)(2,1)}), bf16[4,128,2048]{2,1,0:T(8,128)(2,1)S(1)}, u32[]{:S(2)}, u32[]{:S(2)}) %all-to-all-start) | async-done | bytes 2097184 | tf_op jit(solution)/shard_map/all_to_all | solution.py:25
  47.8 1.1 broadcast_in_dim.24
  48.9 18.6 %all-to-all-start.1 = ((bf16[64,512,16]{1,2,0:T(8,128)(2,1)}), bf16[64,512,16]{1,2,0:T(8,128)(2,1)S(1)}, u32[]{:S(2)}, u32[]{:S(2)}) async-start(bf16[64,512,16]{1,2,0:T(8,128)(2,1)} %broadcast_in_dim.24), calls=%async_computation.1 | async-start | bytes 2097152 | tf_op jit(solution)/shard_map/all_to_all | solution.py:25
  68.2 1.3 dynamic-slice
  72.5 1.3 bitcast_add_fusion.1
  74.7 1.0 fusion.126
  77.4 1.3 dynamic-update-slice
  78.6 3.1 all-reduce
  82.6 1.2 convert_element_type.583
  83.8 8.2 %all-gather.2 = bf16[4,1,4]{2,1,0:T(2,128)(2,1)} all-gather(bf16[1,1,4]{2,1,0:T(2,128)(2,1)S(1)} %convert_bitcast_fusion), channel_id=1, replica_groups=mesh['sp_0'=16,'sp_1'=4,'sp_2'=2,'tp'=4] {'sp_1'}, dimensions={0}, use_global_device_ids=true | all-gather | bytes 40 | tf_op jit(solution)/shard_map/all_gather | solution.py:59
  92.8 1.3 copy.60
  94.1 1.3 copy.63
  95.4 1.5 fusion.119
  96.9 1.7 copy.62
  100.0 1.7 copy.65
  104.5 34.2 %all-gather.3 = bf16[16,1,4]{2,1,0:T(2,128)(2,1)S(1)} all-gather(bf16[1,1,4]{2,1,0:T(2,128)(2,1)S(1)} %fusion.112), channel_id=1, replica_groups=mesh['sp_0'=16,'sp_1'=4,'sp_2'=2,'tp'=4] {'sp_0'}, dimensions={0}, use_global_device_ids=true | all-gather | bytes 136 | tf_op jit(solution)/shard_map/all_gather | solution.py:59
  138.6 1.3 slice_convert_fusion.5
  140.5 1.2 fusion.113
  141.6 1.4 fusion.93
  144.0 5.5 %all_to_all.20 = bf16[2,64,512,16]{2,3,1,0:T(8,128)(2,1)S(1)} all-to-all(bf16[2,64,512,16]{2,3,1,0:T(8,128)(2,1)S(1)} %broadcast_in_dim.27), channel_id=1, replica_groups=mesh['sp_0'=16,'sp_1'=4,'sp_2'=2,'tp'=4] {'sp_2'}, dimensions={0} | all-to-all | bytes 4194304 | tf_op jit(solution)/shard_map/all_to_all | solution.py:25
  149.8 1.5 fusion.118
  151.3 13.6 %all-gather.7.cloned.1.call-done = bf16[2048,1536]{1,0:T(8,128)(2,1)} async-done(((bf16[16,1536]{1,0:T(8,128)(2,1)}), bf16[2048,1536]{1,0:T(8,128)(2,1)}) %all-gather.7.cloned.1.call-update) | async-done | bytes 6291472 | tf_op jit(solution)/shard_map/all_gather | solution.py:37
  164.8 1.8 fusion.124
  166.7 2.1 collective-permute-start.3
  168.8 1.9 fusion.122
  170.8 3.2 collective-permute-start.2
  174.3 1.4 collective-permute-done.2
  176.0 1.4 reshape.306
  177.5 1.5 copy.55
  179.0 2.2 fusion.22
  181.2 18.8 %while.13 = (s32[]{:T(128)}, f32[4,64,128]{2,1,0:T(8,128)S(1)}, f32[8,4,64,128]{3,2,1,0:T(8,128)}, f32[8,4]{1,0:T(8,128)}, f32[8,4,64,128]{3,2,1,0:T(8,128)}, /*index=5*/s32[]{:T(128)}, s32[]{:T(128)}) while((s32[]{:T(128)}, f32[4,64,128]{2,1,0:T(8,128)S(1)}, f32[8,4,64,128]{3,2,1,0:T(8,128)}, f32[8,4]{1,0:T(8,128)}, ...), condition=%wide.region_3.4_spmd.clone, body=%wide.region_2.3_spmd.clone.sunk | while | flops 131075 | bytes 656016 | solution.py:239
  182.5 1.0 bitcast_add_fusion.3
  184.9 1.0 bitcast_add_fusion.3
  187.2 1.0 bitcast_add_fusion.3
  189.6 1.0 bitcast_add_fusion.3
  192.0 1.0 bitcast_add_fusion.3
  194.3 1.0 bitcast_add_fusion.3
  196.7 1.0 bitcast_add_fusion.3
  199.0 1.0 bitcast_add_fusion.3
  200.0 1.9 all-gather.1
  203.3 12.6 %all_gather.35 = bf16[4,4,64,128]{3,2,1,0:T(8,128)(2,1)S(1)} all-gather(bf16[1,4,64,128]{3,2,1,0:T(8,128)(2,1)S(1)} %fusion.92), channel_id=1, replica_groups=mesh['sp_0'=16,'sp_1'=4,'sp_2'=2,'tp'=4] {'sp_1'}, dimensions={0}, use_global_device_ids=true | all-gather | bytes 327680 | tf_op jit(solution)/shard_map/all_gather | solution.py:59
  216.7 1.4 fusion.91
  218.1 1.7 fusion.123
  219.9 1.9 collective-permute-start.4
  221.8 1.9 convolution_convert_fusion.3
  223.8 2.7 convert_multiply_fusion.2
  226.5 1.9 collective-permute-start.1
  228.5 2.1 collective-permute-start
  231.4 1.9 collective-permute-done
  233.9 6.5 %fusion.10 = f32[512,2048]{1,0:T(8,128)} fusion(bf16[256,2048]{0,1:T(8,128)(2,1)} %bitcast.220, bf16[512,2048]{1,0:T(8,128)(2,1)S(1)} %bitcast.215, bf16[2048,1536]{1,0:T(8,128)(2,1)} %all-gather.7.cloned.1.call-done, f32[2,256]{1,0:T(2,128)} %convert_multiply_fusion.3, f32[512,256]{1,0:T(8,128)} %get-tuple-element.121, f32[256]{0:T(256)} %bitcast.230, ...), kind=kOutput, calls=%fused_computation.24 | convolution fusion | flops 1075183616 | bytes 8918016 | tf_op jit(solution)/shard_map/dot_general | solution.py:270
  240.4 2.3 convolution_bitcast_fusion.1
  242.7 44.7 %all-gather.9.cloned.1.call-done = bf16[16,4,64,128]{3,2,1,0:T(8,128)(2,1)} async-done(((bf16[1,4,64,128]{3,2,1,0:T(8,128)(2,1)}), bf16[16,4,64,128]{3,2,1,0:T(8,128)(2,1)}) %all-gather.9.cloned.1.call-update) | async-done | bytes 1048592 | tf_op jit(solution)/shard_map/all_gather | solution.py:59
  287.4 2.1 fusion.90
  289.5 2.7 fusion.5
  292.2 1.6 copy.67
  293.8 1.4 reshape.312
  295.2 2.1 fusion.125
  298.5 2.9 add_convert_fusion
  301.5 20.7 %all_to_all.21 = bf16[4,128,2048]{2,1,0:T(8,128)(2,1)} all-to-all(bf16[4,128,2048]{2,1,0:T(8,128)(2,1)S(1)} %bitcast.217), channel_id=1, replica_groups=mesh['sp_0'=16,'sp_1'=4,'sp_2'=2,'tp'=4] {'tp'}, dimensions={0} | all-to-all | bytes 4194304 | tf_op jit(solution)/shard_map/all_to_all | solution.py:97
  322.2 2.9 reduce_sum.42
  (136 shorter events, 35.3 us)
Async XLA Ops:
  6.5 66.0 %copy-start = (bf16[2048,4]{0,1:T(4,128)(2,1)S(1)}, bf16[2048,4]{0,1:T(4,128)(2,1)}, u32[]{:S(2)}) copy-start(bf16[2048,4]{0,1:T(4,128)(2,1)} %param.32) | copy-start | bytes 49156
  6.5 158.3 %all-gather.7.cloned.1.call-start = ((), (), s32[]{:S(2)}) async-start(), calls=%async_computation.4 | async-start | bytes 6340608 | tf_op jit(solution)/shard_map/all_gather | solution.py:37
  11.4 0.6 copy-start.5
  16.9 4.6 %copy-start.8 = (bf16[256,16]{0,1:T(8,128)(2,1)S(1)}, bf16[256,16]{0,1:T(8,128)(2,1)}, u32[]{:S(2)}) copy-start(bf16[256,16]{0,1:T(8,128)(2,1)} %param.43) | copy-start | bytes 24580
  16.9 4.6 %copy-start.9 = (bf16[256,16]{0,1:T(8,128)(2,1)S(1)}, bf16[256,16]{0,1:T(8,128)(2,1)}, u32[]{:S(2)}) copy-start(bf16[256,16]{0,1:T(8,128)(2,1)} %param.42) | copy-start | bytes 24580
  16.9 30.9 %all-to-all-start = ((bf16[4,128,2048]{2,1,0:T(8,128)(2,1)}), bf16[4,128,2048]{2,1,0:T(8,128)(2,1)S(1)}, u32[]{:S(2)}, u32[]{:S(2)}) async-start(bf16[4,128,2048]{2,1,0:T(8,128)(2,1)} %broadcast_in_dim.23), calls=%async_computation | async-start | bytes 4194304 | tf_op jit(solution)/shard_map/all_to_all | solution.py:25
  21.5 46.7 %copy-start.24 = (bf16[4,128]{1,0:T(4,128)(2,1)S(1)}, bf16[4,128]{1,0:T(4,128)(2,1)}, u32[]{:S(2)}) copy-start(bf16[4,128]{1,0:T(4,128)(2,1)} %param.35) | copy-start | bytes 3076
  21.5 46.7 %copy-start.25 = (bf16[4,128]{1,0:T(4,128)(2,1)S(1)}, bf16[4,128]{1,0:T(4,128)(2,1)}, u32[]{:S(2)}) copy-start(bf16[4,128]{1,0:T(4,128)(2,1)} %param.36) | copy-start | bytes 3076
  21.5 48.6 %copy-start.27 = (f32[4]{0:T(128)S(1)}, f32[4]{0:T(128)}, u32[]{:S(2)}) copy-start(f32[4]{0:T(128)} %param.38) | copy-start | bytes 52
  21.5 49.8 %copy-start.10 = (bf16[3,256]{1,0:T(4,128)(2,1)S(1)}, bf16[3,256]{1,0:T(4,128)(2,1)}, u32[]{:S(2)}) copy-start(bf16[3,256]{1,0:T(4,128)(2,1)} %param.33) | copy-start | bytes 4612
  21.5 50.4 %copy-start.7 = (bf16[4,256]{1,0:T(4,128)(2,1)S(1)}, bf16[4,256]{1,0:T(4,128)(2,1)}, u32[]{:S(2)}) copy-start(bf16[4,256]{1,0:T(4,128)(2,1)} %param.34) | copy-start | bytes 6148
  21.6 51.0 %copy-start.6 = (f32[4,512]{1,0:T(4,128)S(1)}, f32[4,512]{1,0:T(4,128)}, u32[]{:S(2)}) copy-start(f32[4,512]{1,0:T(4,128)} %param.39) | copy-start | bytes 24580
  21.6 50.9 %copy-start.26 = (f32[4]{0:T(128)S(1)}, f32[4]{0:T(128)}, u32[]{:S(2)}) copy-start(f32[4]{0:T(128)} %param.37) | copy-start | bytes 52
  48.9 94.8 %all-to-all-start.1 = ((bf16[64,512,16]{1,2,0:T(8,128)(2,1)}), bf16[64,512,16]{1,2,0:T(8,128)(2,1)S(1)}, u32[]{:S(2)}, u32[]{:S(2)}) async-start(bf16[64,512,16]{1,2,0:T(8,128)(2,1)} %broadcast_in_dim.24), calls=%async_computation.1 | async-start | bytes 2097152 | tf_op jit(solution)/shard_map/all_to_all | solution.py:25
  67.6 219.8 %all-gather.9.cloned.1.call-start = ((), (), s32[]{:S(2)}) async-start(), calls=%async_computation.5 | async-start | bytes 1114112 | tf_op jit(solution)/shard_map/all_gather | solution.py:59
  166.6 7.5 %copy-start.19 = (f32[128]{0:T(128)S(1)}, f32[128]{0:T(128)}, u32[]{:S(2)}) copy-start(f32[128]{0:T(128)} %get-tuple-element.105) | copy-start | bytes 1540
  166.6 7.5 %copy-start.20 = (f32[128]{0:T(128)S(1)}, f32[128]{0:T(128)}, u32[]{:S(2)}) copy-start(f32[128]{0:T(128)} %get-tuple-element.106) | copy-start | bytes 1540
  166.6 7.5 %copy-start.21 = (f32[128]{0:T(128)S(1)}, f32[128]{0:T(128)}, u32[]{:S(2)}) copy-start(f32[128]{0:T(128)} %get-tuple-element.107) | copy-start | bytes 1540
  166.6 7.5 %copy-start.22 = (f32[128]{0:T(128)S(1)}, f32[128]{0:T(128)}, u32[]{:S(2)}) copy-start(f32[128]{0:T(128)} %get-tuple-element.108) | copy-start | bytes 1540
  166.6 9.1 %copy-start.11 = (f32[1,256]{1,0:T(1,128)S(1)}, f32[1,256]{1,0:T(1,128)}, u32[]{:S(2)}) copy-start(f32[1,256]{1,0:T(1,128)} %get-tuple-element.113) | copy-start | bytes 3076
  166.7 9.0 %copy-start.12 = (f32[1,256]{1,0:T(1,128)S(1)}, f32[1,256]{1,0:T(1,128)}, u32[]{:S(2)}) copy-start(f32[1,256]{1,0:T(1,128)} %get-tuple-element.114) | copy-start | bytes 3076
  166.7 9.0 %copy-start.13 = (f32[1,256]{1,0:T(1,128)S(1)}, f32[1,256]{1,0:T(1,128)}, u32[]{:S(2)}) copy-start(f32[1,256]{1,0:T(1,128)} %get-tuple-element.115) | copy-start | bytes 3076
  166.7 9.0 %copy-start.14 = (f32[1,256]{1,0:T(1,128)S(1)}, f32[1,256]{1,0:T(1,128)}, u32[]{:S(2)}) copy-start(f32[1,256]{1,0:T(1,128)} %get-tuple-element.116) | copy-start | bytes 3076
  166.7 7.3 %collective-permute-start.3 = (bf16[3,128]{1,0:T(4,128)(2,1)S(1)}, bf16[3,128]{1,0:T(4,128)(2,1)S(1)}, u32[]{:S(2)}, u32[]{:S(2)}) collective-permute-start(bf16[3,128]{1,0:T(4,128)(2,1)S(1)} %slice.362), channel_id=1, source_target_pairs={{0,4},{4,8},{8,12},{12,16},{16,20},{20,24},{24,28},{28,32},{32,36}... | collective-permute-start | bytes 2312 | tf_op jit(solution)/shard_map/ppermute | solution.py:44
  170.8 4.9 %collective-permute-start.2 = (bf16[3,256]{1,0:T(4,128)(2,1)S(1)}, bf16[3,256]{1,0:T(4,128)(2,1)S(1)}, u32[]{:S(2)}, u32[]{:S(2)}) collective-permute-start(bf16[3,256]{1,0:T(4,128)(2,1)S(1)} %slice.354), channel_id=1, source_target_pairs={{0,4},{4,8},{8,12},{12,16},{16,20},{20,24},{24,28},{28,32},{32,36}... | collective-permute-start | bytes 4616 | tf_op jit(solution)/shard_map/ppermute | solution.py:44
  201.9 0.7 copy-start.4
  216.0 0.7 copy-start.3
  219.9 10.7 %collective-permute-start.4 = (bf16[3,128]{1,0:T(4,128)(2,1)S(1)}, bf16[3,128]{1,0:T(4,128)(2,1)S(1)}, u32[]{:S(2)}, u32[]{:S(2)}) collective-permute-start(bf16[3,128]{1,0:T(4,128)(2,1)S(1)} %slice.367), channel_id=1, source_target_pairs={{0,4},{4,8},{8,12},{12,16},{16,20},{20,24},{24,28},{28,32},{32,36}... | collective-permute-start | bytes 2312 | tf_op jit(solution)/shard_map/ppermute | solution.py:44
  223.8 6.8 %copy-start.15 = (f32[128]{0:T(128)S(1)}, f32[128]{0:T(128)}, u32[]{:S(2)}) copy-start(f32[128]{0:T(128)} %get-tuple-element.109) | copy-start | bytes 1540
  223.8 6.8 %copy-start.16 = (f32[128]{0:T(128)S(1)}, f32[128]{0:T(128)}, u32[]{:S(2)}) copy-start(f32[128]{0:T(128)} %get-tuple-element.110) | copy-start | bytes 1540
  223.8 6.8 %copy-start.17 = (f32[128]{0:T(128)S(1)}, f32[128]{0:T(128)}, u32[]{:S(2)}) copy-start(f32[128]{0:T(128)} %get-tuple-element.111) | copy-start | bytes 1540
  223.8 6.8 %copy-start.18 = (f32[128]{0:T(128)S(1)}, f32[128]{0:T(128)}, u32[]{:S(2)}) copy-start(f32[128]{0:T(128)} %get-tuple-element.112) | copy-start | bytes 1540
  226.5 4.9 %collective-permute-start.1 = (bf16[2,256]{1,0:T(2,128)(2,1)S(1)}, bf16[2,256]{1,0:T(2,128)(2,1)S(1)}, u32[]{:S(2)}, u32[]{:S(2)}) collective-permute-start(bf16[2,256]{1,0:T(2,128)(2,1)S(1)} %slice.347), channel_id=1, source_target_pairs={{0,4},{4,8},{8,12},{12,16},{16,20},{20,24},{24,28},{28,32},{32,36}... | collective-permute-start | bytes 3080 | tf_op jit(solution)/shard_map/ppermute | solution.py:44
  228.5 4.9 %collective-permute-start = (bf16[2,256]{1,0:T(2,128)(2,1)S(1)}, bf16[2,256]{1,0:T(2,128)(2,1)S(1)}, u32[]{:S(2)}, u32[]{:S(2)}) collective-permute-start(bf16[2,256]{1,0:T(2,128)(2,1)S(1)} %slice.346), channel_id=1, source_target_pairs={{0,4},{4,8},{8,12},{12,16},{16,20},{20,24},{24,28},{28,32},{32,36}... | collective-permute-start | bytes 3080 | tf_op jit(solution)/shard_map/ppermute | solution.py:44
  287.4 2.1 copy-start.2
  297.3 1.2 copy-start.1
  297.3 1.2 copy-start.23
Sparse Core Ops, SparseCore 0:
  12.2 152.5 all-gather.6
  218.2 69.1 all-gather.8
where the time goes:
time: 334 us; the launch traced here: 332 us
  waiting for transfers between devices  88.5 us (26%)
  blocking collectives  86.2 us (26%)
  local copies, waits for them, and re-layouts  39.4 us (12%)
  other arithmetic  38.3 us (11%)
  starting transfers between devices  34.6 us (10%)
  matrix products  30.1 us (9%)
  between operations  14.6 us (4%)
    all_gather x4, blocking collectives, prefix_by_axis(): lax.all_gather(part.astype(kind), axis)  56.9 us
    all_gather x1, waiting for transfers between devices, prefix_by_axis(): lax.all_gather(part.astype(kind), axis)  44.7 us
    all_to_all x2, waiting for transfers between devices, copy_for_each(): lax.all_to_all(jnp.broadcast_to(shard[None], (devices, *shard.shape)), ax...  26.2 us
    all_to_all x2, starting transfers between devices, copy_for_each(): lax.all_to_all(jnp.broadcast_to(shard[None], (devices, *shard.shape)), ax...  23.2 us
    all_to_all x1, blocking collectives, summed_on_arrival(): lax.all_to_all(tiles, axis, split_axis=0, concat_axis=0, tiled=True)  20.7 us
    all_gather x1, waiting for transfers between devices, side_by_side(): whole = lax.all_gather(both, axis, axis=dim, tiled=True)  13.6 us
    dot_general x6, matrix products, per_device(): jnp.dot(normed, weight_rows, preferred_element_type=jnp.float32)  12.2 us
    ppermute x5, starting transfers between devices, shifted(): return lax.ppermute(shard, axis, pairs)  11.3 us
  transfers between devices with their start and end apart: 9, of which 6 were waited for; matrix products, arithmetic and copies ran while one was open for 17% of the time, Pallas kernels for 0%

commit v1 on v0

v1 whole, which is shorter than its diff:
```python
import jax
import jax.numpy as jnp
from jax import lax
from jax.experimental import pallas as pl
from jax.experimental.pallas import tpu as pltpu
from jax.sharding import Mesh
from jax.sharding import PartitionSpec as P

SP = ("z", "x", "c")
SP_TP = ("z", "x", "c", "tp")
EPS = 1e-05
ROWS = 512
HALO = 16
BLK = 128
NB = ROWS // BLK
F32 = jnp.float32
BF16 = jnp.bfloat16


def call(body, outs, args, specs=None, scratch=()):
    vmem = pl.BlockSpec(memory_space=pltpu.VMEM)
    specs = specs or {}
    return pl.pallas_call(
        body,
        out_shape=outs,
        in_specs=[specs.get(i, vmem) for i in range(len(args))],
        out_specs=jax.tree.map(lambda _: vmem, outs),
        scratch_shapes=list(scratch),
    )(*args)


HBM = pl.BlockSpec(memory_space=pltpu.HBM)
SMEM = pl.BlockSpec(memory_space=pltpu.SMEM)


def shape(dims, kind):
    return jax.ShapeDtypeStruct(dims, kind)


def dot(a, b):
    return jnp.dot(a, b, preferred_element_type=F32)


def dot_nt(a, b):
    return lax.dot_general(a, b, (((1,), (1,)), ((), ())), preferred_element_type=F32)


def per_head(v):
    rows = v.shape[0]
    low = lax.broadcasted_iota(jnp.int32, (rows, 128), 1) < 64
    pairs = [
        jnp.where(
            low,
            jnp.broadcast_to(v[:, 2 * p : 2 * p + 1], (rows, 128)),
            jnp.broadcast_to(v[:, 2 * p + 1 : 2 * p + 2], (rows, 128)),
        )
        for p in range(2)
    ]
    return jnp.concatenate(pairs, axis=1)


def silu(v):
    return v / (1.0 + jnp.exp(-v))


def assemble(c, own, other, whole, sems, wait):
    for x in range(4):
        for side, src in ((0, own), (1, other)):
            at = c if side == 0 else 1 - c
            copy = pltpu.make_async_copy(
                src.at[x], whole.at[:, x, at], sems.at[2 * x + side]
            )
            if wait:
                copy.wait()
            else:
                copy.start()


def taps(ref, weights, cols, count):
    w = weights[...].astype(F32)
    out = None
    for k in range(count):
        part = w[k : k + 1, :] * ref[pl.ds(HALO - count + 1 + k, ROWS), cols]
        out = part if out is None else out + part
    return out


def norm_body(tok, halo, gain, ws, bias, rate, spikes, normed, dt, cum, cum_t):
    g = gain[...].astype(F32)

    def rows_of(v):
        f = v.astype(F32)
        scaled = f * lax.rsqrt(jnp.mean(f * f, axis=1, keepdims=True) + EPS)
        return (scaled * g).astype(BF16)

    normed[0:HALO, :] = rows_of(halo[...])
    for y in range(4):

        def some(i, _, y=y):
            at = pl.multiple_of(i * 16, 16)
            to = pl.multiple_of(HALO + y * 128 + i * 16, 16)
            normed[pl.ds(to, 16), :] = rows_of(tok[y, pl.ds(at, 16), :])
            return 0

        lax.fori_loop(0, 8, some, 0, unroll=2)
    raw = dot(normed[HALO:, :], ws[...]) + bias[...]
    step = jnp.maximum(raw, 0.0) + jnp.log1p(jnp.exp(-jnp.abs(raw)))
    dt[...] = step
    logs = -step * jnp.exp(rate[...]) + spikes[...]
    r = lax.broadcasted_iota(jnp.int32, (BLK, BLK), 0)
    s = lax.broadcasted_iota(jnp.int32, (BLK, BLK), 1)
    lower = jnp.where(r >= s, 1.0, 0.0).astype(F32)
    carry = jnp.zeros((1, 128), F32)
    for b in range(NB):
        part = (
            jnp.dot(
                lower,
                logs[b * BLK : (b + 1) * BLK],
                precision=lax.Precision.HIGHEST,
                preferred_element_type=F32,
            )
            + carry
        )
        cum[b * BLK : (b + 1) * BLK, :] = part
        cum_t[:, b * BLK : (b + 1) * BLK] = part.T[0:8, :]
        carry = part[BLK - 1 : BLK, :]


def first_body(
    c_ref, normed, own, other, dt, cum, input_taps, write_taps,
    weighted, seq_input, seq_write, local, pieces,
    whole, fields, sems,
):
    c = c_ref[0]
    assemble(c, own, other, whole, sems, False)
    assemble(c, own, other, whole, sems, True)
    projected = dot(normed[...], whole[...].reshape(2048, 384))
    fields[...] = projected.astype(BF16).astype(F32)
    xin = silu(taps(fields, input_taps, slice(0, 256), 4))
    write = silu(taps(fields, write_taps, slice(256, 384), 4))
    seq_input[...] = xin
    seq_write[...] = write.astype(BF16)
    scaled = xin * per_head(dt[:, 0:128])
    weighted[...] = scaled.astype(BF16)
    state = jnp.zeros((128, 256), F32)
    before = jnp.zeros((1, 128), F32)
    for b in range(NB):
        rows = slice(b * BLK, (b + 1) * BLK)
        end = cum[(b + 1) * BLK - 1 : (b + 1) * BLK, :]
        local[b] = state.astype(BF16)
        to_end = per_head(jnp.exp(end - cum[rows, :]))
        added = dot(write[rows].T.astype(BF16), (scaled[rows] * to_end).astype(BF16))
        state = state * per_head(jnp.exp(end - before)) + added
        before = end
    decay = per_head(jnp.exp(before))
    high = decay.astype(BF16).astype(F32)
    low = decay - high
    tail = jnp.where(
        lax.broadcasted_iota(jnp.int32, (8, 256), 0) < 4,
        jnp.broadcast_to(high, (8, 256)),
        jnp.broadcast_to(low, (8, 256)),
    ).astype(BF16)
    for j in range(8):
        pieces[j, 0:16, :] = state[16 * j : 16 * (j + 1)].astype(BF16)
        pieces[j, 16:24, :] = tail


def piece_of(ref, j):
    v = ref[j].astype(F32)
    return v[0:16], v[16:17] + v[20:21]


def plane_body(got, send):
    state = jnp.zeros((16, 256), F32)
    decay = jnp.ones((1, 256), F32)
    for j in range(8):
        s, d = piece_of(got, j)
        state = state * d + s
        decay = decay * d
    high = decay.astype(BF16).astype(F32)
    tail = jnp.where(
        lax.broadcasted_iota(jnp.int32, (8, 256), 0) < 4,
        jnp.broadcast_to(high, (8, 256)),
        jnp.broadcast_to(decay - high, (8, 256)),
    )
    one = jnp.concatenate([state, tail], axis=0).astype(BF16)
    for k in range(16):
        send[k] = one


def enter_body(z_ref, got, planes, out):
    z = z_ref[0]
    state = jnp.zeros((16, 256), F32)
    for k in range(16):
        s, d = piece_of(planes, k)
        state = jnp.where(k < z, state * d + s, state)
    for j in range(8):
        out[j] = state.astype(BF16)
        s, d = piece_of(got, j)
        state = state * d + s


def rest_body(
    c_ref, normed, own, other, weighted, seq_input, seq_write, local, cum, cum_t,
    read_taps, gated_taps, direct,
    partly, read_out, gate, mixer,
    whole, fields, sems,
):
    c = c_ref[0]
    assemble(c, own, other, whole, sems, False)
    assemble(c, own, other, whole, sems, True)
    n = normed[...]

    def projected(lo, hi):
        w = whole[:, :, :, :, lo:hi].reshape(2048, hi - lo)
        return dot(n, w).astype(BF16).astype(F32)

    fields[:, 0:128] = projected(0, 128)
    read = silu(taps(fields, read_taps, slice(0, 128), 4)).astype(BF16)
    read_out[...] = read
    gate[...] = silu(projected(128, 384)[HALO:])
    inner = projected(640, 896)
    fields[...] = inner * projected(896, 1152)
    outer = projected(384, 640)[HALO:]
    mixer[...] = (outer * taps(fields, gated_taps, slice(0, 256), 3)).astype(BF16)
    r = lax.broadcasted_iota(jnp.int32, (BLK, BLK), 0)
    s = lax.broadcasted_iota(jnp.int32, (BLK, BLK), 1)
    causal = r >= s
    low = s < 64
    before = jnp.zeros((1, 128), F32)
    for b in range(NB):
        rows = slice(b * BLK, (b + 1) * BLK)
        rb = read[rows]
        scores = dot_nt(rb, seq_write[rows, :])
        here = cum[rows, :]
        from_local = dot(rb, local[b]) * per_head(jnp.exp(here - before))
        before = here[BLK - 1 : BLK, :]
        halves = []
        for p in range(2):
            pair = weighted[rows, 128 * p : 128 * (p + 1)]
            two = []
            for h in (2 * p, 2 * p + 1):
                gap = here[:, h : h + 1] - cum_t[h : h + 1, rows]
                damped = scores * jnp.exp(jnp.where(causal, gap, -jnp.inf))
                two.append(dot(damped.astype(BF16), pair))
            halves.append(jnp.where(low, two[0], two[1]))
        within = jnp.concatenate(halves, axis=1)
        partly[rows, :] = within + from_local + direct[...] * seq_input[rows, :]


def tail_body(
    c_ref, arriving, partly, read, gate, cum, mixer, scale, own, other,
    out,
    whole, act, sems,
):
    c = c_ref[0]
    assemble(c, own, other, whole, sems, False)
    act[:, 0:256] = mixer[...]
    head = partly[...] + dot(read[...], arriving[...]) * per_head(jnp.exp(cum[...]))
    gated = head * gate[...]
    square = gated * gated
    r = lax.broadcasted_iota(jnp.int32, (256, 256), 0) // 64
    s = lax.broadcasted_iota(jnp.int32, (256, 256), 1) // 64
    same = jnp.where(r == s, 1.0 / 64.0, 0.0).astype(BF16)
    high = square.astype(BF16)
    rest = (square - high.astype(F32)).astype(BF16)
    mean = dot(high, same) + dot(rest, same)
    act[:, 256:512] = (gated * lax.rsqrt(mean + EPS) * scale[...].astype(F32)).astype(BF16)
    assemble(c, own, other, whole, sems, True)
    w = whole[...].reshape(2048, 512)
    a = act[...]
    for q in range(4):
        cols = slice(512 * q, 512 * (q + 1))
        out[:, cols] = dot_nt(a, w[cols]).astype(BF16)


def sum_body(got, out):
    v = got[0].astype(F32)
    for y in range(1, 4):
        v = v + got[y].astype(F32)
    out[...] = v.astype(BF16)


def copies(shard, axis):
    n = lax.axis_size(axis)
    return lax.all_to_all(
        jnp.broadcast_to(shard[None], (n, *shard.shape)), axis, 0, 0, tiled=True
    )


def swapped(shard):
    return lax.ppermute(shard, "c", [(0, 1), (1, 0)])


def lanes(v, width=128):
    return jnp.pad(v, ((0, 0), (0, width - v.shape[1])))


def per_device(
    tokens,
    input_norm_scale,
    outer_gate_weight,
    inner_gate_weight,
    value_weight_matrix,
    output_gate_weight,
    state_input_weight,
    write_key_weight,
    read_key_weight,
    step_size_weight,
    gated_conv_weight,
    input_conv_weight,
    write_conv_weight,
    read_conv_weight,
    step_size_bias,
    log_decay_rate,
    decay_spikes,
    direct_path_weight,
    head_norm_scale,
    conv_output_weight,
    state_output_weight,
):
    c = lax.axis_index("c").astype(jnp.int32).reshape(1)
    z = lax.axis_index("z").astype(jnp.int32).reshape(1)
    tok = copies(tokens, "tp")
    own_in = jnp.concatenate(
        [
            state_input_weight,
            write_key_weight,
            read_key_weight,
            output_gate_weight,
            outer_gate_weight,
            inner_gate_weight,
            value_weight_matrix,
        ],
        axis=1,
    )
    column = lax.all_gather(own_in, "z", axis=0, tiled=False)
    first = copies(column[:, :, :384], "x")
    first_other = swapped(first)
    rest = copies(column[:, :, 384:], "x")
    rest_other = swapped(rest)
    own_out = jnp.concatenate([conv_output_weight, state_output_weight], axis=0).T
    wide = copies(copies(own_out, "z"), "x")
    wide_other = swapped(wide)
    steps = 128
    halo = lax.ppermute(tok[3, 112:, :], SP, [(i, i + 1) for i in range(steps - 1)])

    normed, dt, cum, cum_t = call(
        norm_body,
        (
            shape((HALO + ROWS, 2048), BF16),
            shape((ROWS, 128), F32),
            shape((ROWS, 128), F32),
            shape((8, ROWS), F32),
        ),
        (
            tok,
            halo,
            input_norm_scale[None],
            lanes(step_size_weight),
            lanes(step_size_bias[None]),
            lanes(log_decay_rate[None]),
            lanes(decay_spikes.T),
        ),
    )
    weighted, seq_input, seq_write, local, pieces = call(
        first_body,
        (
            shape((ROWS, 256), BF16),
            shape((ROWS, 256), F32),
            shape((ROWS, 128), BF16),
            shape((NB, 128, 256), BF16),
            shape((8, 24, 256), BF16),
        ),
        (c, normed, first, first_other, dt, cum, input_conv_weight, write_conv_weight),
        {0: SMEM, 2: HBM, 3: HBM},
        (
            pltpu.VMEM((16, 4, 2, 16, 384), BF16),
            pltpu.VMEM((HALO + ROWS, 384), F32),
            pltpu.SemaphoreType.DMA((8,)),
        ),
    )
    got = lax.all_to_all(pieces, ("x", "c"), 0, 0, tiled=True)
    planes = lax.all_to_all(
        call(plane_body, shape((16, 24, 256), BF16), (got,)), "z", 0, 0, tiled=True
    )
    entering = call(enter_body, shape((8, 16, 256), BF16), (z, got, planes), {0: SMEM})
    arriving = lax.all_to_all(entering, ("x", "c"), 0, 0, tiled=True).reshape(128, 256)

    direct = jnp.repeat(direct_path_weight, 64)[None]
    partly, read, gate, mixer = call(
        rest_body,
        (
            shape((ROWS, 256), F32),
            shape((ROWS, 128), BF16),
            shape((ROWS, 256), F32),
            shape((ROWS, 256), BF16),
        ),
        (
            c, normed, rest, rest_other, weighted, seq_input, seq_write, local, cum, cum_t,
            read_conv_weight, gated_conv_weight, direct,
        ),
        {0: SMEM, 2: HBM, 3: HBM},
        (
            pltpu.VMEM((16, 4, 2, 16, 1152), BF16),
            pltpu.VMEM((HALO + ROWS, 256), F32),
            pltpu.SemaphoreType.DMA((8,)),
        ),
    )
    partial = call(
        tail_body,
        shape((ROWS, 2048), BF16),
        (c, arriving, partly, read, gate, cum, mixer, head_norm_scale[None], wide, wide_other),
        {0: SMEM, 8: HBM, 9: HBM},
        (
            pltpu.VMEM((16, 4, 2, 16, 512), BF16),
            pltpu.VMEM((ROWS, 512), BF16),
            pltpu.SemaphoreType.DMA((8,)),
        ),
    )
    parts = lax.all_to_all(partial.reshape(4, 128, 2048), "tp", 0, 0, tiled=True)
    return call(sum_body, shape((128, 2048), BF16), (parts,))


def solution(mesh):
    torus = Mesh(mesh.devices.reshape(16, 4, 2, mesh.shape["tp"]), SP_TP)
    rows = P(SP, "tp")
    cols = P("tp", SP)
    taps_ = P(None, "tp")
    heads = P("tp")
    return jax.shard_map(
        per_device,
        mesh=torus,
        in_specs=(
            P(SP_TP, None), P(), rows, rows, rows, rows, rows, rows, rows,
            taps_, taps_, taps_, taps_, taps_, heads, heads, cols, heads, heads, cols, cols,
        ),
        out_specs=P(SP_TP, None),
        check_vma=False,
    )
```

time: 334 us -> 263 us (0.79)
  the two profiles are of different devices: /device:TPU:2 before, /device:TPU:1 now
where the time goes in v1:
time: 263 us; the launch traced here: 262 us
  blocking collectives  113 us (43%)
  starting transfers between devices  59.3 us (23%)
  waiting for transfers between devices  33.4 us (13%)
  Pallas kernels  32.8 us (12%)
  local copies, waits for them, and re-layouts  22.8 us (9%)
    all_to_all x2, blocking collectives, copies(): lax.all_to_all(jnp.broadcast_to(shard[None], (n, *shard.shape)), axis, 0,...  37.5 us
    all_gather x1, blocking collectives, per_device(): column = lax.all_gather(own_in, 'z', axis=0, tiled=False)  33.9 us
    pallas_call x7, Pallas kernels, call(): pl.pallas_call(body, out_shape=outs, in_specs=[specs.get(i, vmem) for i i...  32.8 us
    all_to_all x1, blocking collectives, per_device(): lax.all_to_all(partial.reshape(4, 128, 2048), 'tp', 0, 0, tiled=True)  30.5 us
    all_to_all x3, waiting for transfers between devices, copies(): lax.all_to_all(jnp.broadcast_to(shard[None], (n, *shard.shape)), axis, 0,...  21 us
    ppermute x3, starting transfers between devices, swapped(): return lax.ppermute(shard, 'c', [(0, 1), (1, 0)])  19 us
    all_to_all x3, starting transfers between devices, copies(): lax.all_to_all(jnp.broadcast_to(shard[None], (n, *shard.shape)), axis, 0,...  14.9 us
    ppermute x1, starting transfers between devices, per_device(): lax.ppermute(tok[3, 112:, :], SP, [(i, i + 1) for i in range(steps - 1)])  12.4 us
  transfers between devices with their start and end apart: 9, of which 3 were waited for; matrix products, arithmetic and copies ran while one was open for 5% of the time, Pallas kernels for 9%

profile of v1, /device:TPU:1, one launch (start us, length us, event | category | flops | bytes accessed | tf_op | source)
XLA Modules:
  0.0 261.6 jit_solution(9367044819234571286)
XLA Ops:
  0.0 0.7 constant_dynamic-update-slice_fusion.6
  0.7 0.7 constant_dynamic-update-slice_fusion.5
  1.4 0.7 constant_dynamic-update-slice_fusion.4
  2.1 0.7 constant_dynamic-update-slice_fusion.3
  2.8 0.7 constant_dynamic-update-slice_fusion.2
  3.5 0.7 constant_dynamic-update-slice_fusion.1
  4.2 0.7 constant_dynamic-update-slice_fusion
  4.9 33.9 %all-gather = bf16[256,1536]{1,0:T(8,128)(2,1)S(1)} all-gather(bf16[16,1536]{1,0:T(8,128)(2,1)S(1)} %constant_dynamic-update-slice_fusion), channel_id=2, replica_groups=mesh['z'=16,'x'=4,'c'=2,'tp'=4] {'z'}, dimensions={0}, use_global_device_ids=true | all-gather | bytes 835584 | tf_op jit(solution)/shard_map/all_gather | solution.py:337
  38.8 1.0 broadcast_in_dim.24
  39.8 4.0 %all-to-all-start.1 = ((bf16[4,16,16,384]{3,2,1,0:T(8,128)(2,1)}), bf16[4,16,16,384]{3,2,1,0:T(8,128)(2,1)S(1)}, u32[]{:S(2)}, u32[]{:S(2)}) async-start(bf16[4,16,16,384]{3,2,1,0:T(8,128)(2,1)} %broadcast_in_dim.24), calls=%async_computation.1 | async-start | bytes 1572864 | tf_op jit(solution)/shard_map/all_to_all | solution.py:286
  43.8 0.0 copy-done.9
  43.8 8.3 %all-to-all-done.1.own = bf16[4,16,16,384]{3,2,1,0:T(8,128)(2,1)S(1)} async-done(((bf16[4,16,16,384]{3,2,1,0:T(8,128)(2,1)}), bf16[4,16,16,384]{3,2,1,0:T(8,128)(2,1)S(1)}, u32[]{:S(2)}, u32[]{:S(2)}) %all-to-all-start.1) | async-done | bytes 786464 | tf_op jit(solution)/shard_map/all_to_all | solution.py:286
  52.1 0.8 broadcast_in_dim.53
  52.9 6.3 %all-to-all-start.6 = ((bf16[16,16,512]{2,1,0:T(8,128)(2,1)}), bf16[16,16,512]{2,1,0:T(8,128)(2,1)S(1)}, u32[]{:S(2)}, u32[]{:S(2)}) async-start(bf16[16,16,512]{2,1,0:T(8,128)(2,1)} %broadcast_in_dim.53), calls=%async_computation.6 | async-start | bytes 524288 | tf_op jit(solution)/shard_map/all_to_all | solution.py:286
  59.3 12.7 %all-to-all-done.6 = bf16[16,16,512]{2,1,0:T(8,128)(2,1)S(1)} async-done(((bf16[16,16,512]{2,1,0:T(8,128)(2,1)}), bf16[16,16,512]{2,1,0:T(8,128)(2,1)S(1)}, u32[]{:S(2)}, u32[]{:S(2)}) %all-to-all-start.6) | async-done | bytes 262176 | tf_op jit(solution)/shard_map/all_to_all | solution.py:286
  71.9 0.7 copy-done.3
  72.6 0.2 broadcast_in_dim.50
  72.8 0.0 copy-start.4
  72.8 21.1 %all_to_all.45.own = bf16[4,16,16,1152]{3,2,1,0:T(8,128)(2,1)S(1)} all-to-all(bf16[4,16,16,1152]{3,2,1,0:T(8,128)(2,1)S(1)} %broadcast_in_dim.50), channel_id=1, replica_groups=mesh['z'=16,'x'=4,'c'=2,'tp'=4] {'x'}, dimensions={0} | all-to-all | bytes 4718592 | tf_op jit(solution)/shard_map/all_to_all | solution.py:286
  93.9 0.1 broadcast_in_dim.54
  94.0 16.4 %all_to_all.46.own = bf16[4,16,16,512]{3,2,1,0:T(8,128)(2,1)S(1)} all-to-all(bf16[4,16,16,512]{3,2,1,0:T(8,128)(2,1)S(1)} %broadcast_in_dim.54), channel_id=1, replica_groups=mesh['z'=16,'x'=4,'c'=2,'tp'=4] {'x'}, dimensions={0} | all-to-all | bytes 2097152 | tf_op jit(solution)/shard_map/all_to_all | solution.py:286
  110.5 1.7 broadcast_in_dim.20
  112.2 4.6 %all-to-all-start = ((bf16[4,128,2048]{2,1,0:T(8,128)(2,1)}), bf16[4,128,2048]{2,1,0:T(8,128)(2,1)}, u32[]{:S(2)}, u32[]{:S(2)}) async-start(bf16[4,128,2048]{2,1,0:T(8,128)(2,1)} %broadcast_in_dim.20), calls=%async_computation | async-start | bytes 4194304 | tf_op jit(solution)/shard_map/all_to_all | solution.py:286
  116.7 0.0 copy-done
  116.8 14.7 %collective-permute-start.2 = (bf16[4,16,16,1152]{3,2,1,0:T(8,128)(2,1)S(1)}, bf16[4,16,16,1152]{3,2,1,0:T(8,128)(2,1)}, u32[]{:S(2)}, u32[]{:S(2)}) collective-permute-start(bf16[4,16,16,1152]{3,2,1,0:T(8,128)(2,1)S(1)} %all_to_all.45.own), channel_id=1, source_target_pairs={{0,4},{4,0},{1,5},{5,1},{2,6},{6,2},{3,7},{7,3},{8,12},{12,8},{9,1... | collective-permute-start | bytes 7077896 | tf_op jit(solution)/shard_map/ppermute | solution.py:292
  131.5 1.9 collective-permute-start.1
  133.4 0.0 copy-done.1
  133.4 2.4 collective-permute-start.3
  135.8 0.0 all-to-all-done.tok
  135.8 0.8 slice_bitcast_fusion
  136.7 12.4 %collective-permute-start = (bf16[16,2048]{1,0:T(8,128)(2,1)S(1)}, bf16[16,2048]{1,0:T(8,128)(2,1)S(1)}, u32[]{:S(2)}, u32[]{:S(2)}) collective-permute-start(bf16[16,2048]{1,0:T(8,128)(2,1)S(1)} %slice_bitcast_fusion), channel_id=1, source_target_pairs={{0,4},{4,8},{8,12},{12,16},{16,20},{20,24},{24,28},{28,32},{32,36}... | collective-permute-start | bytes 196616 | tf_op jit(solution)/shard_map/ppermute | solution.py:346
  149.1 1.3 broadcast_in_dim.21.gain
  150.4 0.0 copy-done.8
  150.4 1.1 copy.22
  151.4 1.2 pad.16.bias
  152.7 1.2 pad.17.rate
  153.9 1.6 copy.23
  155.5 1.7 pad.18.spikes
  157.2 2.0 pad.15.ws
  159.1 0.0 collective-permute-done.halo
  159.1 0.6 copy-done.7
  159.8 6.1 %shard_map.199 = (bf16[528,2048]{1,0:T(8,128)(2,1)}, f32[512,128]{1,0:T(8,128)}, f32[512,128]{1,0:T(8,128)}, f32[8,512]{1,0:T(8,128)}) custom-call(bf16[4,128,2048]{2,1,0:T(8,128)(2,1)} %all-to-all-done.tok, bf16[16,2048]{1,0:T(8,128)(2,1)} %copy-done.7, bf16[1,2048]{1,0:T(2,128)(2,1)} %broadcast_in_dim.21.gain, bf16[2048,128]{1,0:T(8,128)(2,1)} %pad.15.ws, ...), custom_call_target="tpu_custom_call" | custom-call | tf_op jit(solution)/shard_map/pallas_call | solution.py:23
  165.9 0.0 collective-permute-done.1.other
  165.9 0.0 copy-start.12
  165.9 6.4 %shard_map.200 = (bf16[512,256]{1,0:T(8,128)(2,1)}, f32[512,256]{1,0:T(8,128)}, bf16[512,128]{1,0:T(8,128)(2,1)}, bf16[4,128,256]{2,1,0:T(8,128)(2,1)}, bf16[8,24,256]{2,1,0:T(8,128)(2,1)}) custom-call(s32[1]{0:T(128)} %bitcast.c_ref, bf16[528,2048]{1,0:T(8,128)(2,1)} %get-tuple-element.18.normed, bf16[4,16,16,384]{3,2,1,0:T(8,128)(2,1)} %copy-done.2, ...), custom_call_target="tpu_custom_call" | custom-call | tf_op jit(solution)/shard_map/pallas_call | solution.py:23
  172.3 11.2 %all_to_all.47.got = bf16[8,24,256]{2,1,0:T(8,128)(2,1)} all-to-all(bf16[8,24,256]{2,1,0:T(8,128)(2,1)} %get-tuple-element.21), channel_id=1, replica_groups=mesh['z'=16,'x'=4,'c'=2,'tp'=4] {'x','c'}, dimensions={0} | all-to-all | bytes 196608 | tf_op jit(solution)/shard_map/all_to_all | solution.py:383
  183.6 1.6 shard_map.201
  185.2 4.7 %all-to-all-start.3 = ((bf16[16,24,256]{2,1,0:T(8,128)(2,1)}), bf16[16,24,256]{2,1,0:T(8,128)(2,1)}, u32[]{:S(2)}, u32[]{:S(2)}) async-start(bf16[16,24,256]{2,1,0:T(8,128)(2,1)} %shard_map.201), calls=%async_computation.3 | async-start | bytes 393216 | tf_op jit(solution)/shard_map/all_to_all | solution.py:384
  189.9 12.4 %all-to-all-done.3.planes = bf16[16,24,256]{2,1,0:T(8,128)(2,1)} async-done(((bf16[16,24,256]{2,1,0:T(8,128)(2,1)}), bf16[16,24,256]{2,1,0:T(8,128)(2,1)}, u32[]{:S(2)}, u32[]{:S(2)}) %all-to-all-start.3) | async-done | bytes 196640 | tf_op jit(solution)/shard_map/all_to_all | solution.py:384
  202.3 1.7 shard_map.202
  203.9 8.2 %all-to-all-start.4 = ((bf16[8,16,256]{2,1,0:T(8,128)(2,1)}), bf16[8,16,256]{2,1,0:T(8,128)(2,1)S(1)}, u32[]{:S(2)}, u32[]{:S(2)}) async-start(bf16[8,16,256]{2,1,0:T(8,128)(2,1)} %shard_map.202), calls=%async_computation.4 | async-start | bytes 131072 | tf_op jit(solution)/shard_map/all_to_all | solution.py:388
  212.2 0.1 broadcast_in_dim.51
  212.3 0.7 broadcast_in_dim_reshape.3.direct
  212.9 0.0 copy-done.12
  212.9 0.5 broadcast_in_dim.52.scale
  213.4 0.0 collective-permute-done.2.other
  213.4 8.8 %shard_map.203 = (f32[512,256]{1,0:T(8,128)}, bf16[512,128]{1,0:T(8,128)(2,1)}, f32[512,256]{1,0:T(8,128)}, bf16[512,256]{1,0:T(8,128)(2,1)}) custom-call(s32[1]{0:T(128)} %bitcast.c_ref, bf16[528,2048]{1,0:T(8,128)(2,1)} %get-tuple-element.18.normed, bf16[4,16,16,1152]{3,2,1,0:T(8,128)(2,1)} %copy-done, ...), custom_call_target="tpu_custom_call" | custom-call | tf_op jit(solution)/shard_map/pallas_call | solution.py:23
  222.2 0.0 all-to-all-done.4
  222.2 0.0 copy-start.6
  222.2 0.0 collective-permute-done.3.other
  222.2 0.6 copy-done.6
  222.9 5.6 %shard_map.204 = bf16[512,2048]{1,0:T(8,128)(2,1)} custom-call(s32[1]{0:T(128)} %bitcast.c_ref, bf16[128,256]{1,0:T(8,128)(2,1)} %bitcast.16, f32[512,256]{1,0:T(8,128)} %get-tuple-element.27.partly, bf16[512,128]{1,0:T(8,128)(2,1)} %get-tuple-element.28.read, f32[512,256]{1,0:T(8,128)} %get-tuple-element.29.gate, f32[512,128]{1,0:T(8,128)} %get-tuple-element.20.cum, ...), custom_call_target="tpu_custom_call" | custom-call | tf_op jit(solution)/shard_map/pallas_call | solution.py:23
  228.5 30.5 %all_to_all.48.got = bf16[4,128,2048]{2,1,0:T(8,128)(2,1)} all-to-all(bf16[4,128,2048]{2,1,0:T(8,128)(2,1)} %bitcast.12), channel_id=1, replica_groups=mesh['z'=16,'x'=4,'c'=2,'tp'=4] {'tp'}, dimensions={0} | all-to-all | bytes 4194304 | tf_op jit(solution)/shard_map/all_to_all | solution.py:421
  259.0 2.6 %shard_map.205 = bf16[128,2048]{1,0:T(8,128)(2,1)} custom-call(bf16[4,128,2048]{2,1,0:T(8,128)(2,1)} %all_to_all.48.got), custom_call_target="tpu_custom_call" | custom-call | tf_op jit(solution)/shard_map/pallas_call | solution.py:23
  (18 shorter events, 0.1 us)
Async XLA Ops:
  0.0 43.8 %copy-start.9 = (bf16[256,16]{0,1:T(8,128)(2,1)S(1)}, bf16[256,16]{0,1:T(8,128)(2,1)}, u32[]{:S(2)}) copy-start(bf16[256,16]{0,1:T(8,128)(2,1)} %param.41) | copy-start | bytes 24580
  0.0 43.8 %copy-start.10 = (bf16[256,16]{0,1:T(8,128)(2,1)S(1)}, bf16[256,16]{0,1:T(8,128)(2,1)}, u32[]{:S(2)}) copy-start(bf16[256,16]{0,1:T(8,128)(2,1)} %param.40) | copy-start | bytes 24580
  39.8 12.4 %all-to-all-start.1 = ((bf16[4,16,16,384]{3,2,1,0:T(8,128)(2,1)}), bf16[4,16,16,384]{3,2,1,0:T(8,128)(2,1)S(1)}, u32[]{:S(2)}, u32[]{:S(2)}) async-start(bf16[4,16,16,384]{3,2,1,0:T(8,128)(2,1)} %broadcast_in_dim.24), calls=%async_computation.1 | async-start | bytes 1572864 | tf_op jit(solution)/shard_map/all_to_all | solution.py:286
  52.1 20.7 %copy-start.2 = (bf16[4,16,16,384]{3,2,1,0:T(8,128)(2,1)}, bf16[4,16,16,384]{3,2,1,0:T(8,128)(2,1)S(1)}, u32[]{:S(2)}) copy-start(bf16[4,16,16,384]{3,2,1,0:T(8,128)(2,1)S(1)} %all-to-all-done.1.own) | copy-start | bytes 2359300
  52.9 19.0 %all-to-all-start.6 = ((bf16[16,16,512]{2,1,0:T(8,128)(2,1)}), bf16[16,16,512]{2,1,0:T(8,128)(2,1)S(1)}, u32[]{:S(2)}, u32[]{:S(2)}) async-start(bf16[16,16,512]{2,1,0:T(8,128)(2,1)} %broadcast_in_dim.53), calls=%async_computation.6 | async-start | bytes 524288 | tf_op jit(solution)/shard_map/all_to_all | solution.py:286
  71.9 0.7 copy-start.3
  72.8 21.1 %copy-start.4 = (bf16[16,16,512]{2,1,0:T(8,128)(2,1)S(1)}, bf16[16,16,512]{2,1,0:T(8,128)(2,1)}, u32[]{:S(2)}) copy-start(bf16[16,16,512]{2,1,0:T(8,128)(2,1)} %copy-done.3) | copy-start | bytes 786436
  93.9 22.8 %copy-start = (bf16[4,16,16,1152]{3,2,1,0:T(8,128)(2,1)}, bf16[4,16,16,1152]{3,2,1,0:T(8,128)(2,1)S(1)}, u32[]{:S(2)}) copy-start(bf16[4,16,16,1152]{3,2,1,0:T(8,128)(2,1)S(1)} %all_to_all.45.own) | copy-start | bytes 7077892
  93.9 16.6 %copy-start.5 = (bf16[128,2048]{1,0:T(8,128)(2,1)S(1)}, bf16[128,2048]{1,0:T(8,128)(2,1)}, u32[]{:S(2)}) copy-start(bf16[128,2048]{1,0:T(8,128)(2,1)} %param.21) | copy-start | bytes 1572868
  110.5 22.9 %copy-start.1 = (bf16[4,16,16,512]{3,2,1,0:T(8,128)(2,1)}, bf16[4,16,16,512]{3,2,1,0:T(8,128)(2,1)S(1)}, u32[]{:S(2)}) copy-start(bf16[4,16,16,512]{3,2,1,0:T(8,128)(2,1)S(1)} %all_to_all.46.own) | copy-start | bytes 3145732
  112.2 38.2 %copy-start.8 = (bf16[2048,4]{0,1:T(4,128)(2,1)S(1)}, bf16[2048,4]{0,1:T(4,128)(2,1)}, u32[]{:S(2)}) copy-start(bf16[2048,4]{0,1:T(4,128)(2,1)} %param.30) | copy-start | bytes 49156
  112.2 23.6 %all-to-all-start = ((bf16[4,128,2048]{2,1,0:T(8,128)(2,1)}), bf16[4,128,2048]{2,1,0:T(8,128)(2,1)}, u32[]{:S(2)}, u32[]{:S(2)}) async-start(bf16[4,128,2048]{2,1,0:T(8,128)(2,1)} %broadcast_in_dim.20), calls=%async_computation | async-start | bytes 4194304 | tf_op jit(solution)/shard_map/all_to_all | solution.py:286
  116.8 96.7 %collective-permute-start.2 = (bf16[4,16,16,1152]{3,2,1,0:T(8,128)(2,1)S(1)}, bf16[4,16,16,1152]{3,2,1,0:T(8,128)(2,1)}, u32[]{:S(2)}, u32[]{:S(2)}) collective-permute-start(bf16[4,16,16,1152]{3,2,1,0:T(8,128)(2,1)S(1)} %all_to_all.45.own), channel_id=1, source_target_pairs={{0,4},{4,0},{1,5},{5,1},{2,6},{6,2},{3,7},{7,3},{8,12},{12,8},{9,1... | collective-permute-start | bytes 7077896 | tf_op jit(solution)/shard_map/ppermute | solution.py:292
  131.5 34.4 %collective-permute-start.1 = (bf16[4,16,16,384]{3,2,1,0:T(8,128)(2,1)}, bf16[4,16,16,384]{3,2,1,0:T(8,128)(2,1)}, u32[]{:S(2)}, u32[]{:S(2)}) collective-permute-start(bf16[4,16,16,384]{3,2,1,0:T(8,128)(2,1)} %copy-done.2), channel_id=1, source_target_pairs={{0,4},{4,0},{1,5},{5,1},{2,6},{6,2},{3,7},{7,3},{8,12},{12,8},{9,1... | collective-permute-start | bytes 2359304 | tf_op jit(solution)/shard_map/ppermute | solution.py:292
  133.4 88.8 %collective-permute-start.3 = (bf16[4,16,16,512]{3,2,1,0:T(8,128)(2,1)S(1)}, bf16[4,16,16,512]{3,2,1,0:T(8,128)(2,1)}, u32[]{:S(2)}, u32[]{:S(2)}) collective-permute-start(bf16[4,16,16,512]{3,2,1,0:T(8,128)(2,1)S(1)} %all_to_all.46.own), channel_id=1, source_target_pairs={{0,4},{4,0},{1,5},{5,1},{2,6},{6,2},{3,7},{7,3},{8,12},{12,8},{9,1... | collective-permute-start | bytes 3145736 | tf_op jit(solution)/shard_map/ppermute | solution.py:292
  136.7 22.5 %collective-permute-start = (bf16[16,2048]{1,0:T(8,128)(2,1)S(1)}, bf16[16,2048]{1,0:T(8,128)(2,1)S(1)}, u32[]{:S(2)}, u32[]{:S(2)}) collective-permute-start(bf16[16,2048]{1,0:T(8,128)(2,1)S(1)} %slice_bitcast_fusion), channel_id=1, source_target_pairs={{0,4},{4,8},{8,12},{12,16},{16,20},{20,24},{24,28},{28,32},{32,36}... | collective-permute-start | bytes 196616 | tf_op jit(solution)/shard_map/ppermute | solution.py:346
  159.1 0.6 copy-start.7
  165.9 46.3 %copy-start.11 = (f32[4]{0:T(128)S(1)}, f32[4]{0:T(128)}, u32[]{:S(2)}) copy-start(f32[4]{0:T(128)} %param.38) | copy-start | bytes 52
  165.9 47.0 %copy-start.12 = (bf16[256]{0:T(256)(128)(2,1)S(1)}, bf16[256]{0:T(256)(128)(2,1)}, u32[]{:S(2)}) copy-start(bf16[256]{0:T(256)(128)(2,1)} %param.39) | copy-start | bytes 1540
  185.2 17.1 %all-to-all-start.3 = ((bf16[16,24,256]{2,1,0:T(8,128)(2,1)}), bf16[16,24,256]{2,1,0:T(8,128)(2,1)}, u32[]{:S(2)}, u32[]{:S(2)}) async-start(bf16[16,24,256]{2,1,0:T(8,128)(2,1)} %shard_map.201), calls=%async_computation.3 | async-start | bytes 393216 | tf_op jit(solution)/shard_map/all_to_all | solution.py:384
  203.9 18.3 %all-to-all-start.4 = ((bf16[8,16,256]{2,1,0:T(8,128)(2,1)}), bf16[8,16,256]{2,1,0:T(8,128)(2,1)S(1)}, u32[]{:S(2)}, u32[]{:S(2)}) async-start(bf16[8,16,256]{2,1,0:T(8,128)(2,1)} %shard_map.202), calls=%async_computation.4 | async-start | bytes 131072 | tf_op jit(solution)/shard_map/all_to_all | solution.py:388
  222.2 0.6 copy-start.6

commit v2 on v1

v2 whole, which is shorter than its diff:
```python
import jax
import jax.numpy as jnp
from jax import lax
from jax.experimental import pallas as pl
from jax.experimental.pallas import tpu as pltpu
from jax.sharding import Mesh
from jax.sharding import PartitionSpec as P

SP = ("z", "x", "c")
SP_TP = ("z", "x", "c", "tp")
EPS = 1e-05
ROWS = 512
HALO = 16
BLK = 128
NB = ROWS // BLK
F32 = jnp.float32
BF16 = jnp.bfloat16


def call(body, outs, args, specs=None, scratch=()):
    vmem = pl.BlockSpec(memory_space=pltpu.VMEM)
    specs = specs or {}
    return pl.pallas_call(
        body,
        out_shape=outs,
        in_specs=[specs.get(i, vmem) for i in range(len(args))],
        out_specs=jax.tree.map(lambda _: vmem, outs),
        scratch_shapes=list(scratch),
    )(*args)


HBM = pl.BlockSpec(memory_space=pltpu.HBM)
SMEM = pl.BlockSpec(memory_space=pltpu.SMEM)


def shape(dims, kind):
    return jax.ShapeDtypeStruct(dims, kind)


def dot(a, b):
    return jnp.dot(a, b, preferred_element_type=F32)


def dot_nt(a, b):
    return lax.dot_general(a, b, (((1,), (1,)), ((), ())), preferred_element_type=F32)


def per_head(v):
    rows = v.shape[0]
    low = lax.broadcasted_iota(jnp.int32, (rows, 128), 1) < 64
    pairs = [
        jnp.where(
            low,
            jnp.broadcast_to(v[:, 2 * p : 2 * p + 1], (rows, 128)),
            jnp.broadcast_to(v[:, 2 * p + 1 : 2 * p + 2], (rows, 128)),
        )
        for p in range(2)
    ]
    return jnp.concatenate(pairs, axis=1)


def silu(v):
    return v / (1.0 + jnp.exp(-v))


def run(copies, wait):
    for copy in copies:
        if wait:
            copy.wait()
        else:
            copy.start()


def first_copies(c, own, other, whole, sems):
    return [
        pltpu.make_async_copy(
            src.at[x], whole.at[:, x, c if side == 0 else 1 - c], sems.at[2 * x + side]
        )
        for x in range(4)
        for side, src in ((0, own), (1, other))
    ]


def ring_copies(x, c, parts, whole, sems, lo, count):
    out = []
    for side in range(2):
        at = c if side == 0 else 1 - c
        for i, (by, z, zs) in enumerate(
            ((0, 0, 16), (3, 0, 16), (1, 0, 16), (2, 0, 8), (2, 8, 8))
        ):
            out.append(
                pltpu.make_async_copy(
                    parts[5 * side + i].at[:, lo : lo + count, :],
                    whole.at[z : z + zs, (x + by) % 4, at],
                    sems.at[5 * side + i],
                )
            )
    return out


def block(whole, q):
    return whole[:, :, :, 16 * q : 16 * (q + 1), :].reshape(2048, 128)


def blocks(whole, lo, count):
    return jnp.concatenate([block(whole, q) for q in range(lo, lo + count)], axis=1)


def taps(ref, weights, cols, count):
    w = weights[...].astype(F32)
    out = None
    for k in range(count):
        part = w[k : k + 1, :] * ref[pl.ds(HALO - count + 1 + k, ROWS), cols]
        out = part if out is None else out + part
    return out


def prep_body(tok, gain, w0, w1, w2, w3, w4, w5, w6, w7, w8, copied, own, left):
    q = 0
    for w in (w0, w1, w2, w3, w4, w5, w6, w7, w8):
        for k in range(w.shape[1] // 128):
            v = w[:, 128 * k : 128 * (k + 1)]
            if q < 15:
                own[16 * q : 16 * (q + 1), :] = v
            else:
                own[240:254, :] = v[0:14]
                f = v.astype(F32)
                left[...] = jnp.concatenate([f[14:15], f[15:16]], axis=1)
            q += 1
    g = gain[...].astype(F32)

    def some(i, _):
        rows = pl.ds(pl.multiple_of(i * 16, 16), 16)
        f = tok[rows, :].astype(F32)
        scaled = f * lax.rsqrt(jnp.mean(f * f, axis=1, keepdims=True) + EPS)
        v = (scaled * g).astype(BF16)
        for y in range(4):
            copied[y, rows, :] = v
        return 0

    lax.fori_loop(0, 8, some, 0, unroll=2)


def cum_body(tok, ws, params, spikes, dt, cum, cum_t):
    n = tok[...].reshape(ROWS, 2048)
    raw = dot_nt(ws[...], n)[0:8] + params[0:8, 0:1]
    step = jnp.maximum(raw, 0.0) + jnp.log1p(jnp.exp(-jnp.abs(raw)))
    logs = -step * jnp.exp(params[0:8, 1:2]) + spikes[...]
    r = lax.broadcasted_iota(jnp.int32, (BLK, BLK), 0)
    s = lax.broadcasted_iota(jnp.int32, (BLK, BLK), 1)
    upper = jnp.where(r <= s, 1.0, 0.0).astype(F32)
    carry = jnp.zeros((8, 1), F32)
    fill = jnp.zeros((BLK - 8, BLK), F32)
    for b in range(NB):
        rows = slice(b * BLK, (b + 1) * BLK)
        part = (
            jnp.dot(
                logs[:, rows],
                upper,
                precision=lax.Precision.HIGHEST,
                preferred_element_type=F32,
            )
            + carry
        )
        cum_t[:, rows] = part
        cum[rows, :] = jnp.concatenate([part, fill], axis=0).T
        dt[rows, :] = jnp.concatenate([step[:, rows], fill], axis=0).T
        carry = part[:, BLK - 1 : BLK]


def first_body(
    pos, tok, halo, own, other, dt, cum, input_taps, write_taps,
    weighted, seq_input, seq_write, local, pieces,
    whole, normed, fields, sems,
):
    moves = first_copies(pos[2], own, other, whole, sems)
    run(moves, False)
    normed[0:HALO, :] = halo[...]
    normed[HALO:, :] = tok[...].reshape(ROWS, 2048)
    run(moves, True)
    projected = dot(normed[...], blocks(whole, 0, 3))
    fields[...] = projected.astype(BF16).astype(F32)
    xin = silu(taps(fields, input_taps, slice(0, 256), 4))
    write = silu(taps(fields, write_taps, slice(256, 384), 4))
    seq_input[...] = xin
    seq_write[...] = write.astype(BF16)
    scaled = xin * per_head(dt[:, 0:128])
    weighted[...] = scaled.astype(BF16)
    state = jnp.zeros((128, 256), F32)
    before = jnp.zeros((1, 128), F32)
    for b in range(NB):
        rows = slice(b * BLK, (b + 1) * BLK)
        end = cum[(b + 1) * BLK - 1 : (b + 1) * BLK, :]
        local[b] = state.astype(BF16)
        to_end = per_head(jnp.exp(end - cum[rows, :]))
        added = dot(write[rows].T.astype(BF16), (scaled[rows] * to_end).astype(BF16))
        state = state * per_head(jnp.exp(end - before)) + added
        before = end
    decay = per_head(jnp.exp(before))
    high = decay.astype(BF16).astype(F32)
    low = decay - high
    tail = jnp.where(
        lax.broadcasted_iota(jnp.int32, (8, 256), 0) < 4,
        jnp.broadcast_to(high, (8, 256)),
        jnp.broadcast_to(low, (8, 256)),
    ).astype(BF16)
    for j in range(8):
        pieces[j, 0:16, :] = state[16 * j : 16 * (j + 1)].astype(BF16)
        pieces[j, 16:24, :] = tail


def piece_of(ref, j):
    v = ref[j].astype(F32)
    return v[0:16], v[16:17] + v[20:21]


def plane_body(got, left, send):
    state = jnp.zeros((16, 256), F32)
    decay = jnp.ones((1, 256), F32)
    for j in range(8):
        s, d = piece_of(got, j)
        state = state * d + s
        decay = decay * d
    high = decay.astype(BF16).astype(F32)
    tail = jnp.where(
        lax.broadcasted_iota(jnp.int32, (8, 256), 0) < 4,
        jnp.broadcast_to(high, (8, 256)),
        jnp.broadcast_to(decay - high, (8, 256)),
    )
    second = lax.broadcasted_iota(jnp.int32, (8, 256), 0) == 1
    tail = jnp.where(second, jnp.broadcast_to(left[...], (8, 256)), tail)
    one = jnp.concatenate([state, tail], axis=0).astype(BF16)
    for k in range(16):
        send[k] = one


def enter_body(pos, got, planes, out):
    z = pos[0]
    state = jnp.zeros((16, 256), F32)
    lefts = []
    for k in range(16):
        lefts.append(planes[k].astype(F32)[17:18])
        s, d = piece_of(planes, k)
        state = jnp.where(k < z, state * d + s, state)
    left = jnp.concatenate(lefts, axis=0).astype(BF16)
    for j in range(8):
        out[j, 0:16, :] = state.astype(BF16)
        out[j, 16:32, :] = left
        s, d = piece_of(got, j)
        state = state * d + s


def rest_body(
    pos, tok, halo, p0, p1, p2, p3, p4, p5, p6, p7, p8, p9,
    weighted, seq_input, seq_write, local, cum, cum_t,
    read_taps, gated_taps, direct,
    partly, read_out, gate, mixer,
    whole, normed, fields, sems,
):
    parts = (p0, p1, p2, p3, p4, p5, p6, p7, p8, p9)
    moves = ring_copies(pos[1], pos[2], parts, whole, sems, 0, 144)
    run(moves, False)
    normed[0:HALO, :] = halo[...]
    normed[HALO:, :] = tok[...].reshape(ROWS, 2048)
    run(moves, True)
    n = normed[...]

    def projected(lo, count):
        return dot(n, blocks(whole, lo, count)).astype(BF16).astype(F32)

    fields[:, 0:128] = projected(0, 1)
    read = silu(taps(fields, read_taps, slice(0, 128), 4)).astype(BF16)
    read_out[...] = read
    gate[...] = silu(projected(1, 2)[HALO:])
    inner = projected(5, 2)
    fields[...] = inner * projected(7, 2)
    outer = projected(3, 2)[HALO:]
    mixer[...] = (outer * taps(fields, gated_taps, slice(0, 256), 3)).astype(BF16)
    r = lax.broadcasted_iota(jnp.int32, (BLK, BLK), 0)
    s = lax.broadcasted_iota(jnp.int32, (BLK, BLK), 1)
    causal = r >= s
    low = s < 64
    before = jnp.zeros((1, 128), F32)
    for b in range(NB):
        rows = slice(b * BLK, (b + 1) * BLK)
        rb = read[rows]
        scores = dot_nt(rb, seq_write[rows, :])
        here = cum[rows, :]
        from_local = dot(rb, local[b]) * per_head(jnp.exp(here - before))
        before = here[BLK - 1 : BLK, :]
        halves = []
        for p in range(2):
            pair = weighted[rows, 128 * p : 128 * (p + 1)]
            two = []
            for h in (2 * p, 2 * p + 1):
                gap = here[:, h : h + 1] - cum_t[h : h + 1, rows]
                damped = scores * jnp.exp(jnp.where(causal, gap, -jnp.inf))
                two.append(dot(damped.astype(BF16), pair))
            halves.append(jnp.where(low, two[0], two[1]))
        within = jnp.concatenate(halves, axis=1)
        partly[rows, :] = within + from_local + direct[...] * seq_input[rows, :]


def tail_body(
    pos, arriving, partly, read, gate, cum, mixer, scale,
    p0, p1, p2, p3, p4, p5, p6, p7, p8, p9,
    out,
    whole, act, sems,
):
    parts = (p0, p1, p2, p3, p4, p5, p6, p7, p8, p9)
    moves = ring_copies(pos[1], pos[2], parts, whole, sems, 144, 64)
    run(moves, False)
    act[:, 0:256] = mixer[...]
    state = jnp.concatenate([arriving[j, 0:16, :] for j in range(8)], axis=0)
    head = partly[...] + dot(read[...], state) * per_head(jnp.exp(cum[...]))
    gated = head * gate[...]
    square = gated * gated
    r = lax.broadcasted_iota(jnp.int32, (256, 256), 0) // 64
    s = lax.broadcasted_iota(jnp.int32, (256, 256), 1) // 64
    same = jnp.where(r == s, 1.0 / 64.0, 0.0).astype(BF16)
    high = square.astype(BF16)
    rest = (square - high.astype(F32)).astype(BF16)
    mean = dot(high, same) + dot(rest, same)
    act[:, 256:512] = (gated * lax.rsqrt(mean + EPS) * scale[...].astype(F32)).astype(BF16)
    run(moves, True)
    row = lax.broadcasted_iota(jnp.int32, (16, 128), 0)
    for j in range(8):
        lefts = arriving[j, 16:32, :].astype(F32)
        for z in range(16):
            tile = whole[z, j // 2, j % 2, 48:64, :].astype(F32)
            for i in range(2):
                v = lefts[z : z + 1, 128 * i : 128 * (i + 1)]
                tile = jnp.where(row == 14 + i, jnp.broadcast_to(v, (16, 128)), tile)
            whole[z, j // 2, j % 2, 48:64, :] = tile.astype(BF16)
    a = act[...]
    for q in range(4):
        cols = slice(512 * q, 512 * (q + 1))
        some = whole.at[4 * q : 4 * (q + 1)]
        w = jnp.concatenate(
            [some[:, :, :, 16 * k : 16 * (k + 1), :].reshape(512, 128) for k in range(4)],
            axis=1,
        )
        out[:, cols] = dot_nt(a, w).astype(BF16)


def sum_body(got, out):
    v = got[0].astype(F32)
    for y in range(1, 4):
        v = v + got[y].astype(F32)
    out[...] = v.astype(BF16)


def exchanged(tiles, axis):
    return lax.all_to_all(tiles, axis, 0, 0, tiled=True)


def copies(shard, axis):
    n = lax.axis_size(axis)
    return exchanged(jnp.broadcast_to(shard[None], (n, *shard.shape)), axis)


def passed(shard, by):
    return lax.ppermute(shard, "x", [(i, (i + by) % 4) for i in range(4)])


def swapped(shard):
    return lax.ppermute(shard, "c", [(0, 1), (1, 0)])


def per_device(
    tokens,
    input_norm_scale,
    outer_gate_weight,
    inner_gate_weight,
    value_weight_matrix,
    output_gate_weight,
    state_input_weight,
    write_key_weight,
    read_key_weight,
    step_size_weight,
    gated_conv_weight,
    input_conv_weight,
    write_conv_weight,
    read_conv_weight,
    step_size_bias,
    log_decay_rate,
    decay_spikes,
    direct_path_weight,
    head_norm_scale,
    conv_output_weight,
    state_output_weight,
):
    pos = jnp.stack([lax.axis_index(a).astype(jnp.int32) for a in SP])
    copied, own, left = call(
        prep_body,
        (shape((4, 128, 2048), BF16), shape((254, 128), BF16), shape((1, 256), F32)),
        (
            tokens,
            input_norm_scale[None],
            state_input_weight,
            write_key_weight,
            read_key_weight,
            output_gate_weight,
            outer_gate_weight,
            inner_gate_weight,
            value_weight_matrix,
            conv_output_weight.T,
            state_output_weight.T,
        ),
    )
    tok = exchanged(copied, "tp")
    column = lax.all_gather(own, "z", axis=0, tiled=False)
    first = copies(column[:, :48], "x")
    first_other = swapped(first)
    ring = [jnp.pad(column[:, 48:], ((0, 0), (0, 2), (0, 0)))]
    ring.append(passed(ring[0], 1))
    ring.append(passed(ring[0], 3))
    ring.append(passed(ring[1][:8], 1))
    ring.append(passed(ring[2][8:], 3))
    ring += [swapped(part) for part in ring]
    halo = lax.ppermute(tok[3, 112:, :], SP, [(i, i + 1) for i in range(127)])

    dt, cum, cum_t = call(
        cum_body,
        (shape((ROWS, 128), F32), shape((ROWS, 128), F32), shape((8, ROWS), F32)),
        (
            tok,
            jnp.pad(step_size_weight.T, ((0, 12), (0, 0))),
            jnp.pad(jnp.stack([step_size_bias, log_decay_rate], 1), ((0, 4), (0, 126))),
            jnp.pad(decay_spikes, ((0, 4), (0, 0))),
        ),
    )
    weighted, seq_input, seq_write, local, pieces = call(
        first_body,
        (
            shape((ROWS, 256), BF16),
            shape((ROWS, 256), F32),
            shape((ROWS, 128), BF16),
            shape((NB, 128, 256), BF16),
            shape((8, 24, 256), BF16),
        ),
        (pos, tok, halo, first, first_other, dt, cum, input_conv_weight, write_conv_weight),
        {0: SMEM, 3: HBM, 4: HBM},
        (
            pltpu.VMEM((16, 4, 2, 48, 128), BF16),
            pltpu.VMEM((HALO + ROWS, 2048), BF16),
            pltpu.VMEM((HALO + ROWS, 384), F32),
            pltpu.SemaphoreType.DMA((8,)),
        ),
    )
    got = exchanged(pieces, ("x", "c"))
    send = call(plane_body, shape((16, 24, 256), BF16), (got, left))
    planes = exchanged(send, "z")
    entering = call(
        enter_body, shape((8, 32, 256), BF16), (pos, got, planes), {0: SMEM}
    )
    arriving = exchanged(entering, ("x", "c"))

    direct = jnp.repeat(direct_path_weight, 64)[None]
    partly, read, gate, mixer = call(
        rest_body,
        (
            shape((ROWS, 256), F32),
            shape((ROWS, 128), BF16),
            shape((ROWS, 256), F32),
            shape((ROWS, 256), BF16),
        ),
        (
            pos, tok, halo, *ring, weighted, seq_input, seq_write, local, cum, cum_t,
            read_conv_weight, gated_conv_weight, direct,
        ),
        {0: SMEM, **{i: HBM for i in range(3, 13)}},
        (
            pltpu.VMEM((16, 4, 2, 144, 128), BF16),
            pltpu.VMEM((HALO + ROWS, 2048), BF16),
            pltpu.VMEM((HALO + ROWS, 256), F32),
            pltpu.SemaphoreType.DMA((10,)),
        ),
    )
    partial = call(
        tail_body,
        shape((ROWS, 2048), BF16),
        (pos, arriving, partly, read, gate, cum, mixer, head_norm_scale[None], *ring),
        {0: SMEM, **{i: HBM for i in range(8, 18)}},
        (
            pltpu.VMEM((16, 4, 2, 64, 128), BF16),
            pltpu.VMEM((ROWS, 512), BF16),
            pltpu.SemaphoreType.DMA((10,)),
        ),
    )
    parts = exchanged(partial.reshape(4, 128, 2048), "tp")
    return call(sum_body, shape((128, 2048), BF16), (parts,))


def solution(mesh):
    torus = Mesh(mesh.devices.reshape(16, 4, 2, mesh.shape["tp"]), SP_TP)
    rows = P(SP, "tp")
    cols = P("tp", SP)
    taps_ = P(None, "tp")
    heads = P("tp")
    return jax.shard_map(
        per_device,
        mesh=torus,
        in_specs=(
            P(SP_TP, None), P(), rows, rows, rows, rows, rows, rows, rows,
            taps_, taps_, taps_, taps_, taps_, heads, heads, cols, heads, heads, cols, cols,
        ),
        out_specs=P(SP_TP, None),
        check_vma=False,
    )
```

time: 263 us -> 206 us (0.78)
  blocking collectives: 113 us -> 79.1 us
  waiting for transfers between devices: 33.4 us -> 10.4 us
  local copies, waits for them, and re-layouts: 22.8 us -> 11.6 us
  starting transfers between devices: 59.3 us -> 68.9 us
    all_to_all x4 -> x2, blocking collectives: 79.3 us -> 43.1 us  [exchanged(): return lax.all_to_all(tiles, axis, 0, 0, tiled=True)]
    all_to_all x5 -> x4, waiting for transfers between devices: 33.4 us -> 8.08 us  [exchanged(): return lax.all_to_all(tiles, axis, 0, 0, tiled=True)]
    ppermute x1 -> x5, starting transfers between devices: 12.4 us -> 22.8 us  [the longest x4 12 us: passed(): return lax.ppermute(shard, 'x', [(i, (i + by) % 4) for i in range(4)])]
    unnamed x34 -> x30, local copies, waits for them, and re-layouts: 8.81 us -> 3.73 us
    pad x4 -> x3, local copies, waits for them, and re-layouts: 6.13 us -> 1.31 us  [the longest x1 0.64 us: per_device(): jnp.pad(step_size_weight.T, ((0, 12), (0, 0)))]
    slice x2 -> x4, local copies, waits for them, and re-layouts: 0.07 us -> 3.7 us  [the longest x1 1.82 us: per_device(): ring.append(passed(ring[2][8:], 3))]
    broadcast_in_dim x5 -> x1, local copies, waits for them, and re-layouts: 3.72 us -> 0.1 us  [copies(): return exchanged(jnp.broadcast_to(shard[None], (n, *shard.shape)), axis)]
    all_to_all x5 -> x4, starting transfers between devices: 27.8 us -> 24.4 us  [exchanged(): return lax.all_to_all(tiles, axis, 0, 0, tiled=True)]
  transfers between devices with their start and end apart: 9 -> 15, of which waited for: 3 -> 2; matrix products, arithmetic and copies ran while one was open for 5% -> 4% of each run, Pallas kernels for 9% -> 11%
where the time goes in v2:
time: 206 us; the launch traced here: 205 us
  blocking collectives  79.1 us (38%)
  starting transfers between devices  68.9 us (33%)
  Pallas kernels  33.5 us (16%)
  local copies, waits for them, and re-layouts  11.6 us (6%)
  waiting for transfers between devices  10.4 us (5%)
    all_to_all x2, blocking collectives, exchanged(): return lax.all_to_all(tiles, axis, 0, 0, tiled=True)  43.1 us
    all_gather x1, blocking collectives, per_device(): column = lax.all_gather(own, 'z', axis=0, tiled=False)  36 us
    pallas_call x8, Pallas kernels, call(): pl.pallas_call(body, out_shape=outs, in_specs=[specs.get(i, vmem) for i i...  33.5 us
    all_to_all x4, starting transfers between devices, exchanged(): return lax.all_to_all(tiles, axis, 0, 0, tiled=True)  24.4 us
    ppermute x6, starting transfers between devices, swapped(): return lax.ppermute(shard, 'c', [(0, 1), (1, 0)])  21.7 us
    ppermute x4, starting transfers between devices, passed(): return lax.ppermute(shard, 'x', [(i, (i + by) % 4) for i in range(4)])  12 us
    ppermute x1, starting transfers between devices, per_device(): halo = lax.ppermute(tok[3, 112:, :], SP, [(i, i + 1) for i in range(127)])  10.8 us
    all_to_all x4, waiting for transfers between devices, exchanged(): return lax.all_to_all(tiles, axis, 0, 0, tiled=True)  8.08 us
  transfers between devices with their start and end apart: 15, of which 2 were waited for; matrix products, arithmetic and copies ran while one was open for 4% of the time, Pallas kernels for 11%

profile of v2, /device:TPU:1, one launch (start us, length us, event | category | flops | bytes accessed | tf_op | source)
XLA Modules:
  0.0 205.2 jit_solution(12313300812091520998)
XLA Ops:
  0.0 1.3 broadcast_in_dim.15.gain
  1.3 3.1 %shard_map.199 = (bf16[4,128,2048]{2,1,0:T(8,128)(2,1)}, bf16[254,128]{1,0:T(8,128)(2,1)}, f32[1,256]{1,0:T(1,128)}) custom-call(bf16[128,2048]{1,0:T(8,128)(2,1)} %tok.1, bf16[1,2048]{1,0:T(2,128)(2,1)} %broadcast_in_dim.15.gain, bf16[16,256]{1,0:T(8,128)(2,1)} %w0.1, bf16[16,128]{1,0:T(8,128)(2,1)} %w1.1, bf16[16,128]{1,0:T(8,128)(2,1)} %w2.1, ...), custom_call_target="tpu_custom_call" | custom-call | tf_op jit(solution)/shard_map/pallas_call | solution.py:23
  4.4 36.0 %all-gather.1 = bf16[16,254,128]{2,1,0:T(8,128)(2,1)S(1)} all-gather(bf16[1,254,128]{2,1,0:T(8,128)(2,1)} %bitcast.13), channel_id=2, replica_groups=mesh['z'=16,'x'=4,'c'=2,'tp'=4] {'z'}, dimensions={0}, use_global_device_ids=true | all-gather | bytes 1105408 | tf_op jit(solution)/shard_map/all_gather | solution.py:412
  40.4 0.1 broadcast_in_dim.16
  40.5 12.3 %all_to_all.30.own = bf16[4,16,48,128]{3,2,1,0:T(8,128)(2,1)} all-to-all(bf16[4,16,48,128]{3,2,1,0:T(8,128)(2,1)S(1)} %broadcast_in_dim.16), channel_id=1, replica_groups=mesh['z'=16,'x'=4,'c'=2,'tp'=4] {'x'}, dimensions={0} | all-to-all | bytes 1572864 | tf_op jit(solution)/shard_map/all_to_all | solution.py:354
  52.8 4.2 %all-to-all-start = ((bf16[4,128,2048]{2,1,0:T(8,128)(2,1)}), bf16[4,128,2048]{2,1,0:T(8,128)(2,1)S(1)}, u32[]{:S(2)}, u32[]{:S(2)}) async-start(bf16[4,128,2048]{2,1,0:T(8,128)(2,1)} %get-tuple-element.20), calls=%async_computation | async-start | bytes 4194304 | tf_op jit(solution)/shard_map/all_to_all | solution.py:354
  57.0 0.0 copy-start.10
  57.0 11.0 %collective-permute-start.1 = (bf16[4,16,48,128]{3,2,1,0:T(8,128)(2,1)}, bf16[4,16,48,128]{3,2,1,0:T(8,128)(2,1)}, u32[]{:S(2)}, u32[]{:S(2)}) collective-permute-start(bf16[4,16,48,128]{3,2,1,0:T(8,128)(2,1)} %all_to_all.30.own), channel_id=1, source_target_pairs={{0,4},{4,0},{1,5},{5,1},{2,6},{6,2},{3,7},{7,3},{8,12},{12,8},{9,1... | collective-permute-start | bytes 2359304 | tf_op jit(solution)/shard_map/ppermute | solution.py:367
  68.0 0.1 slice.22
  68.1 0.1 pad.19.p0
  68.2 2.8 %collective-permute-start.3 = (bf16[16,208,128]{2,1,0:T(8,128)(2,1)S(1)}, bf16[16,208,128]{2,1,0:T(8,128)(2,1)}, u32[]{:S(2)}, u32[]{:S(2)}) collective-permute-start(bf16[16,208,128]{2,1,0:T(8,128)(2,1)S(1)} %pad.19.p0), channel_id=1, source_target_pairs={{0,24},{8,0},{16,8},{24,16},{1,25},{9,1},{17,9},{25,17},{2,26},{10... | collective-permute-start | bytes 2555912 | tf_op jit(solution)/shard_map/ppermute | solution.py:363
  71.0 2.5 %collective-permute-start.2 = (bf16[16,208,128]{2,1,0:T(8,128)(2,1)S(1)}, bf16[16,208,128]{2,1,0:T(8,128)(2,1)}, u32[]{:S(2)}, u32[]{:S(2)}) collective-permute-start(bf16[16,208,128]{2,1,0:T(8,128)(2,1)S(1)} %pad.19.p0), channel_id=1, source_target_pairs={{0,8},{8,16},{16,24},{24,0},{1,9},{9,17},{17,25},{25,1},{2,10},{10... | collective-permute-start | bytes 2555912 | tf_op jit(solution)/shard_map/ppermute | solution.py:363
  73.5 0.6 pad.16.ws
  74.1 0.1 copy.24
  74.2 0.1 copy.25
  74.3 0.6 pad.18.spikes
  74.9 0.7 select_maximum_fusion.params
  75.6 0.0 all-to-all-done.tok
  75.6 10.8 %collective-permute-start = (bf16[16,2048]{1,0:T(8,128)(2,1)S(1)}, bf16[16,2048]{1,0:T(8,128)(2,1)S(1)}, u32[]{:S(2)}, u32[]{:S(2)}) collective-permute-start(bf16[16,2048]{1,0:T(8,128)(2,1)S(1)} %slice_bitcast_fusion), channel_id=1, source_target_pairs={{0,4},{4,8},{8,12},{12,16},{16,20},{20,24},{24,28},{28,32},{32,36}... | collective-permute-start | bytes 196616 | tf_op jit(solution)/shard_map/ppermute | solution.py:421
  86.4 0.6 pad_add_fusion.pos
  87.0 3.5 %shard_map.200 = (f32[512,128]{1,0:T(8,128)}, f32[512,128]{1,0:T(8,128)}, f32[8,512]{1,0:T(8,128)}) custom-call(bf16[4,128,2048]{2,1,0:T(8,128)(2,1)} %copy-done, bf16[16,2048]{1,0:T(8,128)(2,1)} %pad.16.ws, f32[8,128]{1,0:T(8,128)} %select_maximum_fusion.params, f32[8,512]{1,0:T(8,128)} %pad.18.spikes), custom_call_target="tpu_custom_call" | custom-call | tf_op jit(solution)/shard_map/pallas_call | solution.py:23
  90.5 0.0 collective-permute-done.1.other
  90.5 2.3 %collective-permute-done.halo = bf16[16,2048]{1,0:T(8,128)(2,1)S(1)} collective-permute-done((bf16[16,2048]{1,0:T(8,128)(2,1)S(1)}, bf16[16,2048]{1,0:T(8,128)(2,1)S(1)}, u32[]{:S(2)}, u32[]{:S(2)}) %collective-permute-start) | collective-permute-done | bytes 65568 | tf_op jit(solution)/shard_map/ppermute | solution.py:421
  92.9 0.6 copy-done.8
  93.5 6.4 %shard_map.201 = (bf16[512,256]{1,0:T(8,128)(2,1)}, f32[512,256]{1,0:T(8,128)}, bf16[512,128]{1,0:T(8,128)(2,1)}, bf16[4,128,256]{2,1,0:T(8,128)(2,1)}, bf16[8,24,256]{2,1,0:T(8,128)(2,1)}) custom-call(s32[3]{0:T(128)} %pad_add_fusion.pos, bf16[4,128,2048]{2,1,0:T(8,128)(2,1)} %copy-done, bf16[16,2048]{1,0:T(8,128)(2,1)} %copy-done.8, ...), custom_call_target="tpu_custom_call" | custom-call | tf_op jit(solution)/shard_map/pallas_call | solution.py:23
  99.9 0.0 copy-start.13
  99.9 0.0 copy-start.14
  99.9 4.8 %all-to-all-start.2 = ((bf16[8,24,256]{2,1,0:T(8,128)(2,1)}), bf16[8,24,256]{2,1,0:T(8,128)(2,1)S(1)}, u32[]{:S(2)}, u32[]{:S(2)}) async-start(bf16[8,24,256]{2,1,0:T(8,128)(2,1)} %get-tuple-element.24), calls=%async_computation.2 | async-start | bytes 196608 | tf_op jit(solution)/shard_map/all_to_all | solution.py:354
  104.7 1.9 collective-permute-start.6
  106.6 0.0 collective-permute-done.3.p2
  106.6 1.8 slice.24
  108.4 4.8 %collective-permute-start.5 = (bf16[8,208,128]{2,1,0:T(8,128)(2,1)}, bf16[8,208,128]{2,1,0:T(8,128)(2,1)S(1)}, u32[]{:S(2)}, u32[]{:S(2)}) collective-permute-start(bf16[8,208,128]{2,1,0:T(8,128)(2,1)} %slice.24), channel_id=1, source_target_pairs={{0,24},{8,0},{16,8},{24,16},{1,25},{9,1},{17,9},{25,17},{2,26},{10... | collective-permute-start | bytes 1277960 | tf_op jit(solution)/shard_map/ppermute | solution.py:363
  113.3 0.0 collective-permute-done.2.p1
  113.3 1.8 slice.23
  115.1 1.9 collective-permute-start.4
  117.0 2.3 %collective-permute-start.7 = (bf16[16,208,128]{2,1,0:T(8,128)(2,1)}, bf16[16,208,128]{2,1,0:T(8,128)(2,1)S(1)}, u32[]{:S(2)}, u32[]{:S(2)}) collective-permute-start(bf16[16,208,128]{2,1,0:T(8,128)(2,1)} %collective-permute-done.2.p1), channel_id=1, source_target_pairs={{0,4},{4,0},{1,5},{5,1},{2,6},{6,2},{3,7},{7,3},{8,12},{12,8},{9,1... | collective-permute-start | bytes 2555912 | tf_op jit(solution)/shard_map/ppermute | solution.py:367
  119.3 2.0 collective-permute-start.8
  121.4 0.0 all-to-all-done.2.got
  121.4 0.6 copy-done.5
  122.0 1.6 shard_map.202
  123.6 6.4 %all-to-all-start.3 = ((bf16[16,24,256]{2,1,0:T(8,128)(2,1)}), bf16[16,24,256]{2,1,0:T(8,128)(2,1)S(1)}, u32[]{:S(2)}, u32[]{:S(2)}) async-start(bf16[16,24,256]{2,1,0:T(8,128)(2,1)} %shard_map.202), calls=%async_computation.3 | async-start | bytes 393216 | tf_op jit(solution)/shard_map/all_to_all | solution.py:354
  130.0 0.0 collective-permute-done.5.p4
  130.1 2.6 %collective-permute-start.10 = (bf16[8,208,128]{2,1,0:T(8,128)(2,1)S(1)}, bf16[8,208,128]{2,1,0:T(8,128)(2,1)}, u32[]{:S(2)}, u32[]{:S(2)}) collective-permute-start(bf16[8,208,128]{2,1,0:T(8,128)(2,1)S(1)} %collective-permute-done.5.p4), channel_id=1, source_target_pairs={{0,4},{4,0},{1,5},{5,1},{2,6},{6,2},{3,7},{7,3},{8,12},{12,8},{9,1... | collective-permute-start | bytes 1277960 | tf_op jit(solution)/shard_map/ppermute | solution.py:367
  132.7 0.0 collective-permute-done.4.p3
  132.7 1.9 collective-permute-start.9
  134.6 8.1 %all-to-all-done.3.planes = bf16[16,24,256]{2,1,0:T(8,128)(2,1)S(1)} async-done(((bf16[16,24,256]{2,1,0:T(8,128)(2,1)}), bf16[16,24,256]{2,1,0:T(8,128)(2,1)S(1)}, u32[]{:S(2)}, u32[]{:S(2)}) %all-to-all-start.3) | async-done | bytes 196640 | tf_op jit(solution)/shard_map/all_to_all | solution.py:354
  142.7 0.7 copy-done.6
  143.3 1.7 shard_map.203
  145.1 9.0 %all-to-all-start.4 = ((bf16[8,32,256]{2,1,0:T(8,128)(2,1)}), bf16[8,32,256]{2,1,0:T(8,128)(2,1)S(1)}, u32[]{:S(2)}, u32[]{:S(2)}) async-start(bf16[8,32,256]{2,1,0:T(8,128)(2,1)} %shard_map.203), calls=%async_computation.4 | async-start | bytes 262144 | tf_op jit(solution)/shard_map/all_to_all | solution.py:354
  154.0 0.1 broadcast_in_dim.17
  154.1 0.6 broadcast_in_dim_reshape.3.direct
  154.7 0.6 broadcast_in_dim.18.scale
  155.3 0.0 collective-permute-done.6.p5
  155.3 0.0 collective-permute-done.10.p9
  155.3 0.0 collective-permute-done.9.p8
  155.4 0.0 collective-permute-done.8.p7
  155.4 0.9 copy-done.2
  156.2 0.3 copy-done.3
  156.5 8.8 %shard_map.204 = (f32[512,256]{1,0:T(8,128)}, bf16[512,128]{1,0:T(8,128)(2,1)}, f32[512,256]{1,0:T(8,128)}, bf16[512,256]{1,0:T(8,128)(2,1)}) custom-call(s32[3]{0:T(128)} %pad_add_fusion.pos, bf16[4,128,2048]{2,1,0:T(8,128)(2,1)} %copy-done, bf16[16,2048]{1,0:T(8,128)(2,1)} %copy-done.8, bf16[16,208,128]{2,1,0:T(8,128)(2,1)} %copy-done.1, ...), custom_call_target="tpu_custom_call" | custom-call | tf_op jit(solution)/shard_map/pallas_call | solution.py:23
  165.3 0.0 copy-start.7
  165.3 0.6 copy-done.7
  166.0 5.7 %shard_map.205 = bf16[512,2048]{1,0:T(8,128)(2,1)} custom-call(s32[3]{0:T(128)} %pad_add_fusion.pos, bf16[8,32,256]{2,1,0:T(8,128)(2,1)} %copy-done.7, f32[512,256]{1,0:T(8,128)} %get-tuple-element.31.partly, bf16[512,128]{1,0:T(8,128)(2,1)} %get-tuple-element.32.read, f32[512,256]{1,0:T(8,128)} %get-tuple-element.33.gate, ...), custom_call_target="tpu_custom_call" | custom-call | tf_op jit(solution)/shard_map/pallas_call | solution.py:23
  171.7 30.9 %all_to_all.31.got = bf16[4,128,2048]{2,1,0:T(8,128)(2,1)} all-to-all(bf16[4,128,2048]{2,1,0:T(8,128)(2,1)} %bitcast.12), channel_id=1, replica_groups=mesh['z'=16,'x'=4,'c'=2,'tp'=4] {'tp'}, dimensions={0} | all-to-all | bytes 4194304 | tf_op jit(solution)/shard_map/all_to_all | solution.py:354
  202.6 2.6 %shard_map.206 = bf16[128,2048]{1,0:T(8,128)(2,1)} custom-call(bf16[4,128,2048]{2,1,0:T(8,128)(2,1)} %all_to_all.31.got), custom_call_target="tpu_custom_call" | custom-call | tf_op jit(solution)/shard_map/pallas_call | solution.py:23
  (24 shorter events, 0.1 us)
Async XLA Ops:
  52.8 22.8 %all-to-all-start = ((bf16[4,128,2048]{2,1,0:T(8,128)(2,1)}), bf16[4,128,2048]{2,1,0:T(8,128)(2,1)S(1)}, u32[]{:S(2)}, u32[]{:S(2)}) async-start(bf16[4,128,2048]{2,1,0:T(8,128)(2,1)} %get-tuple-element.20), calls=%async_computation | async-start | bytes 4194304 | tf_op jit(solution)/shard_map/all_to_all | solution.py:354
  57.0 16.5 %copy-start.9 = (bf16[2048,4]{0,1:T(4,128)(2,1)S(1)}, bf16[2048,4]{0,1:T(4,128)(2,1)}, u32[]{:S(2)}) copy-start(bf16[2048,4]{0,1:T(4,128)(2,1)} %param.30) | copy-start | bytes 49156
  57.0 17.1 %copy-start.11 = (f32[4]{0:T(128)S(1)}, f32[4]{0:T(128)}, u32[]{:S(2)}) copy-start(f32[4]{0:T(128)} %param.35) | copy-start | bytes 52
  57.0 17.2 %copy-start.12 = (f32[4]{0:T(128)S(1)}, f32[4]{0:T(128)}, u32[]{:S(2)}) copy-start(f32[4]{0:T(128)} %param.36) | copy-start | bytes 52
  57.0 17.3 %copy-start.10 = (f32[4,512]{1,0:T(4,128)S(1)}, f32[4,512]{1,0:T(4,128)}, u32[]{:S(2)}) copy-start(f32[4,512]{1,0:T(4,128)} %param.37) | copy-start | bytes 24580
  57.0 33.5 %collective-permute-start.1 = (bf16[4,16,48,128]{3,2,1,0:T(8,128)(2,1)}, bf16[4,16,48,128]{3,2,1,0:T(8,128)(2,1)}, u32[]{:S(2)}, u32[]{:S(2)}) collective-permute-start(bf16[4,16,48,128]{3,2,1,0:T(8,128)(2,1)} %all_to_all.30.own), channel_id=1, source_target_pairs={{0,4},{4,0},{1,5},{5,1},{2,6},{6,2},{3,7},{7,3},{8,12},{12,8},{9,1... | collective-permute-start | bytes 2359304 | tf_op jit(solution)/shard_map/ppermute | solution.py:367
  68.1 87.2 %copy-start.1 = (bf16[16,208,128]{2,1,0:T(8,128)(2,1)}, bf16[16,208,128]{2,1,0:T(8,128)(2,1)S(1)}, u32[]{:S(2)}) copy-start(bf16[16,208,128]{2,1,0:T(8,128)(2,1)S(1)} %pad.19.p0) | copy-start | bytes 2555908
  68.2 38.4 %collective-permute-start.3 = (bf16[16,208,128]{2,1,0:T(8,128)(2,1)S(1)}, bf16[16,208,128]{2,1,0:T(8,128)(2,1)}, u32[]{:S(2)}, u32[]{:S(2)}) collective-permute-start(bf16[16,208,128]{2,1,0:T(8,128)(2,1)S(1)} %pad.19.p0), channel_id=1, source_target_pairs={{0,24},{8,0},{16,8},{24,16},{1,25},{9,1},{17,9},{25,17},{2,26},{10... | collective-permute-start | bytes 2555912 | tf_op jit(solution)/shard_map/ppermute | solution.py:363
  71.0 42.3 %collective-permute-start.2 = (bf16[16,208,128]{2,1,0:T(8,128)(2,1)S(1)}, bf16[16,208,128]{2,1,0:T(8,128)(2,1)}, u32[]{:S(2)}, u32[]{:S(2)}) collective-permute-start(bf16[16,208,128]{2,1,0:T(8,128)(2,1)S(1)} %pad.19.p0), channel_id=1, source_target_pairs={{0,8},{8,16},{16,24},{24,0},{1,9},{9,17},{17,25},{25,1},{2,10},{10... | collective-permute-start | bytes 2555912 | tf_op jit(solution)/shard_map/ppermute | solution.py:363
  75.6 11.4 %copy-start = (bf16[4,128,2048]{2,1,0:T(8,128)(2,1)}, bf16[4,128,2048]{2,1,0:T(8,128)(2,1)S(1)}, u32[]{:S(2)}) copy-start(bf16[4,128,2048]{2,1,0:T(8,128)(2,1)S(1)} %all-to-all-done.tok) | copy-start | bytes 6291460
  75.6 17.3 %collective-permute-start = (bf16[16,2048]{1,0:T(8,128)(2,1)S(1)}, bf16[16,2048]{1,0:T(8,128)(2,1)S(1)}, u32[]{:S(2)}, u32[]{:S(2)}) collective-permute-start(bf16[16,2048]{1,0:T(8,128)(2,1)S(1)} %slice_bitcast_fusion), channel_id=1, source_target_pairs={{0,4},{4,8},{8,12},{12,16},{16,20},{20,24},{24,28},{28,32},{32,36}... | collective-permute-start | bytes 196616 | tf_op jit(solution)/shard_map/ppermute | solution.py:421
  92.9 0.6 copy-start.8
  99.9 54.1 %copy-start.13 = (f32[4]{0:T(128)S(1)}, f32[4]{0:T(128)}, u32[]{:S(2)}) copy-start(f32[4]{0:T(128)} %param.38) | copy-start | bytes 52
  99.9 54.8 %copy-start.14 = (bf16[256]{0:T(256)(128)(2,1)S(1)}, bf16[256]{0:T(256)(128)(2,1)}, u32[]{:S(2)}) copy-start(bf16[256]{0:T(256)(128)(2,1)} %param.39) | copy-start | bytes 1540
  99.9 21.4 %all-to-all-start.2 = ((bf16[8,24,256]{2,1,0:T(8,128)(2,1)}), bf16[8,24,256]{2,1,0:T(8,128)(2,1)S(1)}, u32[]{:S(2)}, u32[]{:S(2)}) async-start(bf16[8,24,256]{2,1,0:T(8,128)(2,1)} %get-tuple-element.24), calls=%async_computation.2 | async-start | bytes 196608 | tf_op jit(solution)/shard_map/all_to_all | solution.py:354
  104.7 50.6 %collective-permute-start.6 = (bf16[16,208,128]{2,1,0:T(8,128)(2,1)S(1)}, bf16[16,208,128]{2,1,0:T(8,128)(2,1)S(1)}, u32[]{:S(2)}, u32[]{:S(2)}) collective-permute-start(bf16[16,208,128]{2,1,0:T(8,128)(2,1)S(1)} %pad.19.p0), channel_id=1, source_target_pairs={{0,4},{4,0},{1,5},{5,1},{2,6},{6,2},{3,7},{7,3},{8,12},{12,8},{9,1... | collective-permute-start | bytes 2555912 | tf_op jit(solution)/shard_map/ppermute | solution.py:367
  108.4 21.6 %collective-permute-start.5 = (bf16[8,208,128]{2,1,0:T(8,128)(2,1)}, bf16[8,208,128]{2,1,0:T(8,128)(2,1)S(1)}, u32[]{:S(2)}, u32[]{:S(2)}) collective-permute-start(bf16[8,208,128]{2,1,0:T(8,128)(2,1)} %slice.24), channel_id=1, source_target_pairs={{0,24},{8,0},{16,8},{24,16},{1,25},{9,1},{17,9},{25,17},{2,26},{10... | collective-permute-start | bytes 1277960 | tf_op jit(solution)/shard_map/ppermute | solution.py:363
  115.1 17.6 %collective-permute-start.4 = (bf16[8,208,128]{2,1,0:T(8,128)(2,1)}, bf16[8,208,128]{2,1,0:T(8,128)(2,1)}, u32[]{:S(2)}, u32[]{:S(2)}) collective-permute-start(bf16[8,208,128]{2,1,0:T(8,128)(2,1)} %slice.23), channel_id=1, source_target_pairs={{0,8},{8,16},{16,24},{24,0},{1,9},{9,17},{17,25},{25,1},{2,10},{10... | collective-permute-start | bytes 1277960 | tf_op jit(solution)/shard_map/ppermute | solution.py:363
  117.0 38.3 %collective-permute-start.7 = (bf16[16,208,128]{2,1,0:T(8,128)(2,1)}, bf16[16,208,128]{2,1,0:T(8,128)(2,1)S(1)}, u32[]{:S(2)}, u32[]{:S(2)}) collective-permute-start(bf16[16,208,128]{2,1,0:T(8,128)(2,1)} %collective-permute-done.2.p1), channel_id=1, source_target_pairs={{0,4},{4,0},{1,5},{5,1},{2,6},{6,2},{3,7},{7,3},{8,12},{12,8},{9,1... | collective-permute-start | bytes 2555912 | tf_op jit(solution)/shard_map/ppermute | solution.py:367
  119.3 36.0 %collective-permute-start.8 = (bf16[16,208,128]{2,1,0:T(8,128)(2,1)}, bf16[16,208,128]{2,1,0:T(8,128)(2,1)}, u32[]{:S(2)}, u32[]{:S(2)}) collective-permute-start(bf16[16,208,128]{2,1,0:T(8,128)(2,1)} %collective-permute-done.3.p2), channel_id=1, source_target_pairs={{0,4},{4,0},{1,5},{5,1},{2,6},{6,2},{3,7},{7,3},{8,12},{12,8},{9,1... | collective-permute-start | bytes 2555912 | tf_op jit(solution)/shard_map/ppermute | solution.py:367
  121.4 0.6 copy-start.5
  123.6 19.1 %all-to-all-start.3 = ((bf16[16,24,256]{2,1,0:T(8,128)(2,1)}), bf16[16,24,256]{2,1,0:T(8,128)(2,1)S(1)}, u32[]{:S(2)}, u32[]{:S(2)}) async-start(bf16[16,24,256]{2,1,0:T(8,128)(2,1)} %shard_map.202), calls=%async_computation.3 | async-start | bytes 393216 | tf_op jit(solution)/shard_map/all_to_all | solution.py:354
  130.1 25.3 %copy-start.4 = (bf16[8,208,128]{2,1,0:T(8,128)(2,1)}, bf16[8,208,128]{2,1,0:T(8,128)(2,1)S(1)}, u32[]{:S(2)}) copy-start(bf16[8,208,128]{2,1,0:T(8,128)(2,1)S(1)} %collective-permute-done.5.p4) | copy-start | bytes 1277956
  130.1 25.3 %collective-permute-start.10 = (bf16[8,208,128]{2,1,0:T(8,128)(2,1)S(1)}, bf16[8,208,128]{2,1,0:T(8,128)(2,1)}, u32[]{:S(2)}, u32[]{:S(2)}) collective-permute-start(bf16[8,208,128]{2,1,0:T(8,128)(2,1)S(1)} %collective-permute-done.5.p4), channel_id=1, source_target_pairs={{0,4},{4,0},{1,5},{5,1},{2,6},{6,2},{3,7},{7,3},{8,12},{12,8},{9,1... | collective-permute-start | bytes 1277960 | tf_op jit(solution)/shard_map/ppermute | solution.py:367
  132.7 22.7 %collective-permute-start.9 = (bf16[8,208,128]{2,1,0:T(8,128)(2,1)}, bf16[8,208,128]{2,1,0:T(8,128)(2,1)}, u32[]{:S(2)}, u32[]{:S(2)}) collective-permute-start(bf16[8,208,128]{2,1,0:T(8,128)(2,1)} %collective-permute-done.4.p3), channel_id=1, source_target_pairs={{0,4},{4,0},{1,5},{5,1},{2,6},{6,2},{3,7},{7,3},{8,12},{12,8},{9,1... | collective-permute-start | bytes 1277960 | tf_op jit(solution)/shard_map/ppermute | solution.py:367
  142.7 0.7 copy-start.6
  145.1 20.3 %all-to-all-start.4 = ((bf16[8,32,256]{2,1,0:T(8,128)(2,1)}), bf16[8,32,256]{2,1,0:T(8,128)(2,1)S(1)}, u32[]{:S(2)}, u32[]{:S(2)}) async-start(bf16[8,32,256]{2,1,0:T(8,128)(2,1)} %shard_map.203), calls=%async_computation.4 | async-start | bytes 262144 | tf_op jit(solution)/shard_map/all_to_all | solution.py:354
  155.3 0.9 copy-start.2
  155.3 1.2 copy-start.3
  165.3 0.7 copy-start.7

commit v3 on v2

--- a/solution.py
+++ b/solution.py
@@ -71,7 +71,8 @@
             copy.start()
 
 
-def first_copies(c, own, other, whole, sems):
+def first_copies(own, other, whole, sems):
+    c = lax.axis_index("c")
     return [
         pltpu.make_async_copy(
             src.at[x], whole.at[:, x, c if side == 0 else 1 - c], sems.at[2 * x + side]
@@ -81,18 +82,17 @@
     ]
 
 
-def ring_copies(x, c, parts, whole, sems, lo, count):
+def ring_copies(parts, whole, sems, lo, count):
+    x, c = lax.axis_index("x"), lax.axis_index("c")
     out = []
     for side in range(2):
         at = c if side == 0 else 1 - c
-        for i, (by, z, zs) in enumerate(
-            ((0, 0, 16), (3, 0, 16), (1, 0, 16), (2, 0, 8), (2, 8, 8))
-        ):
+        for i, by in enumerate((0, 3 - 2 * at, 1 + 2 * at, 2)):
             out.append(
                 pltpu.make_async_copy(
-                    parts[5 * side + i].at[:, lo : lo + count, :],
-                    whole.at[z : z + zs, (x + by) % 4, at],
-                    sems.at[5 * side + i],
+                    parts[4 * side + i].at[:, lo : lo + count, :],
+                    whole.at[:, (x + by) % 4, at],
+                    sems.at[4 * side + i],
                 )
             )
     return out
@@ -141,16 +141,16 @@
     lax.fori_loop(0, 8, some, 0, unroll=2)
 
 
-def cum_body(tok, ws, params, spikes, dt, cum, cum_t):
+def cum_body(tok, ws, bias, rate, spikes, dt, cum, cum_t, square):
     n = tok[...].reshape(ROWS, 2048)
-    raw = dot_nt(ws[...], n)[0:8] + params[0:8, 0:1]
+    raw = dot_nt(ws[...], n) + bias[...]
     step = jnp.maximum(raw, 0.0) + jnp.log1p(jnp.exp(-jnp.abs(raw)))
-    logs = -step * jnp.exp(params[0:8, 1:2]) + spikes[...]
+    logs = -step * jnp.exp(rate[...]) + spikes[...]
     r = lax.broadcasted_iota(jnp.int32, (BLK, BLK), 0)
     s = lax.broadcasted_iota(jnp.int32, (BLK, BLK), 1)
     upper = jnp.where(r <= s, 1.0, 0.0).astype(F32)
-    carry = jnp.zeros((8, 1), F32)
-    fill = jnp.zeros((BLK - 8, BLK), F32)
+    carry = jnp.zeros((4, 1), F32)
+    square[...] = jnp.zeros(square.shape, F32)
     for b in range(NB):
         rows = slice(b * BLK, (b + 1) * BLK)
         part = (
@@ -162,18 +162,20 @@
             )
             + carry
         )
-        cum_t[:, rows] = part
-        cum[rows, :] = jnp.concatenate([part, fill], axis=0).T
-        dt[rows, :] = jnp.concatenate([step[:, rows], fill], axis=0).T
+        cum_t[0:4, rows] = part
+        square[0, 0:4, :] = part
+        square[1, 0:4, :] = step[:, rows]
+        cum[rows, :] = square[0].T
+        dt[rows, :] = square[1].T
         carry = part[:, BLK - 1 : BLK]
 
 
 def first_body(
-    pos, tok, halo, own, other, dt, cum, input_taps, write_taps,
+    tok, halo, own, other, dt, cum, input_taps, write_taps,
     weighted, seq_input, seq_write, local, pieces,
     whole, normed, fields, sems,
 ):
-    moves = first_copies(pos[2], own, other, whole, sems)
+    moves = first_copies(own, other, whole, sems)
     run(moves, False)
     normed[0:HALO, :] = halo[...]
     normed[HALO:, :] = tok[...].reshape(ROWS, 2048)
@@ -234,8 +236,8 @@
         send[k] = one
 
 
-def enter_body(pos, got, planes, out):
-    z = pos[0]
+def enter_body(got, planes, out):
+    z = lax.axis_index("z")
     state = jnp.zeros((16, 256), F32)
     lefts = []
     for k in range(16):
@@ -251,14 +253,12 @@
 
 
 def rest_body(
-    pos, tok, halo, p0, p1, p2, p3, p4, p5, p6, p7, p8, p9,
-    weighted, seq_input, seq_write, local, cum, cum_t,
-    read_taps, gated_taps, direct,
-    partly, read_out, gate, mixer,
+    tok, halo, p0, p1, p2, p3, p4, p5, p6, p7, read_taps, gated_taps,
+    read_out, gate, mixer,
     whole, normed, fields, sems,
 ):
-    parts = (p0, p1, p2, p3, p4, p5, p6, p7, p8, p9)
-    moves = ring_copies(pos[1], pos[2], parts, whole, sems, 0, 144)
+    parts = (p0, p1, p2, p3, p4, p5, p6, p7)
+    moves = ring_copies(parts, whole, sems, 0, 144)
     run(moves, False)
     normed[0:HALO, :] = halo[...]
     normed[HALO:, :] = tok[...].reshape(ROWS, 2048)
@@ -269,13 +269,18 @@
         return dot(n, blocks(whole, lo, count)).astype(BF16).astype(F32)
 
     fields[:, 0:128] = projected(0, 1)
-    read = silu(taps(fields, read_taps, slice(0, 128), 4)).astype(BF16)
-    read_out[...] = read
+    read_out[...] = silu(taps(fields, read_taps, slice(0, 128), 4)).astype(BF16)
     gate[...] = silu(projected(1, 2)[HALO:])
     inner = projected(5, 2)
     fields[...] = inner * projected(7, 2)
     outer = projected(3, 2)[HALO:]
     mixer[...] = (outer * taps(fields, gated_taps, slice(0, 256), 3)).astype(BF16)
+
+
+def within_body(
+    read, weighted, seq_input, seq_write, local, cum, cum_t, direct, partly
+):
+    weight = per_head(direct[...])
     r = lax.broadcasted_iota(jnp.int32, (BLK, BLK), 0)
     s = lax.broadcasted_iota(jnp.int32, (BLK, BLK), 1)
     causal = r >= s
@@ -283,7 +288,7 @@
     before = jnp.zeros((1, 128), F32)
     for b in range(NB):
         rows = slice(b * BLK, (b + 1) * BLK)
-        rb = read[rows]
+        rb = read[rows, :]
         scores = dot_nt(rb, seq_write[rows, :])
         here = cum[rows, :]
         from_local = dot(rb, local[b]) * per_head(jnp.exp(here - before))
@@ -298,18 +303,47 @@
                 two.append(dot(damped.astype(BF16), pair))
             halves.append(jnp.where(low, two[0], two[1]))
         within = jnp.concatenate(halves, axis=1)
-        partly[rows, :] = within + from_local + direct[...] * seq_input[rows, :]
+        partly[rows, :] = within + from_local + weight * seq_input[rows, :]
+
+
+def wide_weights(parts, arriving, whole, sems):
+    moves = ring_copies(parts, whole, sems, 144, 64)
+    run(moves, False)
+
+    def finish():
+        run(moves, True)
+        row = lax.broadcasted_iota(jnp.int32, (16, 128), 0)
+        for j in range(8):
+            lefts = arriving[j, 16:32, :].astype(F32)
+            for z in range(16):
+                tile = whole[z, j // 2, j % 2, 48:64, :].astype(F32)
+                for i in range(2):
+                    v = lefts[z : z + 1, 128 * i : 128 * (i + 1)]
+                    v = jnp.broadcast_to(v, (16, 128))
+                    tile = jnp.where(row == 14 + i, v, tile)
+                whole[z, j // 2, j % 2, 48:64, :] = tile.astype(BF16)
+
+    return finish
+
+
+def project_out(act, at, whole, out):
+    a = act[pl.ds(pl.multiple_of(at * 128, 128), 128), :]
+    for q in range(4):
+        some = whole.at[4 * q : 4 * (q + 1)]
+        w = jnp.concatenate(
+            [some[:, :, :, 16 * k : 16 * (k + 1), :].reshape(512, 128) for k in range(4)],
+            axis=1,
+        )
+        out[:, 512 * q : 512 * (q + 1)] = dot_nt(a, w).astype(out.dtype)
 
 
 def tail_body(
-    pos, arriving, partly, read, gate, cum, mixer, scale,
-    p0, p1, p2, p3, p4, p5, p6, p7, p8, p9,
-    out,
-    whole, act, sems,
+    arriving, partly, read, gate, cum, mixer, scale,
+    p0, p1, p2, p3, p4, p5, p6, p7,
+    act, far, beside,
+    whole, sems,
 ):
-    parts = (p0, p1, p2, p3, p4, p5, p6, p7, p8, p9)
-    moves = ring_copies(pos[1], pos[2], parts, whole, sems, 144, 64)
-    run(moves, False)
+    finish = wide_weights((p0, p1, p2, p3, p4, p5, p6, p7), arriving, whole, sems)
     act[:, 0:256] = mixer[...]
     state = jnp.concatenate([arriving[j, 0:16, :] for j in range(8)], axis=0)
     head = partly[...] + dot(read[...], state) * per_head(jnp.exp(cum[...]))
@@ -322,32 +356,27 @@
     rest = (square - high.astype(F32)).astype(BF16)
     mean = dot(high, same) + dot(rest, same)
     act[:, 256:512] = (gated * lax.rsqrt(mean + EPS) * scale[...].astype(F32)).astype(BF16)
-    run(moves, True)
-    row = lax.broadcasted_iota(jnp.int32, (16, 128), 0)
-    for j in range(8):
-        lefts = arriving[j, 16:32, :].astype(F32)
-        for z in range(16):
-            tile = whole[z, j // 2, j % 2, 48:64, :].astype(F32)
-            for i in range(2):
-                v = lefts[z : z + 1, 128 * i : 128 * (i + 1)]
-                tile = jnp.where(row == 14 + i, jnp.broadcast_to(v, (16, 128)), tile)
-            whole[z, j // 2, j % 2, 48:64, :] = tile.astype(BF16)
-    a = act[...]
-    for q in range(4):
-        cols = slice(512 * q, 512 * (q + 1))
-        some = whole.at[4 * q : 4 * (q + 1)]
-        w = jnp.concatenate(
-            [some[:, :, :, 16 * k : 16 * (k + 1), :].reshape(512, 128) for k in range(4)],
-            axis=1,
-        )
-        out[:, cols] = dot_nt(a, w).astype(BF16)
-
-
-def sum_body(got, out):
-    v = got[0].astype(F32)
-    for y in range(1, 4):
-        v = v + got[y].astype(F32)
-    out[...] = v.astype(BF16)
+    finish()
+    y, c = lax.axis_index("tp"), lax.axis_index("c")
+    project_out(act, (y + 2) % 4, whole, far)
+    project_out(act, (y + 3 + 2 * c) % 4, whole, beside)
+
+
+def near_body(
+    arriving, act, p0, p1, p2, p3, p4, p5, p6, p7, near, mine, whole, sems
+):
+    wide_weights((p0, p1, p2, p3, p4, p5, p6, p7), arriving, whole, sems)()
+    y, c = lax.axis_index("tp"), lax.axis_index("c")
+    project_out(act, (y + 1 + 2 * c) % 4, whole, near)
+    project_out(act, y, whole, mine)
+
+
+def add_body(near, got, out):
+    out[...] = (near[...] + got[...].astype(F32)).astype(BF16)
+
+
+def sum_body(mine, a, b, out):
+    out[...] = (mine[...] + a[...].astype(F32) + b[...].astype(F32)).astype(BF16)
 
 
 def exchanged(tiles, axis):
@@ -359,8 +388,11 @@
     return exchanged(jnp.broadcast_to(shard[None], (n, *shard.shape)), axis)
 
 
-def passed(shard, by):
-    return lax.ppermute(shard, "x", [(i, (i + by) % 4) for i in range(4)])
+def two_way(shard, axis, toward):
+    steps = [(i, c, (i + (toward if c == 0 else -toward)) % 4) for i in range(4) for c in range(2)]
+    if axis == "x":
+        return lax.ppermute(shard, ("x", "c"), [(2 * i + c, 2 * j + c) for i, c, j in steps])
+    return lax.ppermute(shard, ("c", "tp"), [(4 * c + i, 4 * c + j) for i, c, j in steps])
 
 
 def swapped(shard):
@@ -390,7 +422,6 @@
     conv_output_weight,
     state_output_weight,
 ):
-    pos = jnp.stack([lax.axis_index(a).astype(jnp.int32) for a in SP])
     copied, own, left = call(
         prep_body,
         (shape((4, 128, 2048), BF16), shape((254, 128), BF16), shape((1, 256), F32)),
@@ -413,10 +444,9 @@
     first = copies(column[:, :48], "x")
     first_other = swapped(first)
     ring = [jnp.pad(column[:, 48:], ((0, 0), (0, 2), (0, 0)))]
-    ring.append(passed(ring[0], 1))
-    ring.append(passed(ring[0], 3))
-    ring.append(passed(ring[1][:8], 1))
-    ring.append(passed(ring[2][8:], 3))
+    ring.append(two_way(ring[0], "x", 1))
+    ring.append(two_way(ring[0], "x", -1))
+    ring.append(two_way(ring[1], "x", 1))
     ring += [swapped(part) for part in ring]
     halo = lax.ppermute(tok[3, 112:, :], SP, [(i, i + 1) for i in range(127)])
 
@@ -425,10 +455,12 @@
         (shape((ROWS, 128), F32), shape((ROWS, 128), F32), shape((8, ROWS), F32)),
         (
             tok,
-            jnp.pad(step_size_weight.T, ((0, 12), (0, 0))),
-            jnp.pad(jnp.stack([step_size_bias, log_decay_rate], 1), ((0, 4), (0, 126))),
-            jnp.pad(decay_spikes, ((0, 4), (0, 0))),
-        ),
+            step_size_weight.T,
+            step_size_bias[:, None],
+            log_decay_rate[:, None],
+            decay_spikes,
+        ),
+        scratch=(pltpu.VMEM((2, BLK, BLK), F32),),
     )
     weighted, seq_input, seq_write, local, pieces = call(
         first_body,
@@ -439,8 +471,8 @@
             shape((NB, 128, 256), BF16),
             shape((8, 24, 256), BF16),
         ),
-        (pos, tok, halo, first, first_other, dt, cum, input_conv_weight, write_conv_weight),
-        {0: SMEM, 3: HBM, 4: HBM},
+        (tok, halo, first, first_other, dt, cum, input_conv_weight, write_conv_weight),
+        {2: HBM, 3: HBM},
         (
             pltpu.VMEM((16, 4, 2, 48, 128), BF16),
             pltpu.VMEM((HALO + ROWS, 2048), BF16),
@@ -451,45 +483,50 @@
     got = exchanged(pieces, ("x", "c"))
     send = call(plane_body, shape((16, 24, 256), BF16), (got, left))
     planes = exchanged(send, "z")
-    entering = call(
-        enter_body, shape((8, 32, 256), BF16), (pos, got, planes), {0: SMEM}
-    )
+    entering = call(enter_body, shape((8, 32, 256), BF16), (got, planes))
     arriving = exchanged(entering, ("x", "c"))
 
-    direct = jnp.repeat(direct_path_weight, 64)[None]
-    partly, read, gate, mixer = call(
+    read, gate, mixer = call(
         rest_body,
         (
-            shape((ROWS, 256), F32),
             shape((ROWS, 128), BF16),
             shape((ROWS, 256), F32),
             shape((ROWS, 256), BF16),
         ),
-        (
-            pos, tok, halo, *ring, weighted, seq_input, seq_write, local, cum, cum_t,
-            read_conv_weight, gated_conv_weight, direct,
-        ),
-        {0: SMEM, **{i: HBM for i in range(3, 13)}},
+        (tok, halo, *ring, read_conv_weight, gated_conv_weight),
+        {i: HBM for i in range(2, 10)},
         (
             pltpu.VMEM((16, 4, 2, 144, 128), BF16),
             pltpu.VMEM((HALO + ROWS, 2048), BF16),
             pltpu.VMEM((HALO + ROWS, 256), F32),
-            pltpu.SemaphoreType.DMA((10,)),
-        ),
-    )
-    partial = call(
+            pltpu.SemaphoreType.DMA((8,)),
+        ),
+    )
+    partly = call(
+        within_body,
+        shape((ROWS, 256), F32),
+        (read, weighted, seq_input, seq_write, local, cum, cum_t, direct_path_weight[None]),
+    )
+    wide = (pltpu.VMEM((16, 4, 2, 64, 128), BF16), pltpu.SemaphoreType.DMA((8,)))
+    act, far, beside = call(
         tail_body,
-        shape((ROWS, 2048), BF16),
-        (pos, arriving, partly, read, gate, cum, mixer, head_norm_scale[None], *ring),
-        {0: SMEM, **{i: HBM for i in range(8, 18)}},
-        (
-            pltpu.VMEM((16, 4, 2, 64, 128), BF16),
-            pltpu.VMEM((ROWS, 512), BF16),
-            pltpu.SemaphoreType.DMA((10,)),
-        ),
-    )
-    parts = exchanged(partial.reshape(4, 128, 2048), "tp")
-    return call(sum_body, shape((128, 2048), BF16), (parts,))
+        (shape((ROWS, 512), BF16), shape((128, 2048), BF16), shape((128, 2048), BF16)),
+        (arriving, partly, read, gate, cum, mixer, head_norm_scale[None], *ring),
+        {i: HBM for i in range(7, 15)},
+        wide,
+    )
+    got_far = two_way(far, "tp", 1)
+    got_beside = two_way(beside, "tp", -1)
+    near, mine = call(
+        near_body,
+        (shape((128, 2048), F32), shape((128, 2048), F32)),
+        (arriving, act, *ring),
+        {i: HBM for i in range(2, 10)},
+        wide,
+    )
+    both = call(add_body, shape((128, 2048), BF16), (near, got_far))
+    got_near = two_way(both, "tp", 1)
+    return call(sum_body, shape((128, 2048), BF16), (mine, got_beside, got_near))
 
 
 def solution(mesh):

time: 206 us -> 203 us (0.985)
  the two profiles are of different devices: /device:TPU:1 before, /device:TPU:34 now
where the time goes in v3:
time: 203 us; the launch traced here: 201 us
  blocking collectives  77.6 us (38%)
  starting transfers between devices  49 us (24%)
  Pallas kernels  42.9 us (21%)
  waiting for transfers between devices  23.5 us (12%)
  local copies, waits for them, and re-layouts  8.14 us (4%)
    pallas_call x11, Pallas kernels, call(): pl.pallas_call(body, out_shape=outs, in_specs=[specs.get(i, vmem) for i i...  42.9 us
    all_gather x1, blocking collectives, per_device(): column = lax.all_gather(own, 'z', axis=0, tiled=False)  39.7 us
    all_to_all x2, blocking collectives, exchanged(): return lax.all_to_all(tiles, axis, 0, 0, tiled=True)  37.9 us
    all_to_all x3, starting transfers between devices, exchanged(): return lax.all_to_all(tiles, axis, 0, 0, tiled=True)  17.3 us
    ppermute x3, waiting for transfers between devices, two_way(): lax.ppermute(shard, ('x', 'c'), [(2 * i + c, 2 * j + c) for i, c, j in st...  12.4 us
    ppermute x3, starting transfers between devices, two_way(): lax.ppermute(shard, ('c', 'tp'), [(4 * c + i, 4 * c + j) for i, c, j in s...  11.4 us
    ppermute x3, waiting for transfers between devices, two_way(): lax.ppermute(shard, ('c', 'tp'), [(4 * c + i, 4 * c + j) for i, c, j in s...  11.2 us
    ppermute x5, starting transfers between devices, swapped(): return lax.ppermute(shard, 'c', [(0, 1), (1, 0)])  10.6 us
  transfers between devices with their start and end apart: 15, of which 3 were waited for; matrix products, arithmetic and copies ran while one was open for 1% of the time, Pallas kernels for 16%

profile of v3, /device:TPU:34, one launch (start us, length us, event | category | flops | bytes accessed | tf_op | source)
XLA Modules:
  0.0 201.4 jit_solution(7238415817617769044)
XLA Ops:
  0.0 1.3 broadcast_in_dim.21.gain
  1.3 3.1 %shard_map.199 = (bf16[4,128,2048]{2,1,0:T(8,128)(2,1)}, bf16[254,128]{1,0:T(8,128)(2,1)}, f32[1,256]{1,0:T(1,128)}) custom-call(bf16[128,2048]{1,0:T(8,128)(2,1)} %tok.1, bf16[1,2048]{1,0:T(2,128)(2,1)} %broadcast_in_dim.21.gain, bf16[16,256]{1,0:T(8,128)(2,1)} %w0.1, bf16[16,128]{1,0:T(8,128)(2,1)} %w1.1, bf16[16,128]{1,0:T(8,128)(2,1)} %w2.1, ...), custom_call_target="tpu_custom_call" | custom-call | tf_op jit(solution)/shard_map/pallas_call | solution.py:23
  4.4 39.7 %all-gather.1 = bf16[16,254,128]{2,1,0:T(8,128)(2,1)S(1)} all-gather(bf16[1,254,128]{2,1,0:T(8,128)(2,1)} %bitcast.9), channel_id=2, replica_groups=mesh['z'=16,'x'=4,'c'=2,'tp'=4] {'z'}, dimensions={0}, use_global_device_ids=true | all-gather | bytes 1105408 | tf_op jit(solution)/shard_map/all_gather | solution.py:443
  44.1 0.1 broadcast_in_dim.22
  44.2 12.8 %all_to_all.25.own = bf16[4,16,48,128]{3,2,1,0:T(8,128)(2,1)} all-to-all(bf16[4,16,48,128]{3,2,1,0:T(8,128)(2,1)S(1)} %broadcast_in_dim.22), channel_id=1, replica_groups=mesh['z'=16,'x'=4,'c'=2,'tp'=4] {'x'}, dimensions={0} | all-to-all | bytes 1572864 | tf_op jit(solution)/shard_map/all_to_all | solution.py:383
  57.0 4.5 %all-to-all-start = ((bf16[4,128,2048]{2,1,0:T(8,128)(2,1)}), bf16[4,128,2048]{2,1,0:T(8,128)(2,1)S(1)}, u32[]{:S(2)}, u32[]{:S(2)}) async-start(bf16[4,128,2048]{2,1,0:T(8,128)(2,1)} %get-tuple-element.24), calls=%async_computation | async-start | bytes 4194304 | tf_op jit(solution)/shard_map/all_to_all | solution.py:383
  61.4 0.1 slice.14
  61.5 0.1 pad.4.p0
  61.6 0.0 copy-start.1
  61.6 2.1 %collective-permute-start.2 = (bf16[16,208,128]{2,1,0:T(8,128)(2,1)S(1)}, bf16[16,208,128]{2,1,0:T(8,128)(2,1)}, u32[]{:S(2)}, u32[]{:S(2)}) collective-permute-start(bf16[16,208,128]{2,1,0:T(8,128)(2,1)S(1)} %pad.4.p0), channel_id=1, source_target_pairs={{0,8},{4,28},{8,16},{12,4},{16,24},{20,12},{24,0},{28,20},{1,9},{5... | collective-permute-start | bytes 2555912 | tf_op jit(solution)/shard_map/ppermute | solution.py:394
  63.7 1.9 collective-permute-start.1
  65.6 3.7 %collective-permute-start.3 = (bf16[16,208,128]{2,1,0:T(8,128)(2,1)S(1)}, bf16[16,208,128]{2,1,0:T(8,128)(2,1)}, u32[]{:S(2)}, u32[]{:S(2)}) collective-permute-start(bf16[16,208,128]{2,1,0:T(8,128)(2,1)S(1)} %pad.4.p0), channel_id=1, source_target_pairs={{0,24},{4,12},{8,0},{12,20},{16,8},{20,28},{24,16},{28,4},{1,25},{... | collective-permute-start | bytes 2555912 | tf_op jit(solution)/shard_map/ppermute | solution.py:394
  69.4 12.4 %collective-permute-done.2.p1 = bf16[16,208,128]{2,1,0:T(8,128)(2,1)} collective-permute-done((bf16[16,208,128]{2,1,0:T(8,128)(2,1)S(1)}, bf16[16,208,128]{2,1,0:T(8,128)(2,1)}, u32[]{:S(2)}, u32[]{:S(2)}) %collective-permute-start.2) | collective-permute-done | bytes 852000 | tf_op jit(solution)/shard_map/ppermute | solution.py:394
  81.7 1.9 collective-permute-start.4
  83.6 0.0 all-to-all-done.tok
  83.6 0.0 copy-start
  83.7 1.9 collective-permute-start
  85.6 0.0 copy-done.10
  85.6 0.7 copy.24.bias
  86.3 0.0 copy-done.11
  86.3 0.7 copy.25.rate
  87.0 0.0 copy-done
  87.0 3.6 %shard_map.200 = (f32[512,128]{1,0:T(8,128)}, f32[512,128]{1,0:T(8,128)}, f32[8,512]{1,0:T(8,128)}) custom-call(bf16[4,128,2048]{2,1,0:T(8,128)(2,1)} %copy-done, bf16[4,2048]{1,0:T(4,128)(2,1)} %bitcast.10, f32[4,1]{1,0:T(4,128)} %copy.24.bias, f32[4,1]{1,0:T(4,128)} %copy.25.rate, f32[4,512]{1,0:T(4,128)} %spikes.1), custom_call_target="tpu_custom_call" | custom-call | tf_op jit(solution)/shard_map/pallas_call | solution.py:23
  90.6 0.0 collective-permute-done.1.other
  90.6 0.0 collective-permute-done.halo
  90.6 0.0 copy-start.9
  90.6 0.6 copy-done.9
  91.2 6.4 %shard_map.201 = (bf16[512,256]{1,0:T(8,128)(2,1)}, f32[512,256]{1,0:T(8,128)}, bf16[512,128]{1,0:T(8,128)(2,1)}, bf16[4,128,256]{2,1,0:T(8,128)(2,1)}, bf16[8,24,256]{2,1,0:T(8,128)(2,1)}) custom-call(bf16[4,128,2048]{2,1,0:T(8,128)(2,1)} %copy-done, bf16[16,2048]{1,0:T(8,128)(2,1)} %copy-done.9, bf16[4,16,48,128]{3,2,1,0:T(8,128)(2,1)} %all_to_all.25.own, ...), custom_call_target="tpu_custom_call" | custom-call | tf_op jit(solution)/shard_map/pallas_call | solution.py:23
  97.7 8.1 %all-to-all-start.2 = ((bf16[8,24,256]{2,1,0:T(8,128)(2,1)}), bf16[8,24,256]{2,1,0:T(8,128)(2,1)S(1)}, u32[]{:S(2)}, u32[]{:S(2)}) async-start(bf16[8,24,256]{2,1,0:T(8,128)(2,1)} %get-tuple-element.28), calls=%async_computation.2 | async-start | bytes 196608 | tf_op jit(solution)/shard_map/all_to_all | solution.py:383
  105.7 2.0 collective-permute-start.5
  107.8 2.3 %collective-permute-start.6 = (bf16[16,208,128]{2,1,0:T(8,128)(2,1)}, bf16[16,208,128]{2,1,0:T(8,128)(2,1)S(1)}, u32[]{:S(2)}, u32[]{:S(2)}) collective-permute-start(bf16[16,208,128]{2,1,0:T(8,128)(2,1)} %collective-permute-done.2.p1), channel_id=1, source_target_pairs={{0,4},{4,0},{1,5},{5,1},{2,6},{6,2},{3,7},{7,3},{8,12},{12,8},{9,1... | collective-permute-start | bytes 2555912 | tf_op jit(solution)/shard_map/ppermute | solution.py:399
  110.1 0.0 collective-permute-done.3.p2
  110.1 2.0 %collective-permute-start.7 = (bf16[16,208,128]{2,1,0:T(8,128)(2,1)}, bf16[16,208,128]{2,1,0:T(8,128)(2,1)}, u32[]{:S(2)}, u32[]{:S(2)}) collective-permute-start(bf16[16,208,128]{2,1,0:T(8,128)(2,1)} %collective-permute-done.3.p2), channel_id=1, source_target_pairs={{0,4},{4,0},{1,5},{5,1},{2,6},{6,2},{3,7},{7,3},{8,12},{12,8},{9,1... | collective-permute-start | bytes 2555912 | tf_op jit(solution)/shard_map/ppermute | solution.py:399
  112.1 0.0 collective-permute-done.4.p3
  112.1 2.3 %collective-permute-start.8 = (bf16[16,208,128]{2,1,0:T(8,128)(2,1)}, bf16[16,208,128]{2,1,0:T(8,128)(2,1)}, u32[]{:S(2)}, u32[]{:S(2)}) collective-permute-start(bf16[16,208,128]{2,1,0:T(8,128)(2,1)} %collective-permute-done.4.p3), channel_id=1, source_target_pairs={{0,4},{4,0},{1,5},{5,1},{2,6},{6,2},{3,7},{7,3},{8,12},{12,8},{9,1... | collective-permute-start | bytes 2555912 | tf_op jit(solution)/shard_map/ppermute | solution.py:399
  114.4 0.0 all-to-all-done.2.got
  114.5 0.6 copy-done.5
  115.1 1.6 shard_map.202
  116.7 25.1 %all_to_all.26.planes = bf16[16,24,256]{2,1,0:T(8,128)(2,1)} all-to-all(bf16[16,24,256]{2,1,0:T(8,128)(2,1)} %shard_map.202), channel_id=1, replica_groups=mesh['z'=16,'x'=4,'c'=2,'tp'=4] {'z'}, dimensions={0} | all-to-all | bytes 393216 | tf_op jit(solution)/shard_map/all_to_all | solution.py:383
  141.8 1.7 shard_map.203
  143.6 4.8 %all-to-all-start.4 = ((bf16[8,32,256]{2,1,0:T(8,128)(2,1)}), bf16[8,32,256]{2,1,0:T(8,128)(2,1)S(1)}, u32[]{:S(2)}, u32[]{:S(2)}) async-start(bf16[8,32,256]{2,1,0:T(8,128)(2,1)} %shard_map.203), calls=%async_computation.4 | async-start | bytes 262144 | tf_op jit(solution)/shard_map/all_to_all | solution.py:383
  148.4 0.5 broadcast_in_dim.26.scale
  148.9 0.0 collective-permute-done.5.p4
  148.9 0.0 collective-permute-done.6.p5
  148.9 0.0 collective-permute-done.7.p6
  148.9 0.0 collective-permute-done.8.p7
  148.9 0.9 copy-done.2
  149.9 0.3 copy-done.3
  150.2 7.9 %shard_map.204 = (bf16[512,128]{1,0:T(8,128)(2,1)}, f32[512,256]{1,0:T(8,128)}, bf16[512,256]{1,0:T(8,128)(2,1)}) custom-call(bf16[4,128,2048]{2,1,0:T(8,128)(2,1)} %copy-done, bf16[16,2048]{1,0:T(8,128)(2,1)} %copy-done.9, bf16[16,208,128]{2,1,0:T(8,128)(2,1)} %copy-done.1, bf16[16,208,128]{2,1,0:T(8,128)(2,1)} %collective-permute-done.2.p1, ...), custom_call_target="tpu_custom_call" | custom-call | tf_op jit(solution)/shard_map/pallas_call | solution.py:23
  158.1 3.1 %shard_map.205.partly = f32[512,256]{1,0:T(8,128)} custom-call(bf16[512,128]{1,0:T(8,128)(2,1)} %get-tuple-element.30.read, bf16[512,256]{1,0:T(8,128)(2,1)} %get-tuple-element.31.weighted, f32[512,256]{1,0:T(8,128)} %get-tuple-element.32.seq_input, bf16[512,128]{1,0:T(8,128)(2,1)} %get-tuple-element.33.seq_write, ...), custom_call_target="tpu_custom_call" | custom-call | tf_op jit(solution)/shard_map/pallas_call | solution.py:23
  161.2 0.0 all-to-all-done.4.arriving
  161.2 0.7 copy-done.4
  161.9 5.5 %shard_map.206 = (bf16[512,512]{1,0:T(8,128)(2,1)}, bf16[128,2048]{1,0:T(8,128)(2,1)}, bf16[128,2048]{1,0:T(8,128)(2,1)}) custom-call(bf16[8,32,256]{2,1,0:T(8,128)(2,1)} %copy-done.4, f32[512,256]{1,0:T(8,128)} %shard_map.205.partly, bf16[512,128]{1,0:T(8,128)(2,1)} %get-tuple-element.30.read, f32[512,256]{1,0:T(8,128)} %get-tuple-element.36.gate, ...), custom_call_target="tpu_custom_call" | custom-call | tf_op jit(solution)/shard_map/pallas_call | solution.py:23
  167.3 3.9 %collective-permute-start.10 = (bf16[128,2048]{1,0:T(8,128)(2,1)}, bf16[128,2048]{1,0:T(8,128)(2,1)S(1)}, u32[]{:S(2)}, u32[]{:S(2)}) collective-permute-start(bf16[128,2048]{1,0:T(8,128)(2,1)} %get-tuple-element.42), channel_id=1, source_target_pairs={{0,1},{4,7},{1,2},{5,4},{2,3},{6,5},{3,0},{7,6},{8,9},{12,15},{9,1... | collective-permute-start | bytes 1572872 | tf_op jit(solution)/shard_map/ppermute | solution.py:395
  171.3 3.1 %collective-permute-start.9 = (bf16[128,2048]{1,0:T(8,128)(2,1)}, bf16[128,2048]{1,0:T(8,128)(2,1)S(1)}, u32[]{:S(2)}, u32[]{:S(2)}) collective-permute-start(bf16[128,2048]{1,0:T(8,128)(2,1)} %get-tuple-element.40), channel_id=1, source_target_pairs={{0,3},{4,5},{1,0},{5,6},{2,1},{6,7},{3,2},{7,4},{8,11},{12,13},{9,... | collective-permute-start | bytes 1572872 | tf_op jit(solution)/shard_map/ppermute | solution.py:395
  174.4 5.2 %shard_map.207 = (f32[128,2048]{1,0:T(8,128)}, f32[128,2048]{1,0:T(8,128)}) custom-call(bf16[8,32,256]{2,1,0:T(8,128)(2,1)} %copy-done.4, bf16[512,512]{1,0:T(8,128)(2,1)} %get-tuple-element.38.act, bf16[16,208,128]{2,1,0:T(8,128)(2,1)} %copy-done.1, bf16[16,208,128]{2,1,0:T(8,128)(2,1)} %collective-permute-done.2.p1, ...), custom_call_target="tpu_custom_call" | custom-call | tf_op jit(solution)/shard_map/pallas_call | solution.py:23
  179.6 2.0 %collective-permute-done.10.got = bf16[128,2048]{1,0:T(8,128)(2,1)S(1)} collective-permute-done((bf16[128,2048]{1,0:T(8,128)(2,1)}, bf16[128,2048]{1,0:T(8,128)(2,1)S(1)}, u32[]{:S(2)}, u32[]{:S(2)}) %collective-permute-start.10) | collective-permute-done | bytes 524320 | tf_op jit(solution)/shard_map/ppermute | solution.py:395
  181.6 0.8 copy-done.8
  182.4 2.3 %shard_map.208 = bf16[128,2048]{1,0:T(8,128)(2,1)} custom-call(f32[128,2048]{1,0:T(8,128)} %get-tuple-element.41.near, bf16[128,2048]{1,0:T(8,128)(2,1)} %copy-done.8), custom_call_target="tpu_custom_call" | custom-call | tf_op jit(solution)/shard_map/pallas_call | solution.py:23
  184.6 4.3 %collective-permute-start.11 = (bf16[128,2048]{1,0:T(8,128)(2,1)}, bf16[128,2048]{1,0:T(8,128)(2,1)S(1)}, u32[]{:S(2)}, u32[]{:S(2)}) collective-permute-start(bf16[128,2048]{1,0:T(8,128)(2,1)} %shard_map.208), channel_id=1, source_target_pairs={{0,1},{4,7},{1,2},{5,4},{2,3},{6,5},{3,0},{7,6},{8,9},{12,15},{9,1... | collective-permute-start | bytes 1572872 | tf_op jit(solution)/shard_map/ppermute | solution.py:395
  189.0 0.0 collective-permute-done.9.a
  189.0 9.1 %collective-permute-done.11.b = bf16[128,2048]{1,0:T(8,128)(2,1)S(1)} collective-permute-done((bf16[128,2048]{1,0:T(8,128)(2,1)}, bf16[128,2048]{1,0:T(8,128)(2,1)S(1)}, u32[]{:S(2)}, u32[]{:S(2)}) %collective-permute-start.11) | collective-permute-done | bytes 524320 | tf_op jit(solution)/shard_map/ppermute | solution.py:395
  198.1 0.8 copy-done.7
  198.9 2.5 %shard_map.209 = bf16[128,2048]{1,0:T(8,128)(2,1)} custom-call(f32[128,2048]{1,0:T(8,128)} %get-tuple-element.39.mine, bf16[128,2048]{1,0:T(8,128)(2,1)} %copy-done.6, bf16[128,2048]{1,0:T(8,128)(2,1)} %copy-done.7), custom_call_target="tpu_custom_call" | custom-call | tf_op jit(solution)/shard_map/pallas_call | solution.py:23
  (15 shorter events, 0.0 us)
Async XLA Ops:
  57.0 26.7 %all-to-all-start = ((bf16[4,128,2048]{2,1,0:T(8,128)(2,1)}), bf16[4,128,2048]{2,1,0:T(8,128)(2,1)S(1)}, u32[]{:S(2)}, u32[]{:S(2)}) async-start(bf16[4,128,2048]{2,1,0:T(8,128)(2,1)} %get-tuple-element.24), calls=%async_computation | async-start | bytes 4194304 | tf_op jit(solution)/shard_map/all_to_all | solution.py:383
  61.4 24.2 %copy-start.10 = (f32[4]{0:T(128)S(1)}, f32[4]{0:T(128)}, u32[]{:S(2)}) copy-start(f32[4]{0:T(128)} %param.35) | copy-start | bytes 52
  61.4 24.9 %copy-start.11 = (f32[4]{0:T(128)S(1)}, f32[4]{0:T(128)}, u32[]{:S(2)}) copy-start(f32[4]{0:T(128)} %param.36) | copy-start | bytes 52
  61.6 87.4 %copy-start.1 = (bf16[16,208,128]{2,1,0:T(8,128)(2,1)}, bf16[16,208,128]{2,1,0:T(8,128)(2,1)S(1)}, u32[]{:S(2)}) copy-start(bf16[16,208,128]{2,1,0:T(8,128)(2,1)S(1)} %pad.4.p0) | copy-start | bytes 2555908
  61.6 20.2 %collective-permute-start.2 = (bf16[16,208,128]{2,1,0:T(8,128)(2,1)S(1)}, bf16[16,208,128]{2,1,0:T(8,128)(2,1)}, u32[]{:S(2)}, u32[]{:S(2)}) collective-permute-start(bf16[16,208,128]{2,1,0:T(8,128)(2,1)S(1)} %pad.4.p0), channel_id=1, source_target_pairs={{0,8},{4,28},{8,16},{12,4},{16,24},{20,12},{24,0},{28,20},{1,9},{5... | collective-permute-start | bytes 2555912 | tf_op jit(solution)/shard_map/ppermute | solution.py:394
  63.7 26.9 %collective-permute-start.1 = (bf16[4,16,48,128]{3,2,1,0:T(8,128)(2,1)}, bf16[4,16,48,128]{3,2,1,0:T(8,128)(2,1)}, u32[]{:S(2)}, u32[]{:S(2)}) collective-permute-start(bf16[4,16,48,128]{3,2,1,0:T(8,128)(2,1)} %all_to_all.25.own), channel_id=1, source_target_pairs={{0,4},{4,0},{1,5},{5,1},{2,6},{6,2},{3,7},{7,3},{8,12},{12,8},{9,1... | collective-permute-start | bytes 2359304 | tf_op jit(solution)/shard_map/ppermute | solution.py:399
  65.6 44.4 %collective-permute-start.3 = (bf16[16,208,128]{2,1,0:T(8,128)(2,1)S(1)}, bf16[16,208,128]{2,1,0:T(8,128)(2,1)}, u32[]{:S(2)}, u32[]{:S(2)}) collective-permute-start(bf16[16,208,128]{2,1,0:T(8,128)(2,1)S(1)} %pad.4.p0), channel_id=1, source_target_pairs={{0,24},{4,12},{8,0},{12,20},{16,8},{20,28},{24,16},{28,4},{1,25},{... | collective-permute-start | bytes 2555912 | tf_op jit(solution)/shard_map/ppermute | solution.py:394
  81.7 30.4 %collective-permute-start.4 = (bf16[16,208,128]{2,1,0:T(8,128)(2,1)}, bf16[16,208,128]{2,1,0:T(8,128)(2,1)}, u32[]{:S(2)}, u32[]{:S(2)}) collective-permute-start(bf16[16,208,128]{2,1,0:T(8,128)(2,1)} %collective-permute-done.2.p1), channel_id=1, source_target_pairs={{0,8},{4,28},{8,16},{12,4},{16,24},{20,12},{24,0},{28,20},{1,9},{5... | collective-permute-start | bytes 2555912 | tf_op jit(solution)/shard_map/ppermute | solution.py:394
  83.6 3.3 %copy-start = (bf16[4,128,2048]{2,1,0:T(8,128)(2,1)}, bf16[4,128,2048]{2,1,0:T(8,128)(2,1)S(1)}, u32[]{:S(2)}) copy-start(bf16[4,128,2048]{2,1,0:T(8,128)(2,1)S(1)} %all-to-all-done.tok) | copy-start | bytes 6291460
  83.7 6.9 %collective-permute-start = (bf16[16,2048]{1,0:T(8,128)(2,1)S(1)}, bf16[16,2048]{1,0:T(8,128)(2,1)S(1)}, u32[]{:S(2)}, u32[]{:S(2)}) collective-permute-start(bf16[16,2048]{1,0:T(8,128)(2,1)S(1)} %slice_bitcast_fusion), channel_id=1, source_target_pairs={{0,4},{4,8},{8,12},{12,16},{16,20},{20,24},{24,28},{28,32},{32,36}... | collective-permute-start | bytes 196616 | tf_op jit(solution)/shard_map/ppermute | solution.py:451
  90.6 0.6 copy-start.9
  91.2 57.1 %copy-start.12 = (bf16[256]{0:T(256)(128)(2,1)S(1)}, bf16[256]{0:T(256)(128)(2,1)}, u32[]{:S(2)}) copy-start(bf16[256]{0:T(256)(128)(2,1)} %param.39) | copy-start | bytes 1540
  97.7 16.8 %all-to-all-start.2 = ((bf16[8,24,256]{2,1,0:T(8,128)(2,1)}), bf16[8,24,256]{2,1,0:T(8,128)(2,1)S(1)}, u32[]{:S(2)}, u32[]{:S(2)}) async-start(bf16[8,24,256]{2,1,0:T(8,128)(2,1)} %get-tuple-element.28), calls=%async_computation.2 | async-start | bytes 196608 | tf_op jit(solution)/shard_map/all_to_all | solution.py:383
  105.7 43.1 %collective-permute-start.5 = (bf16[16,208,128]{2,1,0:T(8,128)(2,1)S(1)}, bf16[16,208,128]{2,1,0:T(8,128)(2,1)S(1)}, u32[]{:S(2)}, u32[]{:S(2)}) collective-permute-start(bf16[16,208,128]{2,1,0:T(8,128)(2,1)S(1)} %pad.4.p0), channel_id=1, source_target_pairs={{0,4},{4,0},{1,5},{5,1},{2,6},{6,2},{3,7},{7,3},{8,12},{12,8},{9,1... | collective-permute-start | bytes 2555912 | tf_op jit(solution)/shard_map/ppermute | solution.py:399
  107.8 41.1 %collective-permute-start.6 = (bf16[16,208,128]{2,1,0:T(8,128)(2,1)}, bf16[16,208,128]{2,1,0:T(8,128)(2,1)S(1)}, u32[]{:S(2)}, u32[]{:S(2)}) collective-permute-start(bf16[16,208,128]{2,1,0:T(8,128)(2,1)} %collective-permute-done.2.p1), channel_id=1, source_target_pairs={{0,4},{4,0},{1,5},{5,1},{2,6},{6,2},{3,7},{7,3},{8,12},{12,8},{9,1... | collective-permute-start | bytes 2555912 | tf_op jit(solution)/shard_map/ppermute | solution.py:399
  110.1 38.8 %collective-permute-start.7 = (bf16[16,208,128]{2,1,0:T(8,128)(2,1)}, bf16[16,208,128]{2,1,0:T(8,128)(2,1)}, u32[]{:S(2)}, u32[]{:S(2)}) collective-permute-start(bf16[16,208,128]{2,1,0:T(8,128)(2,1)} %collective-permute-done.3.p2), channel_id=1, source_target_pairs={{0,4},{4,0},{1,5},{5,1},{2,6},{6,2},{3,7},{7,3},{8,12},{12,8},{9,1... | collective-permute-start | bytes 2555912 | tf_op jit(solution)/shard_map/ppermute | solution.py:399
  112.1 36.8 %collective-permute-start.8 = (bf16[16,208,128]{2,1,0:T(8,128)(2,1)}, bf16[16,208,128]{2,1,0:T(8,128)(2,1)}, u32[]{:S(2)}, u32[]{:S(2)}) collective-permute-start(bf16[16,208,128]{2,1,0:T(8,128)(2,1)} %collective-permute-done.4.p3), channel_id=1, source_target_pairs={{0,4},{4,0},{1,5},{5,1},{2,6},{6,2},{3,7},{7,3},{8,12},{12,8},{9,1... | collective-permute-start | bytes 2555912 | tf_op jit(solution)/shard_map/ppermute | solution.py:399
  114.4 0.6 copy-start.5
  143.6 17.7 %all-to-all-start.4 = ((bf16[8,32,256]{2,1,0:T(8,128)(2,1)}), bf16[8,32,256]{2,1,0:T(8,128)(2,1)S(1)}, u32[]{:S(2)}, u32[]{:S(2)}) async-start(bf16[8,32,256]{2,1,0:T(8,128)(2,1)} %shard_map.203), calls=%async_computation.4 | async-start | bytes 262144 | tf_op jit(solution)/shard_map/all_to_all | solution.py:383
  148.9 1.0 copy-start.2
  148.9 1.3 copy-start.3
  161.2 0.7 copy-start.4
  167.3 14.3 %collective-permute-start.10 = (bf16[128,2048]{1,0:T(8,128)(2,1)}, bf16[128,2048]{1,0:T(8,128)(2,1)S(1)}, u32[]{:S(2)}, u32[]{:S(2)}) collective-permute-start(bf16[128,2048]{1,0:T(8,128)(2,1)} %get-tuple-element.42), channel_id=1, source_target_pairs={{0,1},{4,7},{1,2},{5,4},{2,3},{6,5},{3,0},{7,6},{8,9},{12,15},{9,1... | collective-permute-start | bytes 1572872 | tf_op jit(solution)/shard_map/ppermute | solution.py:395
  171.3 17.7 %collective-permute-start.9 = (bf16[128,2048]{1,0:T(8,128)(2,1)}, bf16[128,2048]{1,0:T(8,128)(2,1)S(1)}, u32[]{:S(2)}, u32[]{:S(2)}) collective-permute-start(bf16[128,2048]{1,0:T(8,128)(2,1)} %get-tuple-element.40), channel_id=1, source_target_pairs={{0,3},{4,5},{1,0},{5,6},{2,1},{6,7},{3,2},{7,4},{8,11},{12,13},{9,... | collective-permute-start | bytes 1572872 | tf_op jit(solution)/shard_map/ppermute | solution.py:395
  181.6 0.8 copy-start.8
  184.6 13.5 %collective-permute-start.11 = (bf16[128,2048]{1,0:T(8,128)(2,1)}, bf16[128,2048]{1,0:T(8,128)(2,1)S(1)}, u32[]{:S(2)}, u32[]{:S(2)}) collective-permute-start(bf16[128,2048]{1,0:T(8,128)(2,1)} %shard_map.208), channel_id=1, source_target_pairs={{0,1},{4,7},{1,2},{5,4},{2,3},{6,5},{3,0},{7,6},{8,9},{12,15},{9,1... | collective-permute-start | bytes 1572872 | tf_op jit(solution)/shard_map/ppermute | solution.py:395
  189.0 9.1 %copy-start.6 = (bf16[128,2048]{1,0:T(8,128)(2,1)}, bf16[128,2048]{1,0:T(8,128)(2,1)S(1)}, u32[]{:S(2)}) copy-start(bf16[128,2048]{1,0:T(8,128)(2,1)S(1)} %collective-permute-done.9.a) | copy-start | bytes 1572868
  198.1 0.8 copy-start.7

commit v4 on v3

--- a/solution.py
+++ b/solution.py
@@ -17,20 +17,16 @@
 BF16 = jnp.bfloat16
 
 
-def call(body, outs, args, specs=None, scratch=()):
+def call(body, outs, args, scratch=(), mib=8):
     vmem = pl.BlockSpec(memory_space=pltpu.VMEM)
-    specs = specs or {}
     return pl.pallas_call(
         body,
         out_shape=outs,
-        in_specs=[specs.get(i, vmem) for i in range(len(args))],
+        in_specs=[vmem for _ in args],
         out_specs=jax.tree.map(lambda _: vmem, outs),
         scratch_shapes=list(scratch),
+        compiler_params=pltpu.CompilerParams(vmem_limit_bytes=mib * 2**20),
     )(*args)
-
-
-HBM = pl.BlockSpec(memory_space=pltpu.HBM)
-SMEM = pl.BlockSpec(memory_space=pltpu.SMEM)
 
 
 def shape(dims, kind):
@@ -63,39 +59,36 @@
     return v / (1.0 + jnp.exp(-v))
 
 
-def run(copies, wait):
-    for copy in copies:
-        if wait:
-            copy.wait()
-        else:
-            copy.start()
-
-
-def first_copies(own, other, whole, sems):
+def lay_out(pieces, targets):
+    def some(z, _):
+        for get, x, c in pieces:
+            for ref, lo, count in targets:
+                ref[z, x, c] = get(z, lo, count)
+        return 0
+
+    lax.fori_loop(0, 16, some, 0)
+
+
+def first_pieces(own, other):
     c = lax.axis_index("c")
     return [
-        pltpu.make_async_copy(
-            src.at[x], whole.at[:, x, c if side == 0 else 1 - c], sems.at[2 * x + side]
+        (lambda z, lo, n, r=ref, x=x: r[x, z, lo : lo + n, :], x, at)
+        for ref, at in ((own, c), (other, 1 - c))
+        for x in range(4)
+    ]
+
+
+def ring_pieces(parts):
+    x, c = lax.axis_index("x"), lax.axis_index("c")
+    return [
+        (
+            lambda z, lo, n, r=parts[4 * side + i]: r[z, lo : lo + n, :],
+            (x + by) % 4,
+            at,
         )
-        for x in range(4)
-        for side, src in ((0, own), (1, other))
+        for side, at in ((0, c), (1, 1 - c))
+        for i, by in enumerate((0, 3 - 2 * at, 1 + 2 * at, 2))
     ]
-
-
-def ring_copies(parts, whole, sems, lo, count):
-    x, c = lax.axis_index("x"), lax.axis_index("c")
-    out = []
-    for side in range(2):
-        at = c if side == 0 else 1 - c
-        for i, by in enumerate((0, 3 - 2 * at, 1 + 2 * at, 2)):
-            out.append(
-                pltpu.make_async_copy(
-                    parts[4 * side + i].at[:, lo : lo + count, :],
-                    whole.at[:, (x + by) % 4, at],
-                    sems.at[4 * side + i],
-                )
-            )
-    return out
 
 
 def block(whole, q):
@@ -173,13 +166,11 @@
 def first_body(
     tok, halo, own, other, dt, cum, input_taps, write_taps,
     weighted, seq_input, seq_write, local, pieces,
-    whole, normed, fields, sems,
+    whole, normed, fields,
 ):
-    moves = first_copies(own, other, whole, sems)
-    run(moves, False)
+    lay_out(first_pieces(own, other), ((whole, 0, 48),))
     normed[0:HALO, :] = halo[...]
     normed[HALO:, :] = tok[...].reshape(ROWS, 2048)
-    run(moves, True)
     projected = dot(normed[...], blocks(whole, 0, 3))
     fields[...] = projected.astype(BF16).astype(F32)
     xin = silu(taps(fields, input_taps, slice(0, 256), 4))
@@ -254,15 +245,13 @@
 
 def rest_body(
     tok, halo, p0, p1, p2, p3, p4, p5, p6, p7, read_taps, gated_taps,
-    read_out, gate, mixer,
-    whole, normed, fields, sems,
+    read_out, gate, mixer, wide,
+    whole, normed, fields,
 ):
-    parts = (p0, p1, p2, p3, p4, p5, p6, p7)
-    moves = ring_copies(parts, whole, sems, 0, 144)
-    run(moves, False)
+    parts = ring_pieces((p0, p1, p2, p3, p4, p5, p6, p7))
+    lay_out(parts, ((whole, 0, 144), (wide, 144, 64)))
     normed[0:HALO, :] = halo[...]
     normed[HALO:, :] = tok[...].reshape(ROWS, 2048)
-    run(moves, True)
     n = normed[...]
 
     def projected(lo, count):
@@ -306,44 +295,30 @@
         partly[rows, :] = within + from_local + weight * seq_input[rows, :]
 
 
-def wide_weights(parts, arriving, whole, sems):
-    moves = ring_copies(parts, whole, sems, 144, 64)
-    run(moves, False)
-
-    def finish():
-        run(moves, True)
-        row = lax.broadcasted_iota(jnp.int32, (16, 128), 0)
-        for j in range(8):
-            lefts = arriving[j, 16:32, :].astype(F32)
-            for z in range(16):
-                tile = whole[z, j // 2, j % 2, 48:64, :].astype(F32)
-                for i in range(2):
-                    v = lefts[z : z + 1, 128 * i : 128 * (i + 1)]
-                    v = jnp.broadcast_to(v, (16, 128))
-                    tile = jnp.where(row == 14 + i, v, tile)
-                whole[z, j // 2, j % 2, 48:64, :] = tile.astype(BF16)
-
-    return finish
-
-
-def project_out(act, at, whole, out):
+def patch(wide, arriving, fixed):
+    row = lax.broadcasted_iota(jnp.int32, (16, 128), 0)
+    for j in range(8):
+        lefts = arriving[j, 16:32, :].astype(F32)
+        for z in range(16):
+            tile = wide[z, j // 2, j % 2, 48:64, :].astype(F32)
+            for i in range(2):
+                v = lefts[z : z + 1, 128 * i : 128 * (i + 1)]
+                tile = jnp.where(row == 14 + i, jnp.broadcast_to(v, (16, 128)), tile)
+            fixed[z, j // 2, j % 2] = tile.astype(BF16)
+
+
+def project_out(act, at, wide, fixed, out):
     a = act[pl.ds(pl.multiple_of(at * 128, 128), 128), :]
     for q in range(4):
-        some = whole.at[4 * q : 4 * (q + 1)]
-        w = jnp.concatenate(
-            [some[:, :, :, 16 * k : 16 * (k + 1), :].reshape(512, 128) for k in range(4)],
-            axis=1,
-        )
+        zs = slice(4 * q, 4 * (q + 1))
+        w = [wide[zs, :, :, 16 * k : 16 * (k + 1), :].reshape(512, 128) for k in range(3)]
+        w = jnp.concatenate([*w, fixed[zs].reshape(512, 128)], axis=1)
         out[:, 512 * q : 512 * (q + 1)] = dot_nt(a, w).astype(out.dtype)
 
 
 def tail_body(
-    arriving, partly, read, gate, cum, mixer, scale,
-    p0, p1, p2, p3, p4, p5, p6, p7,
-    act, far, beside,
-    whole, sems,
+    arriving, partly, read, gate, cum, mixer, scale, wide, act, far, fixed
 ):
-    finish = wide_weights((p0, p1, p2, p3, p4, p5, p6, p7), arriving, whole, sems)
     act[:, 0:256] = mixer[...]
     state = jnp.concatenate([arriving[j, 0:16, :] for j in range(8)], axis=0)
     head = partly[...] + dot(read[...], state) * per_head(jnp.exp(cum[...]))
@@ -356,27 +331,24 @@
     rest = (square - high.astype(F32)).astype(BF16)
     mean = dot(high, same) + dot(rest, same)
     act[:, 256:512] = (gated * lax.rsqrt(mean + EPS) * scale[...].astype(F32)).astype(BF16)
-    finish()
+    patch(wide, arriving, fixed)
+    project_out(act, (lax.axis_index("tp") + 2) % 4, wide, fixed, far)
+
+
+def near_body(act, wide, fixed, beside, near, mine):
     y, c = lax.axis_index("tp"), lax.axis_index("c")
-    project_out(act, (y + 2) % 4, whole, far)
-    project_out(act, (y + 3 + 2 * c) % 4, whole, beside)
-
-
-def near_body(
-    arriving, act, p0, p1, p2, p3, p4, p5, p6, p7, near, mine, whole, sems
-):
-    wide_weights((p0, p1, p2, p3, p4, p5, p6, p7), arriving, whole, sems)()
-    y, c = lax.axis_index("tp"), lax.axis_index("c")
-    project_out(act, (y + 1 + 2 * c) % 4, whole, near)
-    project_out(act, y, whole, mine)
+    project_out(act, (y + 3 + 2 * c) % 4, wide, fixed, beside)
+    project_out(act, (y + 1 + 2 * c) % 4, wide, fixed, near)
+    project_out(act, y, wide, fixed, mine)
 
 
 def add_body(near, got, out):
-    out[...] = (near[...] + got[...].astype(F32)).astype(BF16)
+    out[...] = (near[...].astype(F32) + got[...].astype(F32)).astype(BF16)
 
 
 def sum_body(mine, a, b, out):
-    out[...] = (mine[...] + a[...].astype(F32) + b[...].astype(F32)).astype(BF16)
+    v = mine[...].astype(F32) + a[...].astype(F32)
+    out[...] = (v + b[...].astype(F32)).astype(BF16)
 
 
 def exchanged(tiles, axis):
@@ -472,13 +444,12 @@
             shape((8, 24, 256), BF16),
         ),
         (tok, halo, first, first_other, dt, cum, input_conv_weight, write_conv_weight),
-        {2: HBM, 3: HBM},
         (
             pltpu.VMEM((16, 4, 2, 48, 128), BF16),
             pltpu.VMEM((HALO + ROWS, 2048), BF16),
             pltpu.VMEM((HALO + ROWS, 384), F32),
-            pltpu.SemaphoreType.DMA((8,)),
-        ),
+        ),
+        mib=16,
     )
     got = exchanged(pieces, ("x", "c"))
     send = call(plane_body, shape((16, 24, 256), BF16), (got, left))
@@ -486,44 +457,43 @@
     entering = call(enter_body, shape((8, 32, 256), BF16), (got, planes))
     arriving = exchanged(entering, ("x", "c"))
 
-    read, gate, mixer = call(
+    read, gate, mixer, wide = call(
         rest_body,
         (
             shape((ROWS, 128), BF16),
             shape((ROWS, 256), F32),
             shape((ROWS, 256), BF16),
+            shape((16, 4, 2, 64, 128), BF16),
         ),
         (tok, halo, *ring, read_conv_weight, gated_conv_weight),
-        {i: HBM for i in range(2, 10)},
-        (
+        scratch=(
             pltpu.VMEM((16, 4, 2, 144, 128), BF16),
             pltpu.VMEM((HALO + ROWS, 2048), BF16),
             pltpu.VMEM((HALO + ROWS, 256), F32),
-            pltpu.SemaphoreType.DMA((8,)),
-        ),
+        ),
+        mib=28,
     )
     partly = call(
         within_body,
         shape((ROWS, 256), F32),
         (read, weighted, seq_input, seq_write, local, cum, cum_t, direct_path_weight[None]),
     )
-    wide = (pltpu.VMEM((16, 4, 2, 64, 128), BF16), pltpu.SemaphoreType.DMA((8,)))
-    act, far, beside = call(
+    act, far, fixed = call(
         tail_body,
-        (shape((ROWS, 512), BF16), shape((128, 2048), BF16), shape((128, 2048), BF16)),
-        (arriving, partly, read, gate, cum, mixer, head_norm_scale[None], *ring),
-        {i: HBM for i in range(7, 15)},
-        wide,
+        (
+            shape((ROWS, 512), BF16),
+            shape((128, 2048), BF16),
+            shape((16, 4, 2, 16, 128), BF16),
+        ),
+        (arriving, partly, read, gate, cum, mixer, head_norm_scale[None], wide),
+        mib=16,
     )
     got_far = two_way(far, "tp", 1)
+    block_ = shape((128, 2048), BF16)
+    beside, near, mine = call(
+        near_body, (block_, block_, block_), (act, wide, fixed), mib=12
+    )
     got_beside = two_way(beside, "tp", -1)
-    near, mine = call(
-        near_body,
-        (shape((128, 2048), F32), shape((128, 2048), F32)),
-        (arriving, act, *ring),
-        {i: HBM for i in range(2, 10)},
-        wide,
-    )
     both = call(add_body, shape((128, 2048), BF16), (near, got_far))
     got_near = two_way(both, "tp", 1)
     return call(sum_body, shape((128, 2048), BF16), (mine, got_beside, got_near))

time: 203 us -> 195 us (0.961)
  Pallas kernels: 42.9 us -> 19.7 us
  local copies, waits for them, and re-layouts: 8.14 us -> 20 us
  waiting for transfers between devices: 23.5 us -> 27.4 us
    pallas_call x11, Pallas kernels: 42.9 us -> 19.7 us  [call(): pl.pallas_call(body, out_shape=outs, in_specs=[vmem for _ in args], out_s...]
    unnamed x26 -> x72, local copies, waits for them, and re-layouts: 4.73 us -> 18.3 us
    ppermute x1, waiting for transfers between devices: 0.01 us -> 2.94 us  [per_device(): halo = lax.ppermute(tok[3, 112:, :], SP, [(i, i + 1) for i in range(127)])]
  transfers between devices with their start and end apart: 15 -> 15, of which waited for: 3 -> 5; matrix products, arithmetic and copies ran while one was open for 1% -> 0% of each run, Pallas kernels for 16% -> 9%
where the time goes in v4:
time: 195 us; the launch traced here: 193 us
  blocking collectives  78.2 us (40%)
  starting transfers between devices  47.6 us (24%)
  waiting for transfers between devices  27.4 us (14%)
  local copies, waits for them, and re-layouts  20 us (10%)
  Pallas kernels  19.7 us (10%)
    all_gather x1, blocking collectives, per_device(): column = lax.all_gather(own, 'z', axis=0, tiled=False)  39.4 us
    all_to_all x2, blocking collectives, exchanged(): return lax.all_to_all(tiles, axis, 0, 0, tiled=True)  38.8 us
    pallas_call x11, Pallas kernels, call(): pl.pallas_call(body, out_shape=outs, in_specs=[vmem for _ in args], out_s...  19.7 us
    unnamed x72, local copies, waits for them, and re-layouts  18.3 us
    all_to_all x3, starting transfers between devices, exchanged(): return lax.all_to_all(tiles, axis, 0, 0, tiled=True)  16.5 us
    ppermute x3, waiting for transfers between devices, two_way(): lax.ppermute(shard, ('x', 'c'), [(2 * i + c, 2 * j + c) for i, c, j in st...  12.4 us
    ppermute x3, waiting for transfers between devices, two_way(): lax.ppermute(shard, ('c', 'tp'), [(4 * c + i, 4 * c + j) for i, c, j in s...  12.1 us
    ppermute x3, starting transfers between devices, two_way(): lax.ppermute(shard, ('c', 'tp'), [(4 * c + i, 4 * c + j) for i, c, j in s...  10.9 us
  transfers between devices with their start and end apart: 15, of which 5 were waited for; matrix products, arithmetic and copies ran while one was open for 0% of the time, Pallas kernels for 9%

profile of v4, /device:TPU:34, one launch (start us, length us, event | category | flops | bytes accessed | tf_op | source)
XLA Modules:
  0.0 193.4 jit_solution(10406803044756967856)
XLA Ops:
  0.0 0.7 broadcast_in_dim.21.gain
  0.7 1.0 copy-done.7
  1.7 0.7 copy-done.17
  2.4 0.7 copy-done.18
  3.1 0.7 copy-done.19
  3.8 0.7 copy-done.20
  4.5 0.7 copy-done.21
  5.2 0.7 copy-done.22
  5.9 0.7 copy-done.23
  6.6 0.7 copy-done.25
  7.3 0.7 copy-done.26
  8.0 0.6 shard_map.199
  8.6 1.3 copy-done.2
  9.9 39.4 %all-gather.1 = bf16[16,254,128]{2,1,0:T(8,128)(2,1)S(1)} all-gather(bf16[1,254,128]{2,1,0:T(8,128)(2,1)S(1)} %bitcast.9), channel_id=2, replica_groups=mesh['z'=16,'x'=4,'c'=2,'tp'=4] {'z'}, dimensions={0}, use_global_device_ids=true | all-gather | bytes 1105408 | tf_op jit(solution)/shard_map/all_gather | solution.py:415
  49.4 0.1 broadcast_in_dim.22
  49.5 12.8 %all_to_all.25.own = bf16[4,16,48,128]{3,2,1,0:T(8,128)(2,1)} all-to-all(bf16[4,16,48,128]{3,2,1,0:T(8,128)(2,1)S(1)} %broadcast_in_dim.22), channel_id=1, replica_groups=mesh['z'=16,'x'=4,'c'=2,'tp'=4] {'x'}, dimensions={0} | all-to-all | bytes 1572864 | tf_op jit(solution)/shard_map/all_to_all | solution.py:355
  62.3 4.5 %all-to-all-start = ((bf16[4,128,2048]{2,1,0:T(8,128)(2,1)}), bf16[4,128,2048]{2,1,0:T(8,128)(2,1)S(1)}, u32[]{:S(2)}, u32[]{:S(2)}) async-start(bf16[4,128,2048]{2,1,0:T(8,128)(2,1)} %copy-done.2), calls=%async_computation | async-start | bytes 4194304 | tf_op jit(solution)/shard_map/all_to_all | solution.py:355
  66.8 0.1 slice.14
  66.8 0.0 copy-start.29
  66.8 0.1 pad.4.p0
  66.9 2.1 %collective-permute-start.2 = (bf16[16,208,128]{2,1,0:T(8,128)(2,1)S(1)}, bf16[16,208,128]{2,1,0:T(8,128)(2,1)}, u32[]{:S(2)}, u32[]{:S(2)}) collective-permute-start(bf16[16,208,128]{2,1,0:T(8,128)(2,1)S(1)} %pad.4.p0), channel_id=1, source_target_pairs={{0,8},{4,28},{8,16},{12,4},{16,24},{20,12},{24,0},{28,20},{1,9},{5... | collective-permute-start | bytes 2555912 | tf_op jit(solution)/shard_map/ppermute | solution.py:366
  69.1 1.9 collective-permute-start.1
  71.0 3.7 %collective-permute-start.3 = (bf16[16,208,128]{2,1,0:T(8,128)(2,1)S(1)}, bf16[16,208,128]{2,1,0:T(8,128)(2,1)}, u32[]{:S(2)}, u32[]{:S(2)}) collective-permute-start(bf16[16,208,128]{2,1,0:T(8,128)(2,1)S(1)} %pad.4.p0), channel_id=1, source_target_pairs={{0,24},{4,12},{8,0},{12,20},{16,8},{20,28},{24,16},{28,4},{1,25},{... | collective-permute-start | bytes 2555912 | tf_op jit(solution)/shard_map/ppermute | solution.py:366
  74.7 12.4 %collective-permute-done.2.p1 = bf16[16,208,128]{2,1,0:T(8,128)(2,1)} collective-permute-done((bf16[16,208,128]{2,1,0:T(8,128)(2,1)S(1)}, bf16[16,208,128]{2,1,0:T(8,128)(2,1)}, u32[]{:S(2)}, u32[]{:S(2)}) %collective-permute-start.2) | collective-permute-done | bytes 852000 | tf_op jit(solution)/shard_map/ppermute | solution.py:366
  87.1 1.9 collective-permute-start.4
  89.0 1.9 collective-permute-start
  91.0 0.1 copy.24.bias
  91.1 0.1 copy.25.rate
  91.1 1.2 shard_map.200
  92.4 2.9 %collective-permute-done.halo = bf16[16,2048]{1,0:T(8,128)(2,1)S(1)} collective-permute-done((bf16[16,2048]{1,0:T(8,128)(2,1)S(1)}, bf16[16,2048]{1,0:T(8,128)(2,1)S(1)}, u32[]{:S(2)}, u32[]{:S(2)}) %collective-permute-start) | collective-permute-done | bytes 65568 | tf_op jit(solution)/shard_map/ppermute | solution.py:423
  95.3 4.5 %shard_map.201 = (bf16[512,256]{1,0:T(8,128)(2,1)S(1)}, f32[512,256]{1,0:T(8,128)S(1)}, bf16[512,128]{1,0:T(8,128)(2,1)S(1)}, bf16[4,128,256]{2,1,0:T(8,128)(2,1)S(1)}, bf16[8,24,256]{2,1,0:T(8,128)(2,1)}) custom-call(bf16[4,128,2048]{2,1,0:T(8,128)(2,1)S(1)} %all-to-all-done.tok, bf16[16,2048]{1,0:T(8,128)(2,1)S(1)} %collective-permute-done.halo, ...), custom_call_target="tpu_custom_call" | custom-call | tf_op jit(solution)/shard_map/pallas_call | solution.py:22
  99.8 0.8 copy-done.3
  100.6 0.7 copy-done.8
  101.3 0.7 copy-done.10
  102.0 0.6 copy-done.14
  102.7 7.2 %all-to-all-start.2 = ((bf16[8,24,256]{2,1,0:T(8,128)(2,1)}), bf16[8,24,256]{2,1,0:T(8,128)(2,1)S(1)}, u32[]{:S(2)}, u32[]{:S(2)}) async-start(bf16[8,24,256]{2,1,0:T(8,128)(2,1)} %get-tuple-element.30), calls=%async_computation.2 | async-start | bytes 196608 | tf_op jit(solution)/shard_map/all_to_all | solution.py:355
  109.9 2.0 %collective-permute-start.5 = (bf16[16,208,128]{2,1,0:T(8,128)(2,1)S(1)}, bf16[16,208,128]{2,1,0:T(8,128)(2,1)}, u32[]{:S(2)}, u32[]{:S(2)}) collective-permute-start(bf16[16,208,128]{2,1,0:T(8,128)(2,1)S(1)} %pad.4.p0), channel_id=1, source_target_pairs={{0,4},{4,0},{1,5},{5,1},{2,6},{6,2},{3,7},{7,3},{8,12},{12,8},{9,1... | collective-permute-start | bytes 2555912 | tf_op jit(solution)/shard_map/ppermute | solution.py:371
  111.9 2.3 %collective-permute-start.6 = (bf16[16,208,128]{2,1,0:T(8,128)(2,1)}, bf16[16,208,128]{2,1,0:T(8,128)(2,1)}, u32[]{:S(2)}, u32[]{:S(2)}) collective-permute-start(bf16[16,208,128]{2,1,0:T(8,128)(2,1)} %collective-permute-done.2.p1), channel_id=1, source_target_pairs={{0,4},{4,0},{1,5},{5,1},{2,6},{6,2},{3,7},{7,3},{8,12},{12,8},{9,1... | collective-permute-start | bytes 2555912 | tf_op jit(solution)/shard_map/ppermute | solution.py:371
  114.2 2.0 %collective-permute-start.7 = (bf16[16,208,128]{2,1,0:T(8,128)(2,1)}, bf16[16,208,128]{2,1,0:T(8,128)(2,1)}, u32[]{:S(2)}, u32[]{:S(2)}) collective-permute-start(bf16[16,208,128]{2,1,0:T(8,128)(2,1)} %collective-permute-done.3.p2), channel_id=1, source_target_pairs={{0,4},{4,0},{1,5},{5,1},{2,6},{6,2},{3,7},{7,3},{8,12},{12,8},{9,1... | collective-permute-start | bytes 2555912 | tf_op jit(solution)/shard_map/ppermute | solution.py:371
  116.3 2.3 %collective-permute-start.8 = (bf16[16,208,128]{2,1,0:T(8,128)(2,1)}, bf16[16,208,128]{2,1,0:T(8,128)(2,1)}, u32[]{:S(2)}, u32[]{:S(2)}) collective-permute-start(bf16[16,208,128]{2,1,0:T(8,128)(2,1)} %collective-permute-done.4.p3), channel_id=1, source_target_pairs={{0,4},{4,0},{1,5},{5,1},{2,6},{6,2},{3,7},{7,3},{8,12},{12,8},{9,1... | collective-permute-start | bytes 2555912 | tf_op jit(solution)/shard_map/ppermute | solution.py:371
  118.6 26.1 %all_to_all.26.planes = bf16[16,24,256]{2,1,0:T(8,128)(2,1)S(1)} all-to-all(bf16[16,24,256]{2,1,0:T(8,128)(2,1)S(1)} %shard_map.202), channel_id=1, replica_groups=mesh['z'=16,'x'=4,'c'=2,'tp'=4] {'z'}, dimensions={0} | all-to-all | bytes 393216 | tf_op jit(solution)/shard_map/all_to_all | solution.py:355
  144.7 0.7 shard_map.203
  145.4 4.8 %all-to-all-start.4 = ((bf16[8,32,256]{2,1,0:T(8,128)(2,1)}), bf16[8,32,256]{2,1,0:T(8,128)(2,1)S(1)}, u32[]{:S(2)}, u32[]{:S(2)}) async-start(bf16[8,32,256]{2,1,0:T(8,128)(2,1)} %shard_map.203), calls=%async_computation.4 | async-start | bytes 262144 | tf_op jit(solution)/shard_map/all_to_all | solution.py:355
  150.3 0.5 broadcast_in_dim.26.scale
  150.9 0.8 copy-done.28
  151.6 0.7 copy-done.31
  152.3 6.7 %shard_map.204 = (bf16[512,128]{1,0:T(8,128)(2,1)S(1)}, f32[512,256]{1,0:T(8,128)S(1)}, bf16[512,256]{1,0:T(8,128)(2,1)S(1)}, bf16[16,4,2,64,128]{4,3,2,1,0:T(8,128)(2,1)S(1)}) custom-call(bf16[4,128,2048]{2,1,0:T(8,128)(2,1)S(1)} %all-to-all-done.tok, bf16[16,2048]{1,0:T(8,128)(2,1)S(1)} %collective-permute-done.halo, bf16[16,208,128]{2,1,0:T(8,128)(2,1)S(1)} %pad.4.p0, ...), custom_call_target="tpu_custom_call" | custom-call | tf_op jit(solution)/shard_map/pallas_call | solution.py:22
  159.0 1.3 copy-done
  160.3 0.8 copy-done.5
  161.1 0.7 copy-done.12
  161.9 1.0 shard_map.205.partly
  162.9 0.6 copy-done.1
  163.4 1.0 copy-done.6
  164.5 0.9 copy-done.13
  165.4 1.7 shard_map.206
  167.1 3.9 %collective-permute-start.10 = (bf16[128,2048]{1,0:T(8,128)(2,1)S(1)}, bf16[128,2048]{1,0:T(8,128)(2,1)S(1)}, u32[]{:S(2)}, u32[]{:S(2)}) collective-permute-start(bf16[128,2048]{1,0:T(8,128)(2,1)S(1)} %get-tuple-element.46), channel_id=1, source_target_pairs={{0,1},{4,7},{1,2},{5,4},{2,3},{6,5},{3,0},{7,6},{8,9},{12,15},{9,1... | collective-permute-start | bytes 1572872 | tf_op jit(solution)/shard_map/ppermute | solution.py:367
  171.0 2.2 %shard_map.207 = (bf16[128,2048]{1,0:T(8,128)(2,1)S(1)}, bf16[128,2048]{1,0:T(8,128)(2,1)S(1)}, bf16[128,2048]{1,0:T(8,128)(2,1)S(1)}) custom-call(bf16[512,512]{1,0:T(8,128)(2,1)S(1)} %get-tuple-element.41.act, bf16[16,4,2,64,128]{4,3,2,1,0:T(8,128)(2,1)S(1)} %copy-done.1, bf16[16,4,2,16,128]{4,3,2,1,0:T(8,128)(2,1)S(1)} %get-tuple-element.42.fixed), custom_call_target="tpu_custom_call" | custom-call | tf_op jit(solution)/shard_map/pallas_call | solution.py:22
  173.2 3.1 %collective-permute-start.9 = (bf16[128,2048]{1,0:T(8,128)(2,1)S(1)}, bf16[128,2048]{1,0:T(8,128)(2,1)S(1)}, u32[]{:S(2)}, u32[]{:S(2)}) collective-permute-start(bf16[128,2048]{1,0:T(8,128)(2,1)S(1)} %get-tuple-element.44), channel_id=1, source_target_pairs={{0,3},{4,5},{1,0},{5,6},{2,1},{6,7},{3,2},{7,4},{8,11},{12,13},{9,... | collective-permute-start | bytes 1572872 | tf_op jit(solution)/shard_map/ppermute | solution.py:367
  176.3 3.1 %collective-permute-done.10.got = bf16[128,2048]{1,0:T(8,128)(2,1)S(1)} collective-permute-done((bf16[128,2048]{1,0:T(8,128)(2,1)S(1)}, bf16[128,2048]{1,0:T(8,128)(2,1)S(1)}, u32[]{:S(2)}, u32[]{:S(2)}) %collective-permute-start.10) | collective-permute-done | bytes 524320 | tf_op jit(solution)/shard_map/ppermute | solution.py:367
  179.4 0.1 shard_map.208
  179.5 3.9 %collective-permute-start.11 = (bf16[128,2048]{1,0:T(8,128)(2,1)S(1)}, bf16[128,2048]{1,0:T(8,128)(2,1)S(1)}, u32[]{:S(2)}, u32[]{:S(2)}) collective-permute-start(bf16[128,2048]{1,0:T(8,128)(2,1)S(1)} %shard_map.208), channel_id=1, source_target_pairs={{0,1},{4,7},{1,2},{5,4},{2,3},{6,5},{3,0},{7,6},{8,9},{12,15},{9,1... | collective-permute-start | bytes 1572872 | tf_op jit(solution)/shard_map/ppermute | solution.py:367
  183.4 1.7 collective-permute-done.9.a
  185.1 7.3 %collective-permute-done.11.b = bf16[128,2048]{1,0:T(8,128)(2,1)S(1)} collective-permute-done((bf16[128,2048]{1,0:T(8,128)(2,1)S(1)}, bf16[128,2048]{1,0:T(8,128)(2,1)S(1)}, u32[]{:S(2)}, u32[]{:S(2)}) %collective-permute-start.11) | collective-permute-done | bytes 524320 | tf_op jit(solution)/shard_map/ppermute | solution.py:367
  192.4 1.0 shard_map.209
  (61 shorter events, 0.2 us)
Async XLA Ops:
  0.7 1.0 copy-start.7
  1.7 0.7 copy-start.17
  2.4 0.7 copy-start.18
  3.1 0.7 copy-start.19
  3.8 0.7 copy-start.20
  4.5 0.7 copy-start.21
  5.2 0.7 copy-start.22
  5.9 0.7 copy-start.23
  6.6 0.7 copy-start.25
  7.3 0.7 copy-start.26
  8.6 1.4 copy-start.2
  62.3 26.7 %all-to-all-start = ((bf16[4,128,2048]{2,1,0:T(8,128)(2,1)}), bf16[4,128,2048]{2,1,0:T(8,128)(2,1)S(1)}, u32[]{:S(2)}, u32[]{:S(2)}) async-start(bf16[4,128,2048]{2,1,0:T(8,128)(2,1)} %copy-done.2), calls=%async_computation | async-start | bytes 4194304 | tf_op jit(solution)/shard_map/all_to_all | solution.py:355
  66.7 24.2 %copy-start.33 = (f32[4]{0:T(128)S(1)}, f32[4]{0:T(128)}, u32[]{:S(2)}) copy-start(f32[4]{0:T(128)} %param.35) | copy-start | bytes 52
  66.7 24.3 %copy-start.34 = (f32[4]{0:T(128)S(1)}, f32[4]{0:T(128)}, u32[]{:S(2)}) copy-start(f32[4]{0:T(128)} %param.36) | copy-start | bytes 52
  66.7 24.4 %copy-start.16 = (bf16[2048,4]{0,1:T(4,128)(2,1)S(1)}, bf16[2048,4]{0,1:T(4,128)(2,1)}, u32[]{:S(2)}) copy-start(bf16[2048,4]{0,1:T(4,128)(2,1)} %param.30) | copy-start | bytes 49156
  66.7 24.4 %copy-start.24 = (f32[4,512]{1,0:T(4,128)S(1)}, f32[4,512]{1,0:T(4,128)}, u32[]{:S(2)}) copy-start(f32[4,512]{1,0:T(4,128)} %spikes.1) | copy-start | bytes 24580
  66.8 28.5 %copy-start.27 = (bf16[4,256]{1,0:T(4,128)(2,1)S(1)}, bf16[4,256]{1,0:T(4,128)(2,1)}, u32[]{:S(2)}) copy-start(bf16[4,256]{1,0:T(4,128)(2,1)} %input_taps.1) | copy-start | bytes 6148
  66.8 28.5 %copy-start.29 = (bf16[4,128]{1,0:T(4,128)(2,1)S(1)}, bf16[4,128]{1,0:T(4,128)(2,1)}, u32[]{:S(2)}) copy-start(bf16[4,128]{1,0:T(4,128)(2,1)} %write_taps.1) | copy-start | bytes 3076
  66.9 20.2 %collective-permute-start.2 = (bf16[16,208,128]{2,1,0:T(8,128)(2,1)S(1)}, bf16[16,208,128]{2,1,0:T(8,128)(2,1)}, u32[]{:S(2)}, u32[]{:S(2)}) collective-permute-start(bf16[16,208,128]{2,1,0:T(8,128)(2,1)S(1)} %pad.4.p0), channel_id=1, source_target_pairs={{0,8},{4,28},{8,16},{12,4},{16,24},{20,12},{24,0},{28,20},{1,9},{5... | collective-permute-start | bytes 2555912 | tf_op jit(solution)/shard_map/ppermute | solution.py:366
  69.1 23.3 %collective-permute-start.1 = (bf16[4,16,48,128]{3,2,1,0:T(8,128)(2,1)}, bf16[4,16,48,128]{3,2,1,0:T(8,128)(2,1)}, u32[]{:S(2)}, u32[]{:S(2)}) collective-permute-start(bf16[4,16,48,128]{3,2,1,0:T(8,128)(2,1)} %all_to_all.25.own), channel_id=1, source_target_pairs={{0,4},{4,0},{1,5},{5,1},{2,6},{6,2},{3,7},{7,3},{8,12},{12,8},{9,1... | collective-permute-start | bytes 2359304 | tf_op jit(solution)/shard_map/ppermute | solution.py:371
  71.0 43.2 %collective-permute-start.3 = (bf16[16,208,128]{2,1,0:T(8,128)(2,1)S(1)}, bf16[16,208,128]{2,1,0:T(8,128)(2,1)}, u32[]{:S(2)}, u32[]{:S(2)}) collective-permute-start(bf16[16,208,128]{2,1,0:T(8,128)(2,1)S(1)} %pad.4.p0), channel_id=1, source_target_pairs={{0,24},{4,12},{8,0},{12,20},{16,8},{20,28},{24,16},{28,4},{1,25},{... | collective-permute-start | bytes 2555912 | tf_op jit(solution)/shard_map/ppermute | solution.py:366
  87.1 29.2 %collective-permute-start.4 = (bf16[16,208,128]{2,1,0:T(8,128)(2,1)}, bf16[16,208,128]{2,1,0:T(8,128)(2,1)}, u32[]{:S(2)}, u32[]{:S(2)}) collective-permute-start(bf16[16,208,128]{2,1,0:T(8,128)(2,1)} %collective-permute-done.2.p1), channel_id=1, source_target_pairs={{0,8},{4,28},{8,16},{12,4},{16,24},{20,12},{24,0},{28,20},{1,9},{5... | collective-permute-start | bytes 2555912 | tf_op jit(solution)/shard_map/ppermute | solution.py:366
  89.0 6.3 %collective-permute-start = (bf16[16,2048]{1,0:T(8,128)(2,1)S(1)}, bf16[16,2048]{1,0:T(8,128)(2,1)S(1)}, u32[]{:S(2)}, u32[]{:S(2)}) collective-permute-start(bf16[16,2048]{1,0:T(8,128)(2,1)S(1)} %slice_bitcast_fusion), channel_id=1, source_target_pairs={{0,4},{4,8},{8,12},{12,16},{16,20},{20,24},{24,28},{28,32},{32,36}... | collective-permute-start | bytes 196616 | tf_op jit(solution)/shard_map/ppermute | solution.py:423
  95.3 54.9 %copy-start.35 = (bf16[256]{0:T(256)(128)(2,1)S(1)}, bf16[256]{0:T(256)(128)(2,1)}, u32[]{:S(2)}) copy-start(bf16[256]{0:T(256)(128)(2,1)} %param.39) | copy-start | bytes 1540
  99.8 0.8 copy-start.3
  100.6 0.7 copy-start.8
  101.3 0.7 copy-start.10
  102.0 0.6 copy-start.14
  102.7 15.9 %all-to-all-start.2 = ((bf16[8,24,256]{2,1,0:T(8,128)(2,1)}), bf16[8,24,256]{2,1,0:T(8,128)(2,1)S(1)}, u32[]{:S(2)}, u32[]{:S(2)}) async-start(bf16[8,24,256]{2,1,0:T(8,128)(2,1)} %get-tuple-element.30), calls=%async_computation.2 | async-start | bytes 196608 | tf_op jit(solution)/shard_map/all_to_all | solution.py:355
  109.9 40.9 %collective-permute-start.5 = (bf16[16,208,128]{2,1,0:T(8,128)(2,1)S(1)}, bf16[16,208,128]{2,1,0:T(8,128)(2,1)}, u32[]{:S(2)}, u32[]{:S(2)}) collective-permute-start(bf16[16,208,128]{2,1,0:T(8,128)(2,1)S(1)} %pad.4.p0), channel_id=1, source_target_pairs={{0,4},{4,0},{1,5},{5,1},{2,6},{6,2},{3,7},{7,3},{8,12},{12,8},{9,1... | collective-permute-start | bytes 2555912 | tf_op jit(solution)/shard_map/ppermute | solution.py:371
  111.9 38.9 %collective-permute-start.6 = (bf16[16,208,128]{2,1,0:T(8,128)(2,1)}, bf16[16,208,128]{2,1,0:T(8,128)(2,1)}, u32[]{:S(2)}, u32[]{:S(2)}) collective-permute-start(bf16[16,208,128]{2,1,0:T(8,128)(2,1)} %collective-permute-done.2.p1), channel_id=1, source_target_pairs={{0,4},{4,0},{1,5},{5,1},{2,6},{6,2},{3,7},{7,3},{8,12},{12,8},{9,1... | collective-permute-start | bytes 2555912 | tf_op jit(solution)/shard_map/ppermute | solution.py:371
  114.2 36.6 %collective-permute-start.7 = (bf16[16,208,128]{2,1,0:T(8,128)(2,1)}, bf16[16,208,128]{2,1,0:T(8,128)(2,1)}, u32[]{:S(2)}, u32[]{:S(2)}) collective-permute-start(bf16[16,208,128]{2,1,0:T(8,128)(2,1)} %collective-permute-done.3.p2), channel_id=1, source_target_pairs={{0,4},{4,0},{1,5},{5,1},{2,6},{6,2},{3,7},{7,3},{8,12},{12,8},{9,1... | collective-permute-start | bytes 2555912 | tf_op jit(solution)/shard_map/ppermute | solution.py:371
  116.3 34.6 %collective-permute-start.8 = (bf16[16,208,128]{2,1,0:T(8,128)(2,1)}, bf16[16,208,128]{2,1,0:T(8,128)(2,1)}, u32[]{:S(2)}, u32[]{:S(2)}) collective-permute-start(bf16[16,208,128]{2,1,0:T(8,128)(2,1)} %collective-permute-done.4.p3), channel_id=1, source_target_pairs={{0,4},{4,0},{1,5},{5,1},{2,6},{6,2},{3,7},{7,3},{8,12},{12,8},{9,1... | collective-permute-start | bytes 2555912 | tf_op jit(solution)/shard_map/ppermute | solution.py:371
  145.4 17.4 %all-to-all-start.4 = ((bf16[8,32,256]{2,1,0:T(8,128)(2,1)}), bf16[8,32,256]{2,1,0:T(8,128)(2,1)S(1)}, u32[]{:S(2)}, u32[]{:S(2)}) async-start(bf16[8,32,256]{2,1,0:T(8,128)(2,1)} %shard_map.203), calls=%async_computation.4 | async-start | bytes 262144 | tf_op jit(solution)/shard_map/all_to_all | solution.py:355
  150.2 11.6 %copy-start.32 = (f32[4]{0:T(128)S(1)}, f32[4]{0:T(128)}, u32[]{:S(2)}) copy-start(f32[4]{0:T(128)} %param.38) | copy-start | bytes 52
  150.8 11.0 %copy-start.4 = (f32[512,256]{1,0:T(8,128)S(1)}, f32[512,256]{1,0:T(8,128)}, u32[]{:S(2)}) copy-start(f32[512,256]{1,0:T(8,128)} %copy-done.3) | copy-start | bytes 1572868
  150.8 11.0 %copy-start.9 = (bf16[512,256]{1,0:T(8,128)(2,1)S(1)}, bf16[512,256]{1,0:T(8,128)(2,1)}, u32[]{:S(2)}) copy-start(bf16[512,256]{1,0:T(8,128)(2,1)} %copy-done.8) | copy-start | bytes 786436
  150.8 11.0 %copy-start.11 = (bf16[4,128,256]{2,1,0:T(8,128)(2,1)S(1)}, bf16[4,128,256]{2,1,0:T(8,128)(2,1)}, u32[]{:S(2)}) copy-start(bf16[4,128,256]{2,1,0:T(8,128)(2,1)} %copy-done.10) | copy-start | bytes 786436
  150.8 11.1 %copy-start.15 = (bf16[512,128]{1,0:T(8,128)(2,1)S(1)}, bf16[512,128]{1,0:T(8,128)(2,1)}, u32[]{:S(2)}) copy-start(bf16[512,128]{1,0:T(8,128)(2,1)} %copy-done.14) | copy-start | bytes 393220
  150.8 0.8 copy-start.28
  151.6 0.7 copy-start.31
  159.0 1.3 copy-start
  160.3 0.8 copy-start.5
  161.1 0.7 copy-start.12
  161.8 1.0 copy-start.30
  161.8 1.6 copy-start.1
  163.4 1.0 copy-start.6
  164.5 0.9 copy-start.13
  167.1 12.3 %collective-permute-start.10 = (bf16[128,2048]{1,0:T(8,128)(2,1)S(1)}, bf16[128,2048]{1,0:T(8,128)(2,1)S(1)}, u32[]{:S(2)}, u32[]{:S(2)}) collective-permute-start(bf16[128,2048]{1,0:T(8,128)(2,1)S(1)} %get-tuple-element.46), channel_id=1, source_target_pairs={{0,1},{4,7},{1,2},{5,4},{2,3},{6,5},{3,0},{7,6},{8,9},{12,15},{9,1... | collective-permute-start | bytes 1572872 | tf_op jit(solution)/shard_map/ppermute | solution.py:367
  173.2 11.9 %collective-permute-start.9 = (bf16[128,2048]{1,0:T(8,128)(2,1)S(1)}, bf16[128,2048]{1,0:T(8,128)(2,1)S(1)}, u32[]{:S(2)}, u32[]{:S(2)}) collective-permute-start(bf16[128,2048]{1,0:T(8,128)(2,1)S(1)} %get-tuple-element.44), channel_id=1, source_target_pairs={{0,3},{4,5},{1,0},{5,6},{2,1},{6,7},{3,2},{7,4},{8,11},{12,13},{9,... | collective-permute-start | bytes 1572872 | tf_op jit(solution)/shard_map/ppermute | solution.py:367
  179.5 12.9 %collective-permute-start.11 = (bf16[128,2048]{1,0:T(8,128)(2,1)S(1)}, bf16[128,2048]{1,0:T(8,128)(2,1)S(1)}, u32[]{:S(2)}, u32[]{:S(2)}) collective-permute-start(bf16[128,2048]{1,0:T(8,128)(2,1)S(1)} %shard_map.208), channel_id=1, source_target_pairs={{0,1},{4,7},{1,2},{5,4},{2,3},{6,5},{3,0},{7,6},{8,9},{12,15},{9,1... | collective-permute-start | bytes 1572872 | tf_op jit(solution)/shard_map/ppermute | solution.py:367

commit v5 on v4

--- a/solution.py
+++ b/solution.py
@@ -17,20 +17,36 @@
 BF16 = jnp.bfloat16
 
 
-def call(body, outs, args, scratch=(), mib=8):
+def call(body, outs, args, scratch=(), mib=8, far_in=(), far_out=()):
     vmem = pl.BlockSpec(memory_space=pltpu.VMEM)
+    hbm = pl.BlockSpec(memory_space=pltpu.HBM)
+    many = isinstance(outs, tuple)
+    args = [
+        pltpu.with_memory_space_constraint(a, pltpu.HBM) if i in far_in else a
+        for i, a in enumerate(args)
+    ]
     return pl.pallas_call(
         body,
         out_shape=outs,
-        in_specs=[vmem for _ in args],
-        out_specs=jax.tree.map(lambda _: vmem, outs),
+        in_specs=[hbm if i in far_in else vmem for i in range(len(args))],
+        out_specs=tuple(hbm if i in far_out else vmem for i in range(len(outs))) if many else vmem,
         scratch_shapes=list(scratch),
-        compiler_params=pltpu.CompilerParams(vmem_limit_bytes=mib * 2**20),
+        compiler_params=pltpu.CompilerParams(
+            vmem_limit_bytes=None if mib is None else mib * 2**20
+        ),
     )(*args)
 
 
 def shape(dims, kind):
     return jax.ShapeDtypeStruct(dims, kind)
+
+
+def on_chip(dims, kind):
+    return pltpu.VMEM(dims, kind)
+
+
+def main_memory(dims, kind):
+    return pltpu.HBM(dims, kind)
 
 
 def dot(a, b):
@@ -78,17 +94,44 @@
     ]
 
 
-def ring_pieces(parts):
+def ring_places():
     x, c = lax.axis_index("x"), lax.axis_index("c")
     return [
-        (
-            lambda z, lo, n, r=parts[4 * side + i]: r[z, lo : lo + n, :],
-            (x + by) % 4,
-            at,
+        ((x + by) % 4, at)
+        for at in (c, 1 - c)
+        for by in (0, 3 - 2 * at, 1 + 2 * at, 2)
+    ]
+
+
+def ring_copies(parts, which, target, lo, count, sems):
+    places = ring_places()
+    copies = []
+    for i in which:
+        x, at = places[i]
+        copies.append(
+            pltpu.make_async_copy(
+                parts[i].at[:, lo : lo + count, :], target.at[:, x, at], sems.at[i]
+            )
         )
-        for side, at in ((0, c), (1, 1 - c))
-        for i, by in enumerate((0, 3 - 2 * at, 1 + 2 * at, 2))
+    for copy in copies:
+        copy.start()
+    return copies
+
+
+def ring_pieces(parts, which):
+    places = ring_places()
+    return [
+        (lambda z, lo, n, r=parts[i]: r[z, lo : lo + n, :], *places[i]) for i in which
     ]
+
+
+FAR = (0, 1, 2, 4)
+NEAR = (3, 5, 6, 7)
+
+
+def wait_for(copies):
+    for copy in copies:
+        copy.wait()
 
 
 def block(whole, q):
@@ -99,8 +142,7 @@
     return jnp.concatenate([block(whole, q) for q in range(lo, lo + count)], axis=1)
 
 
-def taps(ref, weights, cols, count):
-    w = weights[...].astype(F32)
+def taps(ref, w, cols, count):
     out = None
     for k in range(count):
         part = w[k : k + 1, :] * ref[pl.ds(HALO - count + 1 + k, ROWS), cols]
@@ -108,7 +150,11 @@
     return out
 
 
-def prep_body(tok, gain, w0, w1, w2, w3, w4, w5, w6, w7, w8, copied, own, left):
+def prep_body(
+    tok, gain, w0, w1, w2, w3, w4, w5, w6, w7, w8,
+    gated_taps, input_taps, write_taps, read_taps, scale, direct, bias, rate,
+    copied, own, left, small,
+):
     q = 0
     for w in (w0, w1, w2, w3, w4, w5, w6, w7, w8):
         for k in range(w.shape[1] // 128):
@@ -120,7 +166,18 @@
                 f = v.astype(F32)
                 left[...] = jnp.concatenate([f[14:15], f[15:16]], axis=1)
             q += 1
-    g = gain[...].astype(F32)
+    small[...] = jnp.zeros(small.shape, F32)
+    small[0:3, :] = gated_taps[...].astype(F32)
+    small[3:7, :] = input_taps[...].astype(F32)
+    small[7:11, 0:128] = write_taps[...].astype(F32)
+    small[11:15, 0:128] = read_taps[...].astype(F32)
+    f = scale[...].astype(F32)
+    small[15:16, :] = jnp.concatenate([f[0:1], f[1:2]], axis=1)
+    small[16:17, 0:4] = direct[...]
+    small[17:18, 0:4] = bias[...]
+    small[18:19, 0:4] = rate[...]
+    f = gain[...].astype(F32)
+    g = jnp.concatenate([f[i : i + 1] for i in range(16)], axis=1)
 
     def some(i, _):
         rows = pl.ds(pl.multiple_of(i * 16, 16), 16)
@@ -134,16 +191,30 @@
     lax.fori_loop(0, 8, some, 0, unroll=2)
 
 
-def cum_body(tok, ws, bias, rate, spikes, dt, cum, cum_t, square):
+def cut_body(column, first, ring):
+    for z in range(16):
+        v = column[z, 0:48, :]
+        for x in range(4):
+            first[x, z] = v
+        ring[z, 0:192, :] = column[z, 48:240, :]
+        v = column[z, 240:254, :].astype(F32)
+        ring[z, 192:208, :] = jnp.concatenate([v, v[0:2]], axis=0).astype(BF16)
+
+
+def cum_body(tok, ws, small, spikes, dt, cum, cum_t, edge, square):
+    edge[...] = tok[3, 112:128, :]
     n = tok[...].reshape(ROWS, 2048)
-    raw = dot_nt(ws[...], n) + bias[...]
+    square[...] = jnp.zeros(square.shape, F32)
+    square[0, 0:2, :] = small[17:19, 0:128]
+    columns = square[0].T[0:4, :]
+    raw = dot_nt(ws[...], n) + columns[:, 0:1]
     step = jnp.maximum(raw, 0.0) + jnp.log1p(jnp.exp(-jnp.abs(raw)))
-    logs = -step * jnp.exp(rate[...]) + spikes[...]
+    logs = -step * jnp.exp(columns[:, 1:2]) + spikes[...]
+    square[0] = jnp.zeros((BLK, BLK), F32)
     r = lax.broadcasted_iota(jnp.int32, (BLK, BLK), 0)
     s = lax.broadcasted_iota(jnp.int32, (BLK, BLK), 1)
     upper = jnp.where(r <= s, 1.0, 0.0).astype(F32)
     carry = jnp.zeros((4, 1), F32)
-    square[...] = jnp.zeros(square.shape, F32)
     for b in range(NB):
         rows = slice(b * BLK, (b + 1) * BLK)
         part = (
@@ -163,18 +234,29 @@
         carry = part[:, BLK - 1 : BLK]
 
 
+def fetches(tok, normed, sem):
+    copies = [
+        pltpu.make_async_copy(tok.at[y], normed.at[HALO + 128 * y : HALO + 128 * (y + 1)], sem.at[y])
+        for y in range(4)
+    ]
+    for copy in copies:
+        copy.start()
+    return copies
+
+
 def first_body(
-    tok, halo, own, other, dt, cum, input_taps, write_taps,
+    tok, halo, own, other, dt, cum, small,
     weighted, seq_input, seq_write, local, pieces,
-    whole, normed, fields,
+    whole, normed, fields, sem,
 ):
+    fetch = fetches(tok, normed, sem)
+    normed[0:HALO, :] = halo[...]
     lay_out(first_pieces(own, other), ((whole, 0, 48),))
-    normed[0:HALO, :] = halo[...]
-    normed[HALO:, :] = tok[...].reshape(ROWS, 2048)
+    wait_for(fetch)
     projected = dot(normed[...], blocks(whole, 0, 3))
     fields[...] = projected.astype(BF16).astype(F32)
-    xin = silu(taps(fields, input_taps, slice(0, 256), 4))
-    write = silu(taps(fields, write_taps, slice(256, 384), 4))
+    xin = silu(taps(fields, small[3:7, :], slice(0, 256), 4))
+    write = silu(taps(fields, small[7:11, 0:128], slice(256, 384), 4))
     seq_input[...] = xin
     seq_write[...] = write.astype(BF16)
     scaled = xin * per_head(dt[:, 0:128])
@@ -244,32 +326,39 @@
 
 
 def rest_body(
-    tok, halo, p0, p1, p2, p3, p4, p5, p6, p7, read_taps, gated_taps,
+    tok, halo, p0, p1, p2, p3, p4, p5, p6, p7, small,
     read_out, gate, mixer, wide,
-    whole, normed, fields,
+    whole, more, normed, fields, sem, sems,
 ):
-    parts = ring_pieces((p0, p1, p2, p3, p4, p5, p6, p7))
-    lay_out(parts, ((whole, 0, 144), (wide, 144, 64)))
+    parts = (p0, p1, p2, p3, p4, p5, p6, p7)
+    fetch = fetches(tok, normed, sem)
+    one = ring_copies(parts, FAR, whole, 0, 48, sems.at[0])
+    two = ring_copies(parts, FAR, more, 48, 96, sems.at[1])
+    store = ring_copies(parts, range(8), wide, 144, 64, sems.at[2])
     normed[0:HALO, :] = halo[...]
-    normed[HALO:, :] = tok[...].reshape(ROWS, 2048)
+    lay_out(ring_pieces(parts, NEAR), ((whole, 0, 48), (more, 48, 96)))
+    wait_for(fetch)
+    wait_for(one)
     n = normed[...]
 
-    def projected(lo, count):
-        return dot(n, blocks(whole, lo, count)).astype(BF16).astype(F32)
-
-    fields[:, 0:128] = projected(0, 1)
-    read_out[...] = silu(taps(fields, read_taps, slice(0, 128), 4)).astype(BF16)
-    gate[...] = silu(projected(1, 2)[HALO:])
-    inner = projected(5, 2)
-    fields[...] = inner * projected(7, 2)
-    outer = projected(3, 2)[HALO:]
-    mixer[...] = (outer * taps(fields, gated_taps, slice(0, 256), 3)).astype(BF16)
+    def projected(ref, lo, count):
+        return dot(n, blocks(ref, lo, count)).astype(BF16).astype(F32)
+
+    fields[:, 0:128] = projected(whole, 0, 1)
+    read_out[...] = silu(taps(fields, small[11:15, 0:128], slice(0, 128), 4)).astype(BF16)
+    gate[...] = silu(projected(whole, 1, 2)[HALO:])
+    wait_for(two)
+    inner = projected(more, 2, 2)
+    fields[...] = inner * projected(more, 4, 2)
+    outer = projected(more, 0, 2)[HALO:]
+    mixer[...] = (outer * taps(fields, small[0:3, :], slice(0, 256), 3)).astype(BF16)
+    wait_for(store)
 
 
 def within_body(
-    read, weighted, seq_input, seq_write, local, cum, cum_t, direct, partly
+    read, weighted, seq_input, seq_write, local, cum, cum_t, small, partly
 ):
-    weight = per_head(direct[...])
+    weight = per_head(small[16:17, 0:128])
     r = lax.broadcasted_iota(jnp.int32, (BLK, BLK), 0)
     s = lax.broadcasted_iota(jnp.int32, (BLK, BLK), 1)
     causal = r >= s
@@ -295,7 +384,7 @@
         partly[rows, :] = within + from_local + weight * seq_input[rows, :]
 
 
-def patch(wide, arriving, fixed):
+def patch(wide, arriving):
     row = lax.broadcasted_iota(jnp.int32, (16, 128), 0)
     for j in range(8):
         lefts = arriving[j, 16:32, :].astype(F32)
@@ -304,21 +393,23 @@
             for i in range(2):
                 v = lefts[z : z + 1, 128 * i : 128 * (i + 1)]
                 tile = jnp.where(row == 14 + i, jnp.broadcast_to(v, (16, 128)), tile)
-            fixed[z, j // 2, j % 2] = tile.astype(BF16)
-
-
-def project_out(act, at, wide, fixed, out):
+            wide[z, j // 2, j % 2, 48:64, :] = tile.astype(BF16)
+
+
+def project_out(act, at, wide, out):
     a = act[pl.ds(pl.multiple_of(at * 128, 128), 128), :]
     for q in range(4):
         zs = slice(4 * q, 4 * (q + 1))
-        w = [wide[zs, :, :, 16 * k : 16 * (k + 1), :].reshape(512, 128) for k in range(3)]
-        w = jnp.concatenate([*w, fixed[zs].reshape(512, 128)], axis=1)
+        w = [wide[zs, :, :, 16 * k : 16 * (k + 1), :].reshape(512, 128) for k in range(4)]
+        w = jnp.concatenate(w, axis=1)
         out[:, 512 * q : 512 * (q + 1)] = dot_nt(a, w).astype(out.dtype)
 
 
 def tail_body(
-    arriving, partly, read, gate, cum, mixer, scale, wide, act, far, fixed
+    arriving, partly, read, gate, cum, mixer, small, stored, act, far, wide, sem
 ):
+    fetch = pltpu.make_async_copy(stored, wide, sem)
+    fetch.start()
     act[:, 0:256] = mixer[...]
     state = jnp.concatenate([arriving[j, 0:16, :] for j in range(8)], axis=0)
     head = partly[...] + dot(read[...], state) * per_head(jnp.exp(cum[...]))
@@ -330,16 +421,17 @@
     high = square.astype(BF16)
     rest = (square - high.astype(F32)).astype(BF16)
     mean = dot(high, same) + dot(rest, same)
-    act[:, 256:512] = (gated * lax.rsqrt(mean + EPS) * scale[...].astype(F32)).astype(BF16)
-    patch(wide, arriving, fixed)
-    project_out(act, (lax.axis_index("tp") + 2) % 4, wide, fixed, far)
-
-
-def near_body(act, wide, fixed, beside, near, mine):
+    act[:, 256:512] = (gated * lax.rsqrt(mean + EPS) * small[15:16, :]).astype(BF16)
+    fetch.wait()
+    patch(wide, arriving)
+    project_out(act, (lax.axis_index("tp") + 2) % 4, wide, far)
+
+
+def near_body(act, wide, beside, near, mine):
     y, c = lax.axis_index("tp"), lax.axis_index("c")
-    project_out(act, (y + 3 + 2 * c) % 4, wide, fixed, beside)
-    project_out(act, (y + 1 + 2 * c) % 4, wide, fixed, near)
-    project_out(act, y, wide, fixed, mine)
+    project_out(act, (y + 3 + 2 * c) % 4, wide, beside)
+    project_out(act, (y + 1 + 2 * c) % 4, wide, near)
+    project_out(act, y, wide, mine)
 
 
 def add_body(near, got, out):
@@ -353,11 +445,6 @@
 
 def exchanged(tiles, axis):
     return lax.all_to_all(tiles, axis, 0, 0, tiled=True)
-
-
-def copies(shard, axis):
-    n = lax.axis_size(axis)
-    return exchanged(jnp.broadcast_to(shard[None], (n, *shard.shape)), axis)
 
 
 def two_way(shard, axis, toward):
@@ -394,12 +481,17 @@
     conv_output_weight,
     state_output_weight,
 ):
-    copied, own, left = call(
+    copied, own, left, small = call(
         prep_body,
-        (shape((4, 128, 2048), BF16), shape((254, 128), BF16), shape((1, 256), F32)),
+        (
+            shape((4, 128, 2048), BF16),
+            shape((254, 128), BF16),
+            shape((1, 256), F32),
+            shape((24, 256), F32),
+        ),
         (
             tokens,
-            input_norm_scale[None],
+            input_norm_scale.reshape(16, 128),
             state_input_weight,
             write_key_weight,
             read_key_weight,
@@ -409,47 +501,61 @@
             value_weight_matrix,
             conv_output_weight.T,
             state_output_weight.T,
-        ),
+            gated_conv_weight,
+            input_conv_weight,
+            write_conv_weight,
+            read_conv_weight,
+            head_norm_scale.reshape(2, 128),
+            direct_path_weight[None],
+            step_size_bias[None],
+            log_decay_rate[None],
+        ),
+        mib=None,
     )
     tok = exchanged(copied, "tp")
     column = lax.all_gather(own, "z", axis=0, tiled=False)
-    first = copies(column[:, :48], "x")
+    first, ring = call(
+        cut_body,
+        (main_memory((4, 16, 48, 128), BF16), main_memory((16, 208, 128), BF16)),
+        (column,),
+    )
+    first = exchanged(first, "x")
     first_other = swapped(first)
-    ring = [jnp.pad(column[:, 48:], ((0, 0), (0, 2), (0, 0)))]
+    ring = [ring]
     ring.append(two_way(ring[0], "x", 1))
     ring.append(two_way(ring[0], "x", -1))
     ring.append(two_way(ring[1], "x", 1))
     ring += [swapped(part) for part in ring]
-    halo = lax.ppermute(tok[3, 112:, :], SP, [(i, i + 1) for i in range(127)])
-
-    dt, cum, cum_t = call(
+    dt, cum, cum_t, edge = call(
         cum_body,
-        (shape((ROWS, 128), F32), shape((ROWS, 128), F32), shape((8, ROWS), F32)),
         (
-            tok,
-            step_size_weight.T,
-            step_size_bias[:, None],
-            log_decay_rate[:, None],
-            decay_spikes,
-        ),
+            shape((ROWS, 128), F32),
+            shape((ROWS, 128), F32),
+            shape((8, ROWS), F32),
+            shape((HALO, 2048), BF16),
+        ),
+        (tok, step_size_weight.T, small, decay_spikes),
         scratch=(pltpu.VMEM((2, BLK, BLK), F32),),
     )
+    halo = lax.ppermute(edge, SP, [(i, i + 1) for i in range(127)])
     weighted, seq_input, seq_write, local, pieces = call(
         first_body,
         (
-            shape((ROWS, 256), BF16),
-            shape((ROWS, 256), F32),
-            shape((ROWS, 128), BF16),
-            shape((NB, 128, 256), BF16),
-            shape((8, 24, 256), BF16),
-        ),
-        (tok, halo, first, first_other, dt, cum, input_conv_weight, write_conv_weight),
+            main_memory((ROWS, 256), BF16),
+            main_memory((ROWS, 256), F32),
+            main_memory((ROWS, 128), BF16),
+            main_memory((NB, 128, 256), BF16),
+            main_memory((8, 24, 256), BF16),
+        ),
+        (tok, halo, first, first_other, dt, cum, small),
         (
             pltpu.VMEM((16, 4, 2, 48, 128), BF16),
             pltpu.VMEM((HALO + ROWS, 2048), BF16),
             pltpu.VMEM((HALO + ROWS, 384), F32),
+            pltpu.SemaphoreType.DMA((4,)),
         ),
         mib=16,
+        far_in=(0,),
     )
     got = exchanged(pieces, ("x", "c"))
     send = call(plane_body, shape((16, 24, 256), BF16), (got, left))
@@ -460,39 +566,44 @@
     read, gate, mixer, wide = call(
         rest_body,
         (
-            shape((ROWS, 128), BF16),
-            shape((ROWS, 256), F32),
-            shape((ROWS, 256), BF16),
-            shape((16, 4, 2, 64, 128), BF16),
-        ),
-        (tok, halo, *ring, read_conv_weight, gated_conv_weight),
+            on_chip((ROWS, 128), BF16),
+            on_chip((ROWS, 256), F32),
+            on_chip((ROWS, 256), BF16),
+            main_memory((16, 4, 2, 64, 128), BF16),
+        ),
+        (tok, halo, *ring, small),
         scratch=(
-            pltpu.VMEM((16, 4, 2, 144, 128), BF16),
+            pltpu.VMEM((16, 4, 2, 48, 128), BF16),
+            pltpu.VMEM((16, 4, 2, 96, 128), BF16),
             pltpu.VMEM((HALO + ROWS, 2048), BF16),
             pltpu.VMEM((HALO + ROWS, 256), F32),
-        ),
-        mib=28,
+            pltpu.SemaphoreType.DMA((4,)),
+            pltpu.SemaphoreType.DMA((3, 8)),
+        ),
+        mib=20,
+        far_in=(0, *(2 + i for i in FAR)),
+        far_out=(3,),
     )
     partly = call(
         within_body,
         shape((ROWS, 256), F32),
-        (read, weighted, seq_input, seq_write, local, cum, cum_t, direct_path_weight[None]),
-    )
-    act, far, fixed = call(
+        (read, weighted, seq_input, seq_write, local, cum, cum_t, small),
+    )
+    act, far, wide = call(
         tail_body,
         (
-            shape((ROWS, 512), BF16),
+            on_chip((ROWS, 512), BF16),
             shape((128, 2048), BF16),
-            shape((16, 4, 2, 16, 128), BF16),
-        ),
-        (arriving, partly, read, gate, cum, mixer, head_norm_scale[None], wide),
+            on_chip((16, 4, 2, 64, 128), BF16),
+        ),
+        (arriving, partly, read, gate, cum, mixer, small, wide),
+        scratch=(pltpu.SemaphoreType.DMA,),
         mib=16,
+        far_in=(7,),
     )
     got_far = two_way(far, "tp", 1)
     block_ = shape((128, 2048), BF16)
-    beside, near, mine = call(
-        near_body, (block_, block_, block_), (act, wide, fixed), mib=12
-    )
+    beside, near, mine = call(near_body, (block_, block_, block_), (act, wide), mib=12)
     got_beside = two_way(beside, "tp", -1)
     both = call(add_body, shape((128, 2048), BF16), (near, got_far))
     got_near = two_way(both, "tp", 1)

time: 195 us -> 212 us (1.087)
  Pallas kernels: 19.7 us -> 53.5 us
  local copies, waits for them, and re-layouts: 20 us -> 1.62 us
    pallas_call x11 -> x12, Pallas kernels: 19.7 us -> 53.5 us  [call(): pl.pallas_call(body, out_shape=outs, in_specs=[hbm if i in far_in else vm...]
    unnamed x72 -> x26, local copies, waits for them, and re-layouts: 18.3 us -> 1.62 us
  transfers between devices with their start and end apart: 15 -> 15, of which waited for: 5 -> 5; matrix products, arithmetic and copies ran while one was open for 0% -> 0% of each run, Pallas kernels for 9% -> 22%
where the time goes in v5:
time: 212 us; the launch traced here: 211 us
  blocking collectives  78.6 us (37%)
  Pallas kernels  53.5 us (25%)
  starting transfers between devices  47.8 us (23%)
  waiting for transfers between devices  29 us (14%)
    pallas_call x12, Pallas kernels, call(): pl.pallas_call(body, out_shape=outs, in_specs=[hbm if i in far_in else vm...  53.5 us
    all_gather x1, blocking collectives, per_device(): column = lax.all_gather(own, 'z', axis=0, tiled=False)  39.7 us
    all_to_all x2, blocking collectives, exchanged(): return lax.all_to_all(tiles, axis, 0, 0, tiled=True)  38.9 us
    all_to_all x3, starting transfers between devices, exchanged(): return lax.all_to_all(tiles, axis, 0, 0, tiled=True)  16.6 us
    ppermute x3, waiting for transfers between devices, two_way(): lax.ppermute(shard, ('x', 'c'), [(2 * i + c, 2 * j + c) for i, c, j in st...  12.6 us
    ppermute x3, waiting for transfers between devices, two_way(): lax.ppermute(shard, ('c', 'tp'), [(4 * c + i, 4 * c + j) for i, c, j in s...  12.1 us
    ppermute x3, starting transfers between devices, two_way(): lax.ppermute(shard, ('c', 'tp'), [(4 * c + i, 4 * c + j) for i, c, j in s...  11 us
    ppermute x5, starting transfers between devices, swapped(): return lax.ppermute(shard, 'c', [(0, 1), (1, 0)])  10.6 us
  transfers between devices with their start and end apart: 15, of which 5 were waited for; matrix products, arithmetic and copies ran while one was open for 0% of the time, Pallas kernels for 22%

profile of v5, /device:TPU:34, one launch (start us, length us, event | category | flops | bytes accessed | tf_op | source)
XLA Modules:
  0.0 210.8 jit_solution(1936858494652012341)
XLA Ops:
  0.0 3.2 %shard_map.199 = (bf16[4,128,2048]{2,1,0:T(8,128)(2,1)}, bf16[254,128]{1,0:T(8,128)(2,1)}, f32[1,256]{1,0:T(1,128)}, f32[24,256]{1,0:T(8,128)}) custom-call(bf16[128,2048]{1,0:T(8,128)(2,1)} %tok.1, bf16[16,128]{1,0:T(8,128)(2,1)} %bitcast.13, bf16[16,256]{1,0:T(8,128)(2,1)} %w0.1, bf16[16,128]{1,0:T(8,128)(2,1)} %w1.1, bf16[16,128]{1,0:T(8,128)(2,1)} %w2.1, ...), custom_call_target="tpu_custom_call" | custom-call | tf_op jit(solution)/shard_map/pallas_call | solution.py:28
  3.2 39.7 %all-gather.1.column = bf16[16,254,128]{2,1,0:T(8,128)(2,1)S(1)} all-gather(bf16[1,254,128]{2,1,0:T(8,128)(2,1)} %bitcast.10), channel_id=2, replica_groups=mesh['z'=16,'x'=4,'c'=2,'tp'=4] {'z'}, dimensions={0}, use_global_device_ids=true | all-gather | bytes 1105408 | tf_op jit(solution)/shard_map/all_gather | solution.py:516
  42.9 1.4 shard_map.201
  44.2 12.9 %all_to_all.25.own = bf16[4,16,48,128]{3,2,1,0:T(8,128)(2,1)S(1)} all-to-all(bf16[4,16,48,128]{3,2,1,0:T(8,128)(2,1)} %get-tuple-element.34), channel_id=1, replica_groups=mesh['z'=16,'x'=4,'c'=2,'tp'=4] {'x'}, dimensions={0} | all-to-all | bytes 1572864 | tf_op jit(solution)/shard_map/all_to_all | solution.py:447
  57.1 0.0 copy-start.1
  57.1 0.0 copy-start.10
  57.1 0.0 copy-start.11
  57.1 4.6 %all-to-all-start = ((bf16[4,128,2048]{2,1,0:T(8,128)(2,1)}), bf16[4,128,2048]{2,1,0:T(8,128)(2,1)S(1)}, u32[]{:S(2)}, u32[]{:S(2)}) async-start(bf16[4,128,2048]{2,1,0:T(8,128)(2,1)} %get-tuple-element.30), calls=%async_computation | async-start | bytes 4194304 | tf_op jit(solution)/shard_map/all_to_all | solution.py:447
  61.7 2.1 %collective-permute-start.2 = (bf16[16,208,128]{2,1,0:T(8,128)(2,1)}, bf16[16,208,128]{2,1,0:T(8,128)(2,1)}, u32[]{:S(2)}, u32[]{:S(2)}) collective-permute-start(bf16[16,208,128]{2,1,0:T(8,128)(2,1)} %get-tuple-element.39.p0), channel_id=1, source_target_pairs={{0,8},{4,28},{8,16},{12,4},{16,24},{20,12},{24,0},{28,20},{1,9},{5... | collective-permute-start | bytes 2555912 | tf_op jit(solution)/shard_map/ppermute | solution.py:453
  63.8 1.9 collective-permute-start.1
  65.7 3.7 %collective-permute-start.3 = (bf16[16,208,128]{2,1,0:T(8,128)(2,1)}, bf16[16,208,128]{2,1,0:T(8,128)(2,1)}, u32[]{:S(2)}, u32[]{:S(2)}) collective-permute-start(bf16[16,208,128]{2,1,0:T(8,128)(2,1)} %get-tuple-element.39.p0), channel_id=1, source_target_pairs={{0,24},{4,12},{8,0},{12,20},{16,8},{20,28},{24,16},{28,4},{1,25},{... | collective-permute-start | bytes 2555912 | tf_op jit(solution)/shard_map/ppermute | solution.py:453
  69.5 12.6 %collective-permute-done.2.p1 = bf16[16,208,128]{2,1,0:T(8,128)(2,1)} collective-permute-done((bf16[16,208,128]{2,1,0:T(8,128)(2,1)}, bf16[16,208,128]{2,1,0:T(8,128)(2,1)}, u32[]{:S(2)}, u32[]{:S(2)}) %collective-permute-start.2) | collective-permute-done | bytes 852000 | tf_op jit(solution)/shard_map/ppermute | solution.py:453
  82.0 1.9 collective-permute-start.4
  84.0 0.0 all-to-all-done.tok
  84.0 0.0 copy-start
  84.0 0.0 copy-done.1
  84.0 0.0 copy-done.10
  84.0 0.0 copy-done.11
  84.0 1.2 shard_map.200
  85.2 1.9 collective-permute-start
  87.1 0.0 collective-permute-done.1.other
  87.2 4.3 %collective-permute-done.halo = bf16[16,2048]{1,0:T(8,128)(2,1)S(1)} collective-permute-done((bf16[16,2048]{1,0:T(8,128)(2,1)S(1)}, bf16[16,2048]{1,0:T(8,128)(2,1)S(1)}, u32[]{:S(2)}, u32[]{:S(2)}) %collective-permute-start) | collective-permute-done | bytes 65568 | tf_op jit(solution)/shard_map/ppermute | solution.py:540
  91.5 0.0 copy-done
  91.5 0.0 copy-start.12
  91.5 5.8 %shard_map.202 = (bf16[512,256]{1,0:T(8,128)(2,1)}, f32[512,256]{1,0:T(8,128)}, bf16[512,128]{1,0:T(8,128)(2,1)}, bf16[4,128,256]{2,1,0:T(8,128)(2,1)}, bf16[8,24,256]{2,1,0:T(8,128)(2,1)}) custom-call(bf16[4,128,2048]{2,1,0:T(8,128)(2,1)} %copy-done, bf16[16,2048]{1,0:T(8,128)(2,1)S(1)} %collective-permute-done.halo, ...), custom_call_target="tpu_custom_call" | custom-call | tf_op jit(solution)/shard_map/pallas_call | solution.py:28
  97.3 7.2 %all-to-all-start.2 = ((bf16[8,24,256]{2,1,0:T(8,128)(2,1)}), bf16[8,24,256]{2,1,0:T(8,128)(2,1)S(1)}, u32[]{:S(2)}, u32[]{:S(2)}) async-start(bf16[8,24,256]{2,1,0:T(8,128)(2,1)} %get-tuple-element.37), calls=%async_computation.2 | async-start | bytes 196608 | tf_op jit(solution)/shard_map/all_to_all | solution.py:447
  104.5 2.0 collective-permute-start.5
  106.6 2.3 %collective-permute-start.6 = (bf16[16,208,128]{2,1,0:T(8,128)(2,1)}, bf16[16,208,128]{2,1,0:T(8,128)(2,1)S(1)}, u32[]{:S(2)}, u32[]{:S(2)}) collective-permute-start(bf16[16,208,128]{2,1,0:T(8,128)(2,1)} %collective-permute-done.2.p1), channel_id=1, source_target_pairs={{0,4},{4,0},{1,5},{5,1},{2,6},{6,2},{3,7},{7,3},{8,12},{12,8},{9,1... | collective-permute-start | bytes 2555912 | tf_op jit(solution)/shard_map/ppermute | solution.py:458
  108.9 0.0 collective-permute-done.3.p2
  108.9 2.0 collective-permute-start.7
  110.9 0.0 collective-permute-done.4.p3
  110.9 2.3 %collective-permute-start.8 = (bf16[16,208,128]{2,1,0:T(8,128)(2,1)}, bf16[16,208,128]{2,1,0:T(8,128)(2,1)S(1)}, u32[]{:S(2)}, u32[]{:S(2)}) collective-permute-start(bf16[16,208,128]{2,1,0:T(8,128)(2,1)} %collective-permute-done.4.p3), channel_id=1, source_target_pairs={{0,4},{4,0},{1,5},{5,1},{2,6},{6,2},{3,7},{7,3},{8,12},{12,8},{9,1... | collective-permute-start | bytes 2555912 | tf_op jit(solution)/shard_map/ppermute | solution.py:458
  113.2 0.0 all-to-all-done.2.got
  113.2 0.0 copy-done.12
  113.3 26.0 %all_to_all.26.planes = bf16[16,24,256]{2,1,0:T(8,128)(2,1)S(1)} all-to-all(bf16[16,24,256]{2,1,0:T(8,128)(2,1)S(1)} %shard_map.203), channel_id=1, replica_groups=mesh['z'=16,'x'=4,'c'=2,'tp'=4] {'z'}, dimensions={0} | all-to-all | bytes 393216 | tf_op jit(solution)/shard_map/all_to_all | solution.py:447
  139.3 0.8 shard_map.204
  140.1 4.8 %all-to-all-start.4 = ((bf16[8,32,256]{2,1,0:T(8,128)(2,1)}), bf16[8,32,256]{2,1,0:T(8,128)(2,1)S(1)}, u32[]{:S(2)}, u32[]{:S(2)}) async-start(bf16[8,32,256]{2,1,0:T(8,128)(2,1)} %shard_map.204), calls=%async_computation.4 | async-start | bytes 262144 | tf_op jit(solution)/shard_map/all_to_all | solution.py:447
  144.9 0.0 copy-start.9
  144.9 0.0 collective-permute-done.5.p4
  144.9 0.0 collective-permute-done.6.p5
  144.9 0.0 collective-permute-done.7.p6
  145.0 0.0 collective-permute-done.8.p7
  145.0 34.4 %shard_map.205 = (bf16[512,128]{1,0:T(8,128)(2,1)S(1)}, f32[512,256]{1,0:T(8,128)S(1)}, bf16[512,256]{1,0:T(8,128)(2,1)S(1)}, bf16[16,4,2,64,128]{4,3,2,1,0:T(8,128)(2,1)}) custom-call(bf16[4,128,2048]{2,1,0:T(8,128)(2,1)} %copy-done, bf16[16,2048]{1,0:T(8,128)(2,1)S(1)} %collective-permute-done.halo, bf16[16,208,128]{2,1,0:T(8,128)(2,1)} %get-tuple-element.39.p0, ...), custom_call_target="tpu_custom_call" | custom-call | tf_op jit(solution)/shard_map/pallas_call | solution.py:28
  179.3 0.0 copy-start.2
  179.4 0.8 copy-done.2
  180.1 0.7 copy-done.7
  180.8 0.0 copy-done.4
  180.8 0.0 copy-done.5
  180.8 0.0 copy-done.6
  180.9 0.0 copy-done.9
  180.9 1.0 shard_map.206.partly
  181.8 0.0 all-to-all-done.4.arriving
  181.8 0.0 copy-done.3
  181.9 0.1 copy-done.8
  181.9 2.6 %shard_map.207 = (bf16[512,512]{1,0:T(8,128)(2,1)S(1)}, bf16[128,2048]{1,0:T(8,128)(2,1)S(1)}, bf16[16,4,2,64,128]{4,3,2,1,0:T(8,128)(2,1)S(1)}) custom-call(bf16[8,32,256]{2,1,0:T(8,128)(2,1)S(1)} %all-to-all-done.4.arriving, f32[512,256]{1,0:T(8,128)S(1)} %shard_map.206.partly, bf16[512,128]{1,0:T(8,128)(2,1)S(1)} %get-tuple-element.40.read, ...), custom_call_target="tpu_custom_call" | custom-call | tf_op jit(solution)/shard_map/pallas_call | solution.py:28
  184.5 3.9 %collective-permute-start.10 = (bf16[128,2048]{1,0:T(8,128)(2,1)S(1)}, bf16[128,2048]{1,0:T(8,128)(2,1)S(1)}, u32[]{:S(2)}, u32[]{:S(2)}) collective-permute-start(bf16[128,2048]{1,0:T(8,128)(2,1)S(1)} %get-tuple-element.54), channel_id=1, source_target_pairs={{0,1},{4,7},{1,2},{5,4},{2,3},{6,5},{3,0},{7,6},{8,9},{12,15},{9,1... | collective-permute-start | bytes 1572872 | tf_op jit(solution)/shard_map/ppermute | solution.py:454
  188.5 2.1 %shard_map.208 = (bf16[128,2048]{1,0:T(8,128)(2,1)S(1)}, bf16[128,2048]{1,0:T(8,128)(2,1)S(1)}, bf16[128,2048]{1,0:T(8,128)(2,1)S(1)}) custom-call(bf16[512,512]{1,0:T(8,128)(2,1)S(1)} %get-tuple-element.49.act, bf16[16,4,2,64,128]{4,3,2,1,0:T(8,128)(2,1)S(1)} %get-tuple-element.50.wide), custom_call_target="tpu_custom_call" | custom-call | tf_op jit(solution)/shard_map/pallas_call | solution.py:28
  190.6 3.1 %collective-permute-start.9 = (bf16[128,2048]{1,0:T(8,128)(2,1)S(1)}, bf16[128,2048]{1,0:T(8,128)(2,1)S(1)}, u32[]{:S(2)}, u32[]{:S(2)}) collective-permute-start(bf16[128,2048]{1,0:T(8,128)(2,1)S(1)} %get-tuple-element.52), channel_id=1, source_target_pairs={{0,3},{4,5},{1,0},{5,6},{2,1},{6,7},{3,2},{7,4},{8,11},{12,13},{9,... | collective-permute-start | bytes 1572872 | tf_op jit(solution)/shard_map/ppermute | solution.py:454
  193.7 3.1 %collective-permute-done.10.got = bf16[128,2048]{1,0:T(8,128)(2,1)S(1)} collective-permute-done((bf16[128,2048]{1,0:T(8,128)(2,1)S(1)}, bf16[128,2048]{1,0:T(8,128)(2,1)S(1)}, u32[]{:S(2)}, u32[]{:S(2)}) %collective-permute-start.10) | collective-permute-done | bytes 524320 | tf_op jit(solution)/shard_map/ppermute | solution.py:454
  196.8 0.1 shard_map.209
  196.9 3.9 %collective-permute-start.11 = (bf16[128,2048]{1,0:T(8,128)(2,1)S(1)}, bf16[128,2048]{1,0:T(8,128)(2,1)S(1)}, u32[]{:S(2)}, u32[]{:S(2)}) collective-permute-start(bf16[128,2048]{1,0:T(8,128)(2,1)S(1)} %shard_map.209), channel_id=1, source_target_pairs={{0,1},{4,7},{1,2},{5,4},{2,3},{6,5},{3,0},{7,6},{8,9},{12,15},{9,1... | collective-permute-start | bytes 1572872 | tf_op jit(solution)/shard_map/ppermute | solution.py:454
  200.8 1.6 collective-permute-done.9.a
  202.5 7.4 %collective-permute-done.11.b = bf16[128,2048]{1,0:T(8,128)(2,1)S(1)} collective-permute-done((bf16[128,2048]{1,0:T(8,128)(2,1)S(1)}, bf16[128,2048]{1,0:T(8,128)(2,1)S(1)}, u32[]{:S(2)}, u32[]{:S(2)}) %collective-permute-start.11) | collective-permute-done | bytes 524320 | tf_op jit(solution)/shard_map/ppermute | solution.py:454
  209.8 1.0 shard_map.210
  (7 shorter events, 0.0 us)
Async XLA Ops:
  57.1 26.9 %copy-start.1 = (f32[24,256]{1,0:T(8,128)S(1)}, f32[24,256]{1,0:T(8,128)}, u32[]{:S(2)}) copy-start(f32[24,256]{1,0:T(8,128)} %get-tuple-element.31.small) | copy-start | bytes 73732
  57.1 26.9 %copy-start.10 = (bf16[2048,4]{0,1:T(4,128)(2,1)S(1)}, bf16[2048,4]{0,1:T(4,128)(2,1)}, u32[]{:S(2)}) copy-start(bf16[2048,4]{0,1:T(4,128)(2,1)} %param.30) | copy-start | bytes 49156
  57.1 26.9 %copy-start.11 = (f32[4,512]{1,0:T(4,128)S(1)}, f32[4,512]{1,0:T(4,128)}, u32[]{:S(2)}) copy-start(f32[4,512]{1,0:T(4,128)} %spikes.1) | copy-start | bytes 24580
  57.1 26.9 %all-to-all-start = ((bf16[4,128,2048]{2,1,0:T(8,128)(2,1)}), bf16[4,128,2048]{2,1,0:T(8,128)(2,1)S(1)}, u32[]{:S(2)}, u32[]{:S(2)}) async-start(bf16[4,128,2048]{2,1,0:T(8,128)(2,1)} %get-tuple-element.30), calls=%async_computation | async-start | bytes 4194304 | tf_op jit(solution)/shard_map/all_to_all | solution.py:447
  61.7 20.3 %collective-permute-start.2 = (bf16[16,208,128]{2,1,0:T(8,128)(2,1)}, bf16[16,208,128]{2,1,0:T(8,128)(2,1)}, u32[]{:S(2)}, u32[]{:S(2)}) collective-permute-start(bf16[16,208,128]{2,1,0:T(8,128)(2,1)} %get-tuple-element.39.p0), channel_id=1, source_target_pairs={{0,8},{4,28},{8,16},{12,4},{16,24},{20,12},{24,0},{28,20},{1,9},{5... | collective-permute-start | bytes 2555912 | tf_op jit(solution)/shard_map/ppermute | solution.py:453
  63.8 23.3 %collective-permute-start.1 = (bf16[4,16,48,128]{3,2,1,0:T(8,128)(2,1)S(1)}, bf16[4,16,48,128]{3,2,1,0:T(8,128)(2,1)}, u32[]{:S(2)}, u32[]{:S(2)}) collective-permute-start(bf16[4,16,48,128]{3,2,1,0:T(8,128)(2,1)S(1)} %all_to_all.25.own), channel_id=1, source_target_pairs={{0,4},{4,0},{1,5},{5,1},{2,6},{6,2},{3,7},{7,3},{8,12},{12,8},{9,1... | collective-permute-start | bytes 2359304 | tf_op jit(solution)/shard_map/ppermute | solution.py:458
  65.7 43.1 %collective-permute-start.3 = (bf16[16,208,128]{2,1,0:T(8,128)(2,1)}, bf16[16,208,128]{2,1,0:T(8,128)(2,1)}, u32[]{:S(2)}, u32[]{:S(2)}) collective-permute-start(bf16[16,208,128]{2,1,0:T(8,128)(2,1)} %get-tuple-element.39.p0), channel_id=1, source_target_pairs={{0,24},{4,12},{8,0},{12,20},{16,8},{20,28},{24,16},{28,4},{1,25},{... | collective-permute-start | bytes 2555912 | tf_op jit(solution)/shard_map/ppermute | solution.py:453
  82.0 28.9 %collective-permute-start.4 = (bf16[16,208,128]{2,1,0:T(8,128)(2,1)}, bf16[16,208,128]{2,1,0:T(8,128)(2,1)}, u32[]{:S(2)}, u32[]{:S(2)}) collective-permute-start(bf16[16,208,128]{2,1,0:T(8,128)(2,1)} %collective-permute-done.2.p1), channel_id=1, source_target_pairs={{0,8},{4,28},{8,16},{12,4},{16,24},{20,12},{24,0},{28,20},{1,9},{5... | collective-permute-start | bytes 2555912 | tf_op jit(solution)/shard_map/ppermute | solution.py:453
  84.0 7.5 %copy-start = (bf16[4,128,2048]{2,1,0:T(8,128)(2,1)}, bf16[4,128,2048]{2,1,0:T(8,128)(2,1)S(1)}, u32[]{:S(2)}) copy-start(bf16[4,128,2048]{2,1,0:T(8,128)(2,1)S(1)} %all-to-all-done.tok) | copy-start | bytes 6291460
  85.2 6.3 %collective-permute-start = (bf16[16,2048]{1,0:T(8,128)(2,1)S(1)}, bf16[16,2048]{1,0:T(8,128)(2,1)S(1)}, u32[]{:S(2)}, u32[]{:S(2)}) collective-permute-start(bf16[16,2048]{1,0:T(8,128)(2,1)S(1)} %get-tuple-element.32), channel_id=1, source_target_pairs={{0,4},{4,8},{8,12},{12,16},{16,20},{20,24},{24,28},{28,32},{32,36}... | collective-permute-start | bytes 196616 | tf_op jit(solution)/shard_map/ppermute | solution.py:540
  91.5 21.7 %copy-start.12 = (f32[1,256]{1,0:T(1,128)S(1)}, f32[1,256]{1,0:T(1,128)}, u32[]{:S(2)}) copy-start(f32[1,256]{1,0:T(1,128)} %get-tuple-element.38.left) | copy-start | bytes 3076
  97.3 15.9 %all-to-all-start.2 = ((bf16[8,24,256]{2,1,0:T(8,128)(2,1)}), bf16[8,24,256]{2,1,0:T(8,128)(2,1)S(1)}, u32[]{:S(2)}, u32[]{:S(2)}) async-start(bf16[8,24,256]{2,1,0:T(8,128)(2,1)} %get-tuple-element.37), calls=%async_computation.2 | async-start | bytes 196608 | tf_op jit(solution)/shard_map/all_to_all | solution.py:447
  104.5 40.4 %collective-permute-start.5 = (bf16[16,208,128]{2,1,0:T(8,128)(2,1)}, bf16[16,208,128]{2,1,0:T(8,128)(2,1)}, u32[]{:S(2)}, u32[]{:S(2)}) collective-permute-start(bf16[16,208,128]{2,1,0:T(8,128)(2,1)} %get-tuple-element.39.p0), channel_id=1, source_target_pairs={{0,4},{4,0},{1,5},{5,1},{2,6},{6,2},{3,7},{7,3},{8,12},{12,8},{9,1... | collective-permute-start | bytes 2555912 | tf_op jit(solution)/shard_map/ppermute | solution.py:458
  106.6 38.4 %collective-permute-start.6 = (bf16[16,208,128]{2,1,0:T(8,128)(2,1)}, bf16[16,208,128]{2,1,0:T(8,128)(2,1)S(1)}, u32[]{:S(2)}, u32[]{:S(2)}) collective-permute-start(bf16[16,208,128]{2,1,0:T(8,128)(2,1)} %collective-permute-done.2.p1), channel_id=1, source_target_pairs={{0,4},{4,0},{1,5},{5,1},{2,6},{6,2},{3,7},{7,3},{8,12},{12,8},{9,1... | collective-permute-start | bytes 2555912 | tf_op jit(solution)/shard_map/ppermute | solution.py:458
  108.9 36.1 %collective-permute-start.7 = (bf16[16,208,128]{2,1,0:T(8,128)(2,1)}, bf16[16,208,128]{2,1,0:T(8,128)(2,1)S(1)}, u32[]{:S(2)}, u32[]{:S(2)}) collective-permute-start(bf16[16,208,128]{2,1,0:T(8,128)(2,1)} %collective-permute-done.3.p2), channel_id=1, source_target_pairs={{0,4},{4,0},{1,5},{5,1},{2,6},{6,2},{3,7},{7,3},{8,12},{12,8},{9,1... | collective-permute-start | bytes 2555912 | tf_op jit(solution)/shard_map/ppermute | solution.py:458
  110.9 34.0 %collective-permute-start.8 = (bf16[16,208,128]{2,1,0:T(8,128)(2,1)}, bf16[16,208,128]{2,1,0:T(8,128)(2,1)S(1)}, u32[]{:S(2)}, u32[]{:S(2)}) collective-permute-start(bf16[16,208,128]{2,1,0:T(8,128)(2,1)} %collective-permute-done.4.p3), channel_id=1, source_target_pairs={{0,4},{4,0},{1,5},{5,1},{2,6},{6,2},{3,7},{7,3},{8,12},{12,8},{9,1... | collective-permute-start | bytes 2555912 | tf_op jit(solution)/shard_map/ppermute | solution.py:458
  140.1 41.7 %all-to-all-start.4 = ((bf16[8,32,256]{2,1,0:T(8,128)(2,1)}), bf16[8,32,256]{2,1,0:T(8,128)(2,1)S(1)}, u32[]{:S(2)}, u32[]{:S(2)}) async-start(bf16[8,32,256]{2,1,0:T(8,128)(2,1)} %shard_map.204), calls=%async_computation.4 | async-start | bytes 262144 | tf_op jit(solution)/shard_map/all_to_all | solution.py:447
  144.9 35.9 %copy-start.4 = (f32[512,256]{1,0:T(8,128)S(1)}, f32[512,256]{1,0:T(8,128)}, u32[]{:S(2)}) copy-start(f32[512,256]{1,0:T(8,128)} %get-tuple-element.42.seq_input) | copy-start | bytes 1572868
  144.9 35.9 %copy-start.5 = (bf16[512,256]{1,0:T(8,128)(2,1)S(1)}, bf16[512,256]{1,0:T(8,128)(2,1)}, u32[]{:S(2)}) copy-start(bf16[512,256]{1,0:T(8,128)(2,1)} %get-tuple-element.41.weighted) | copy-start | bytes 786436
  144.9 35.9 %copy-start.6 = (bf16[4,128,256]{2,1,0:T(8,128)(2,1)S(1)}, bf16[4,128,256]{2,1,0:T(8,128)(2,1)}, u32[]{:S(2)}) copy-start(bf16[4,128,256]{2,1,0:T(8,128)(2,1)} %get-tuple-element.44.local) | copy-start | bytes 786436
  144.9 35.9 %copy-start.9 = (bf16[512,128]{1,0:T(8,128)(2,1)S(1)}, bf16[512,128]{1,0:T(8,128)(2,1)}, u32[]{:S(2)}) copy-start(bf16[512,128]{1,0:T(8,128)(2,1)} %get-tuple-element.43.seq_write) | copy-start | bytes 393220
  179.3 0.8 copy-start.2
  180.1 0.7 copy-start.7
  180.8 1.0 copy-start.3
  180.8 1.1 copy-start.8
  184.5 12.3 %collective-permute-start.10 = (bf16[128,2048]{1,0:T(8,128)(2,1)S(1)}, bf16[128,2048]{1,0:T(8,128)(2,1)S(1)}, u32[]{:S(2)}, u32[]{:S(2)}) collective-permute-start(bf16[128,2048]{1,0:T(8,128)(2,1)S(1)} %get-tuple-element.54), channel_id=1, source_target_pairs={{0,1},{4,7},{1,2},{5,4},{2,3},{6,5},{3,0},{7,6},{8,9},{12,15},{9,1... | collective-permute-start | bytes 1572872 | tf_op jit(solution)/shard_map/ppermute | solution.py:454
  190.6 11.8 %collective-permute-start.9 = (bf16[128,2048]{1,0:T(8,128)(2,1)S(1)}, bf16[128,2048]{1,0:T(8,128)(2,1)S(1)}, u32[]{:S(2)}, u32[]{:S(2)}) collective-permute-start(bf16[128,2048]{1,0:T(8,128)(2,1)S(1)} %get-tuple-element.52), channel_id=1, source_target_pairs={{0,3},{4,5},{1,0},{5,6},{2,1},{6,7},{3,2},{7,4},{8,11},{12,13},{9,... | collective-permute-start | bytes 1572872 | tf_op jit(solution)/shard_map/ppermute | solution.py:454
  196.9 12.9 %collective-permute-start.11 = (bf16[128,2048]{1,0:T(8,128)(2,1)S(1)}, bf16[128,2048]{1,0:T(8,128)(2,1)S(1)}, u32[]{:S(2)}, u32[]{:S(2)}) collective-permute-start(bf16[128,2048]{1,0:T(8,128)(2,1)S(1)} %shard_map.209), channel_id=1, source_target_pairs={{0,1},{4,7},{1,2},{5,4},{2,3},{6,5},{3,0},{7,6},{8,9},{12,15},{9,1... | collective-permute-start | bytes 1572872 | tf_op jit(solution)/shard_map/ppermute | solution.py:454

commit v6 on v5

--- a/solution.py
+++ b/solution.py
@@ -328,15 +328,15 @@
 def rest_body(
     tok, halo, p0, p1, p2, p3, p4, p5, p6, p7, small,
     read_out, gate, mixer, wide,
-    whole, more, normed, fields, sem, sems,
+    whole, more, laid, normed, fields, sem, sems, store_sem,
 ):
     parts = (p0, p1, p2, p3, p4, p5, p6, p7)
     fetch = fetches(tok, normed, sem)
     one = ring_copies(parts, FAR, whole, 0, 48, sems.at[0])
     two = ring_copies(parts, FAR, more, 48, 96, sems.at[1])
-    store = ring_copies(parts, range(8), wide, 144, 64, sems.at[2])
+    three = ring_copies(parts, FAR, laid, 144, 64, sems.at[2])
     normed[0:HALO, :] = halo[...]
-    lay_out(ring_pieces(parts, NEAR), ((whole, 0, 48), (more, 48, 96)))
+    lay_out(ring_pieces(parts, NEAR), ((whole, 0, 48), (more, 48, 96), (laid, 144, 64)))
     wait_for(fetch)
     wait_for(one)
     n = normed[...]
@@ -347,12 +347,15 @@
     fields[:, 0:128] = projected(whole, 0, 1)
     read_out[...] = silu(taps(fields, small[11:15, 0:128], slice(0, 128), 4)).astype(BF16)
     gate[...] = silu(projected(whole, 1, 2)[HALO:])
+    wait_for(three)
+    store = pltpu.make_async_copy(laid, wide, store_sem)
+    store.start()
     wait_for(two)
     inner = projected(more, 2, 2)
     fields[...] = inner * projected(more, 4, 2)
     outer = projected(more, 0, 2)[HALO:]
     mixer[...] = (outer * taps(fields, small[0:3, :], slice(0, 256), 3)).astype(BF16)
-    wait_for(store)
+    store.wait()
 
 
 def within_body(
@@ -575,12 +578,14 @@
         scratch=(
             pltpu.VMEM((16, 4, 2, 48, 128), BF16),
             pltpu.VMEM((16, 4, 2, 96, 128), BF16),
+            pltpu.VMEM((16, 4, 2, 64, 128), BF16),
             pltpu.VMEM((HALO + ROWS, 2048), BF16),
             pltpu.VMEM((HALO + ROWS, 256), F32),
             pltpu.SemaphoreType.DMA((4,)),
             pltpu.SemaphoreType.DMA((3, 8)),
-        ),
-        mib=20,
+            pltpu.SemaphoreType.DMA,
+        ),
+        mib=24,
         far_in=(0, *(2 + i for i in FAR)),
         far_out=(3,),
     )

time: 212 us -> 186 us (0.88)
  Pallas kernels: 53.5 us -> 27.5 us
    pallas_call x12, Pallas kernels: 53.5 us -> 27.5 us  [call(): pl.pallas_call(body, out_shape=outs, in_specs=[hbm if i in far_in else vm...]
  transfers between devices with their start and end apart: 15 -> 15, of which waited for: 5 -> 5; matrix products, arithmetic and copies ran while one was open for 0% -> 0% of each run, Pallas kernels for 22% -> 11%
where the time goes in v6:
time: 186 us; the launch traced here: 185 us
  blocking collectives  78.6 us (42%)
  starting transfers between devices  47.8 us (26%)
  waiting for transfers between devices  29 us (16%)
  Pallas kernels  27.5 us (15%)
    all_gather x1, blocking collectives, per_device(): column = lax.all_gather(own, 'z', axis=0, tiled=False)  39.7 us
    all_to_all x2, blocking collectives, exchanged(): return lax.all_to_all(tiles, axis, 0, 0, tiled=True)  38.9 us
    pallas_call x12, Pallas kernels, call(): pl.pallas_call(body, out_shape=outs, in_specs=[hbm if i in far_in else vm...  27.5 us
    all_to_all x3, starting transfers between devices, exchanged(): return lax.all_to_all(tiles, axis, 0, 0, tiled=True)  16.6 us
    ppermute x3, waiting for transfers between devices, two_way(): lax.ppermute(shard, ('x', 'c'), [(2 * i + c, 2 * j + c) for i, c, j in st...  12.6 us
    ppermute x3, waiting for transfers between devices, two_way(): lax.ppermute(shard, ('c', 'tp'), [(4 * c + i, 4 * c + j) for i, c, j in s...  12.1 us
    ppermute x3, starting transfers between devices, two_way(): lax.ppermute(shard, ('c', 'tp'), [(4 * c + i, 4 * c + j) for i, c, j in s...  10.9 us
    ppermute x5, starting transfers between devices, swapped(): return lax.ppermute(shard, 'c', [(0, 1), (1, 0)])  10.6 us
  transfers between devices with their start and end apart: 15, of which 5 were waited for; matrix products, arithmetic and copies ran while one was open for 0% of the time, Pallas kernels for 11%

profile of v6, /device:TPU:34, one launch (start us, length us, event | category | flops | bytes accessed | tf_op | source)
XLA Modules:
  0.0 184.8 jit_solution(2750132428509744371)
XLA Ops:
  0.0 3.2 %shard_map.199 = (bf16[4,128,2048]{2,1,0:T(8,128)(2,1)}, bf16[254,128]{1,0:T(8,128)(2,1)}, f32[1,256]{1,0:T(1,128)}, f32[24,256]{1,0:T(8,128)}) custom-call(bf16[128,2048]{1,0:T(8,128)(2,1)} %tok.1, bf16[16,128]{1,0:T(8,128)(2,1)} %bitcast.13, bf16[16,256]{1,0:T(8,128)(2,1)} %w0.1, bf16[16,128]{1,0:T(8,128)(2,1)} %w1.1, bf16[16,128]{1,0:T(8,128)(2,1)} %w2.1, ...), custom_call_target="tpu_custom_call" | custom-call | tf_op jit(solution)/shard_map/pallas_call | solution.py:28
  3.2 39.7 %all-gather.1.column = bf16[16,254,128]{2,1,0:T(8,128)(2,1)S(1)} all-gather(bf16[1,254,128]{2,1,0:T(8,128)(2,1)} %bitcast.10), channel_id=2, replica_groups=mesh['z'=16,'x'=4,'c'=2,'tp'=4] {'z'}, dimensions={0}, use_global_device_ids=true | all-gather | bytes 1105408 | tf_op jit(solution)/shard_map/all_gather | solution.py:519
  42.9 1.4 shard_map.201
  44.2 12.9 %all_to_all.25.own = bf16[4,16,48,128]{3,2,1,0:T(8,128)(2,1)S(1)} all-to-all(bf16[4,16,48,128]{3,2,1,0:T(8,128)(2,1)} %get-tuple-element.34), channel_id=1, replica_groups=mesh['z'=16,'x'=4,'c'=2,'tp'=4] {'x'}, dimensions={0} | all-to-all | bytes 1572864 | tf_op jit(solution)/shard_map/all_to_all | solution.py:450
  57.1 0.0 copy-start.1
  57.1 0.0 copy-start.10
  57.1 0.0 copy-start.11
  57.1 4.6 %all-to-all-start = ((bf16[4,128,2048]{2,1,0:T(8,128)(2,1)}), bf16[4,128,2048]{2,1,0:T(8,128)(2,1)S(1)}, u32[]{:S(2)}, u32[]{:S(2)}) async-start(bf16[4,128,2048]{2,1,0:T(8,128)(2,1)} %get-tuple-element.30), calls=%async_computation | async-start | bytes 4194304 | tf_op jit(solution)/shard_map/all_to_all | solution.py:450
  61.7 2.1 %collective-permute-start.2 = (bf16[16,208,128]{2,1,0:T(8,128)(2,1)}, bf16[16,208,128]{2,1,0:T(8,128)(2,1)}, u32[]{:S(2)}, u32[]{:S(2)}) collective-permute-start(bf16[16,208,128]{2,1,0:T(8,128)(2,1)} %get-tuple-element.39.p0), channel_id=1, source_target_pairs={{0,8},{4,28},{8,16},{12,4},{16,24},{20,12},{24,0},{28,20},{1,9},{5... | collective-permute-start | bytes 2555912 | tf_op jit(solution)/shard_map/ppermute | solution.py:456
  63.8 1.9 %collective-permute-start.1 = (bf16[4,16,48,128]{3,2,1,0:T(8,128)(2,1)S(1)}, bf16[4,16,48,128]{3,2,1,0:T(8,128)(2,1)}, u32[]{:S(2)}, u32[]{:S(2)}) collective-permute-start(bf16[4,16,48,128]{3,2,1,0:T(8,128)(2,1)S(1)} %all_to_all.25.own), channel_id=1, source_target_pairs={{0,4},{4,0},{1,5},{5,1},{2,6},{6,2},{3,7},{7,3},{8,12},{12,8},{9,1... | collective-permute-start | bytes 2359304 | tf_op jit(solution)/shard_map/ppermute | solution.py:461
  65.7 3.7 %collective-permute-start.3 = (bf16[16,208,128]{2,1,0:T(8,128)(2,1)}, bf16[16,208,128]{2,1,0:T(8,128)(2,1)}, u32[]{:S(2)}, u32[]{:S(2)}) collective-permute-start(bf16[16,208,128]{2,1,0:T(8,128)(2,1)} %get-tuple-element.39.p0), channel_id=1, source_target_pairs={{0,24},{4,12},{8,0},{12,20},{16,8},{20,28},{24,16},{28,4},{1,25},{... | collective-permute-start | bytes 2555912 | tf_op jit(solution)/shard_map/ppermute | solution.py:456
  69.5 12.6 %collective-permute-done.2.p1 = bf16[16,208,128]{2,1,0:T(8,128)(2,1)} collective-permute-done((bf16[16,208,128]{2,1,0:T(8,128)(2,1)}, bf16[16,208,128]{2,1,0:T(8,128)(2,1)}, u32[]{:S(2)}, u32[]{:S(2)}) %collective-permute-start.2) | collective-permute-done | bytes 852000 | tf_op jit(solution)/shard_map/ppermute | solution.py:456
  82.0 1.9 %collective-permute-start.4 = (bf16[16,208,128]{2,1,0:T(8,128)(2,1)}, bf16[16,208,128]{2,1,0:T(8,128)(2,1)}, u32[]{:S(2)}, u32[]{:S(2)}) collective-permute-start(bf16[16,208,128]{2,1,0:T(8,128)(2,1)} %collective-permute-done.2.p1), channel_id=1, source_target_pairs={{0,8},{4,28},{8,16},{12,4},{16,24},{20,12},{24,0},{28,20},{1,9},{5... | collective-permute-start | bytes 2555912 | tf_op jit(solution)/shard_map/ppermute | solution.py:456
  84.0 0.0 all-to-all-done.tok
  84.0 0.0 copy-start
  84.0 0.0 copy-done.1
  84.0 0.0 copy-done.10
  84.0 0.0 copy-done.11
  84.0 1.2 shard_map.200
  85.2 1.9 %collective-permute-start = (bf16[16,2048]{1,0:T(8,128)(2,1)S(1)}, bf16[16,2048]{1,0:T(8,128)(2,1)S(1)}, u32[]{:S(2)}, u32[]{:S(2)}) collective-permute-start(bf16[16,2048]{1,0:T(8,128)(2,1)S(1)} %get-tuple-element.32), channel_id=1, source_target_pairs={{0,4},{4,8},{8,12},{12,16},{16,20},{20,24},{24,28},{28,32},{32,36}... | collective-permute-start | bytes 196616 | tf_op jit(solution)/shard_map/ppermute | solution.py:543
  87.1 0.0 collective-permute-done.1.other
  87.2 4.3 %collective-permute-done.halo = bf16[16,2048]{1,0:T(8,128)(2,1)S(1)} collective-permute-done((bf16[16,2048]{1,0:T(8,128)(2,1)S(1)}, bf16[16,2048]{1,0:T(8,128)(2,1)S(1)}, u32[]{:S(2)}, u32[]{:S(2)}) %collective-permute-start) | collective-permute-done | bytes 65568 | tf_op jit(solution)/shard_map/ppermute | solution.py:543
  91.5 0.0 copy-done
  91.5 0.0 copy-start.12
  91.5 5.8 %shard_map.202 = (bf16[512,256]{1,0:T(8,128)(2,1)}, f32[512,256]{1,0:T(8,128)}, bf16[512,128]{1,0:T(8,128)(2,1)}, bf16[4,128,256]{2,1,0:T(8,128)(2,1)}, bf16[8,24,256]{2,1,0:T(8,128)(2,1)}) custom-call(bf16[4,128,2048]{2,1,0:T(8,128)(2,1)} %copy-done, bf16[16,2048]{1,0:T(8,128)(2,1)S(1)} %collective-permute-done.halo, ...), custom_call_target="tpu_custom_call" | custom-call | tf_op jit(solution)/shard_map/pallas_call | solution.py:28
  97.3 7.2 %all-to-all-start.2 = ((bf16[8,24,256]{2,1,0:T(8,128)(2,1)}), bf16[8,24,256]{2,1,0:T(8,128)(2,1)S(1)}, u32[]{:S(2)}, u32[]{:S(2)}) async-start(bf16[8,24,256]{2,1,0:T(8,128)(2,1)} %get-tuple-element.37), calls=%async_computation.2 | async-start | bytes 196608 | tf_op jit(solution)/shard_map/all_to_all | solution.py:450
  104.5 2.0 %collective-permute-start.5 = (bf16[16,208,128]{2,1,0:T(8,128)(2,1)}, bf16[16,208,128]{2,1,0:T(8,128)(2,1)}, u32[]{:S(2)}, u32[]{:S(2)}) collective-permute-start(bf16[16,208,128]{2,1,0:T(8,128)(2,1)} %get-tuple-element.39.p0), channel_id=1, source_target_pairs={{0,4},{4,0},{1,5},{5,1},{2,6},{6,2},{3,7},{7,3},{8,12},{12,8},{9,1... | collective-permute-start | bytes 2555912 | tf_op jit(solution)/shard_map/ppermute | solution.py:461
  106.6 2.3 %collective-permute-start.6 = (bf16[16,208,128]{2,1,0:T(8,128)(2,1)}, bf16[16,208,128]{2,1,0:T(8,128)(2,1)S(1)}, u32[]{:S(2)}, u32[]{:S(2)}) collective-permute-start(bf16[16,208,128]{2,1,0:T(8,128)(2,1)} %collective-permute-done.2.p1), channel_id=1, source_target_pairs={{0,4},{4,0},{1,5},{5,1},{2,6},{6,2},{3,7},{7,3},{8,12},{12,8},{9,1... | collective-permute-start | bytes 2555912 | tf_op jit(solution)/shard_map/ppermute | solution.py:461
  108.9 0.0 collective-permute-done.3.p2
  108.9 2.0 %collective-permute-start.7 = (bf16[16,208,128]{2,1,0:T(8,128)(2,1)}, bf16[16,208,128]{2,1,0:T(8,128)(2,1)S(1)}, u32[]{:S(2)}, u32[]{:S(2)}) collective-permute-start(bf16[16,208,128]{2,1,0:T(8,128)(2,1)} %collective-permute-done.3.p2), channel_id=1, source_target_pairs={{0,4},{4,0},{1,5},{5,1},{2,6},{6,2},{3,7},{7,3},{8,12},{12,8},{9,1... | collective-permute-start | bytes 2555912 | tf_op jit(solution)/shard_map/ppermute | solution.py:461
  110.9 0.0 collective-permute-done.4.p3
  110.9 2.3 %collective-permute-start.8 = (bf16[16,208,128]{2,1,0:T(8,128)(2,1)}, bf16[16,208,128]{2,1,0:T(8,128)(2,1)S(1)}, u32[]{:S(2)}, u32[]{:S(2)}) collective-permute-start(bf16[16,208,128]{2,1,0:T(8,128)(2,1)} %collective-permute-done.4.p3), channel_id=1, source_target_pairs={{0,4},{4,0},{1,5},{5,1},{2,6},{6,2},{3,7},{7,3},{8,12},{12,8},{9,1... | collective-permute-start | bytes 2555912 | tf_op jit(solution)/shard_map/ppermute | solution.py:461
  113.2 0.0 all-to-all-done.2.got
  113.2 0.0 copy-done.12
  113.3 26.0 %all_to_all.26.planes = bf16[16,24,256]{2,1,0:T(8,128)(2,1)S(1)} all-to-all(bf16[16,24,256]{2,1,0:T(8,128)(2,1)S(1)} %shard_map.203), channel_id=1, replica_groups=mesh['z'=16,'x'=4,'c'=2,'tp'=4] {'z'}, dimensions={0} | all-to-all | bytes 393216 | tf_op jit(solution)/shard_map/all_to_all | solution.py:450
  139.3 0.8 shard_map.204
  140.1 4.8 %all-to-all-start.4 = ((bf16[8,32,256]{2,1,0:T(8,128)(2,1)}), bf16[8,32,256]{2,1,0:T(8,128)(2,1)S(1)}, u32[]{:S(2)}, u32[]{:S(2)}) async-start(bf16[8,32,256]{2,1,0:T(8,128)(2,1)} %shard_map.204), calls=%async_computation.4 | async-start | bytes 262144 | tf_op jit(solution)/shard_map/all_to_all | solution.py:450
  144.9 0.0 copy-start.9
  144.9 0.0 collective-permute-done.5.p4
  144.9 0.0 collective-permute-done.6.p5
  144.9 0.0 collective-permute-done.7.p6
  145.0 0.0 collective-permute-done.8.p7
  145.0 8.4 %shard_map.205 = (bf16[512,128]{1,0:T(8,128)(2,1)S(1)}, f32[512,256]{1,0:T(8,128)S(1)}, bf16[512,256]{1,0:T(8,128)(2,1)S(1)}, bf16[16,4,2,64,128]{4,3,2,1,0:T(8,128)(2,1)}) custom-call(bf16[4,128,2048]{2,1,0:T(8,128)(2,1)} %copy-done, bf16[16,2048]{1,0:T(8,128)(2,1)S(1)} %collective-permute-done.halo, bf16[16,208,128]{2,1,0:T(8,128)(2,1)} %get-tuple-element.39.p0, ...), custom_call_target="tpu_custom_call" | custom-call | tf_op jit(solution)/shard_map/pallas_call | solution.py:28
  153.4 0.0 copy-start.2
  153.4 0.8 copy-done.2
  154.2 0.7 copy-done.7
  154.8 0.0 copy-done.4
  154.8 0.0 copy-done.5
  154.9 0.0 copy-done.6
  154.9 0.0 copy-done.9
  154.9 1.0 shard_map.206.partly
  155.8 0.0 all-to-all-done.4.arriving
  155.8 0.0 copy-done.3
  155.9 0.1 copy-done.8
  155.9 2.6 %shard_map.207 = (bf16[512,512]{1,0:T(8,128)(2,1)S(1)}, bf16[128,2048]{1,0:T(8,128)(2,1)S(1)}, bf16[16,4,2,64,128]{4,3,2,1,0:T(8,128)(2,1)S(1)}) custom-call(bf16[8,32,256]{2,1,0:T(8,128)(2,1)S(1)} %all-to-all-done.4.arriving, f32[512,256]{1,0:T(8,128)S(1)} %shard_map.206.partly, bf16[512,128]{1,0:T(8,128)(2,1)S(1)} %get-tuple-element.40.read, ...), custom_call_target="tpu_custom_call" | custom-call | tf_op jit(solution)/shard_map/pallas_call | solution.py:28
  158.5 3.9 %collective-permute-start.10 = (bf16[128,2048]{1,0:T(8,128)(2,1)S(1)}, bf16[128,2048]{1,0:T(8,128)(2,1)S(1)}, u32[]{:S(2)}, u32[]{:S(2)}) collective-permute-start(bf16[128,2048]{1,0:T(8,128)(2,1)S(1)} %get-tuple-element.54), channel_id=1, source_target_pairs={{0,1},{4,7},{1,2},{5,4},{2,3},{6,5},{3,0},{7,6},{8,9},{12,15},{9,1... | collective-permute-start | bytes 1572872 | tf_op jit(solution)/shard_map/ppermute | solution.py:457
  162.5 2.1 %shard_map.208 = (bf16[128,2048]{1,0:T(8,128)(2,1)S(1)}, bf16[128,2048]{1,0:T(8,128)(2,1)S(1)}, bf16[128,2048]{1,0:T(8,128)(2,1)S(1)}) custom-call(bf16[512,512]{1,0:T(8,128)(2,1)S(1)} %get-tuple-element.49.act, bf16[16,4,2,64,128]{4,3,2,1,0:T(8,128)(2,1)S(1)} %get-tuple-element.50.wide), custom_call_target="tpu_custom_call" | custom-call | tf_op jit(solution)/shard_map/pallas_call | solution.py:28
  164.6 3.1 %collective-permute-start.9 = (bf16[128,2048]{1,0:T(8,128)(2,1)S(1)}, bf16[128,2048]{1,0:T(8,128)(2,1)S(1)}, u32[]{:S(2)}, u32[]{:S(2)}) collective-permute-start(bf16[128,2048]{1,0:T(8,128)(2,1)S(1)} %get-tuple-element.52), channel_id=1, source_target_pairs={{0,3},{4,5},{1,0},{5,6},{2,1},{6,7},{3,2},{7,4},{8,11},{12,13},{9,... | collective-permute-start | bytes 1572872 | tf_op jit(solution)/shard_map/ppermute | solution.py:457
  167.8 3.1 %collective-permute-done.10.got = bf16[128,2048]{1,0:T(8,128)(2,1)S(1)} collective-permute-done((bf16[128,2048]{1,0:T(8,128)(2,1)S(1)}, bf16[128,2048]{1,0:T(8,128)(2,1)S(1)}, u32[]{:S(2)}, u32[]{:S(2)}) %collective-permute-start.10) | collective-permute-done | bytes 524320 | tf_op jit(solution)/shard_map/ppermute | solution.py:457
  170.8 0.1 shard_map.209
  171.0 3.9 %collective-permute-start.11 = (bf16[128,2048]{1,0:T(8,128)(2,1)S(1)}, bf16[128,2048]{1,0:T(8,128)(2,1)S(1)}, u32[]{:S(2)}, u32[]{:S(2)}) collective-permute-start(bf16[128,2048]{1,0:T(8,128)(2,1)S(1)} %shard_map.209), channel_id=1, source_target_pairs={{0,1},{4,7},{1,2},{5,4},{2,3},{6,5},{3,0},{7,6},{8,9},{12,15},{9,1... | collective-permute-start | bytes 1572872 | tf_op jit(solution)/shard_map/ppermute | solution.py:457
  174.8 1.6 collective-permute-done.9.a
  176.4 7.4 %collective-permute-done.11.b = bf16[128,2048]{1,0:T(8,128)(2,1)S(1)} collective-permute-done((bf16[128,2048]{1,0:T(8,128)(2,1)S(1)}, bf16[128,2048]{1,0:T(8,128)(2,1)S(1)}, u32[]{:S(2)}, u32[]{:S(2)}) %collective-permute-start.11) | collective-permute-done | bytes 524320 | tf_op jit(solution)/shard_map/ppermute | solution.py:457
  183.9 1.0 shard_map.210
  (7 shorter events, 0.0 us)
Async XLA Ops:
  57.1 26.9 %copy-start.1 = (f32[24,256]{1,0:T(8,128)S(1)}, f32[24,256]{1,0:T(8,128)}, u32[]{:S(2)}) copy-start(f32[24,256]{1,0:T(8,128)} %get-tuple-element.31.small) | copy-start | bytes 73732
  57.1 26.9 %copy-start.10 = (bf16[2048,4]{0,1:T(4,128)(2,1)S(1)}, bf16[2048,4]{0,1:T(4,128)(2,1)}, u32[]{:S(2)}) copy-start(bf16[2048,4]{0,1:T(4,128)(2,1)} %param.30) | copy-start | bytes 49156
  57.1 26.9 %copy-start.11 = (f32[4,512]{1,0:T(4,128)S(1)}, f32[4,512]{1,0:T(4,128)}, u32[]{:S(2)}) copy-start(f32[4,512]{1,0:T(4,128)} %spikes.1) | copy-start | bytes 24580
  57.1 26.9 %all-to-all-start = ((bf16[4,128,2048]{2,1,0:T(8,128)(2,1)}), bf16[4,128,2048]{2,1,0:T(8,128)(2,1)S(1)}, u32[]{:S(2)}, u32[]{:S(2)}) async-start(bf16[4,128,2048]{2,1,0:T(8,128)(2,1)} %get-tuple-element.30), calls=%async_computation | async-start | bytes 4194304 | tf_op jit(solution)/shard_map/all_to_all | solution.py:450
  61.7 20.3 %collective-permute-start.2 = (bf16[16,208,128]{2,1,0:T(8,128)(2,1)}, bf16[16,208,128]{2,1,0:T(8,128)(2,1)}, u32[]{:S(2)}, u32[]{:S(2)}) collective-permute-start(bf16[16,208,128]{2,1,0:T(8,128)(2,1)} %get-tuple-element.39.p0), channel_id=1, source_target_pairs={{0,8},{4,28},{8,16},{12,4},{16,24},{20,12},{24,0},{28,20},{1,9},{5... | collective-permute-start | bytes 2555912 | tf_op jit(solution)/shard_map/ppermute | solution.py:456
  63.8 23.3 %collective-permute-start.1 = (bf16[4,16,48,128]{3,2,1,0:T(8,128)(2,1)S(1)}, bf16[4,16,48,128]{3,2,1,0:T(8,128)(2,1)}, u32[]{:S(2)}, u32[]{:S(2)}) collective-permute-start(bf16[4,16,48,128]{3,2,1,0:T(8,128)(2,1)S(1)} %all_to_all.25.own), channel_id=1, source_target_pairs={{0,4},{4,0},{1,5},{5,1},{2,6},{6,2},{3,7},{7,3},{8,12},{12,8},{9,1... | collective-permute-start | bytes 2359304 | tf_op jit(solution)/shard_map/ppermute | solution.py:461
  65.7 43.1 %collective-permute-start.3 = (bf16[16,208,128]{2,1,0:T(8,128)(2,1)}, bf16[16,208,128]{2,1,0:T(8,128)(2,1)}, u32[]{:S(2)}, u32[]{:S(2)}) collective-permute-start(bf16[16,208,128]{2,1,0:T(8,128)(2,1)} %get-tuple-element.39.p0), channel_id=1, source_target_pairs={{0,24},{4,12},{8,0},{12,20},{16,8},{20,28},{24,16},{28,4},{1,25},{... | collective-permute-start | bytes 2555912 | tf_op jit(solution)/shard_map/ppermute | solution.py:456
  82.0 28.9 %collective-permute-start.4 = (bf16[16,208,128]{2,1,0:T(8,128)(2,1)}, bf16[16,208,128]{2,1,0:T(8,128)(2,1)}, u32[]{:S(2)}, u32[]{:S(2)}) collective-permute-start(bf16[16,208,128]{2,1,0:T(8,128)(2,1)} %collective-permute-done.2.p1), channel_id=1, source_target_pairs={{0,8},{4,28},{8,16},{12,4},{16,24},{20,12},{24,0},{28,20},{1,9},{5... | collective-permute-start | bytes 2555912 | tf_op jit(solution)/shard_map/ppermute | solution.py:456
  84.0 7.5 %copy-start = (bf16[4,128,2048]{2,1,0:T(8,128)(2,1)}, bf16[4,128,2048]{2,1,0:T(8,128)(2,1)S(1)}, u32[]{:S(2)}) copy-start(bf16[4,128,2048]{2,1,0:T(8,128)(2,1)S(1)} %all-to-all-done.tok) | copy-start | bytes 6291460
  85.2 6.3 %collective-permute-start = (bf16[16,2048]{1,0:T(8,128)(2,1)S(1)}, bf16[16,2048]{1,0:T(8,128)(2,1)S(1)}, u32[]{:S(2)}, u32[]{:S(2)}) collective-permute-start(bf16[16,2048]{1,0:T(8,128)(2,1)S(1)} %get-tuple-element.32), channel_id=1, source_target_pairs={{0,4},{4,8},{8,12},{12,16},{16,20},{20,24},{24,28},{28,32},{32,36}... | collective-permute-start | bytes 196616 | tf_op jit(solution)/shard_map/ppermute | solution.py:543
  91.5 21.7 %copy-start.12 = (f32[1,256]{1,0:T(1,128)S(1)}, f32[1,256]{1,0:T(1,128)}, u32[]{:S(2)}) copy-start(f32[1,256]{1,0:T(1,128)} %get-tuple-element.38.left) | copy-start | bytes 3076
  97.3 15.9 %all-to-all-start.2 = ((bf16[8,24,256]{2,1,0:T(8,128)(2,1)}), bf16[8,24,256]{2,1,0:T(8,128)(2,1)S(1)}, u32[]{:S(2)}, u32[]{:S(2)}) async-start(bf16[8,24,256]{2,1,0:T(8,128)(2,1)} %get-tuple-element.37), calls=%async_computation.2 | async-start | bytes 196608 | tf_op jit(solution)/shard_map/all_to_all | solution.py:450
  104.5 40.4 %collective-permute-start.5 = (bf16[16,208,128]{2,1,0:T(8,128)(2,1)}, bf16[16,208,128]{2,1,0:T(8,128)(2,1)}, u32[]{:S(2)}, u32[]{:S(2)}) collective-permute-start(bf16[16,208,128]{2,1,0:T(8,128)(2,1)} %get-tuple-element.39.p0), channel_id=1, source_target_pairs={{0,4},{4,0},{1,5},{5,1},{2,6},{6,2},{3,7},{7,3},{8,12},{12,8},{9,1... | collective-permute-start | bytes 2555912 | tf_op jit(solution)/shard_map/ppermute | solution.py:461
  106.6 38.4 %collective-permute-start.6 = (bf16[16,208,128]{2,1,0:T(8,128)(2,1)}, bf16[16,208,128]{2,1,0:T(8,128)(2,1)S(1)}, u32[]{:S(2)}, u32[]{:S(2)}) collective-permute-start(bf16[16,208,128]{2,1,0:T(8,128)(2,1)} %collective-permute-done.2.p1), channel_id=1, source_target_pairs={{0,4},{4,0},{1,5},{5,1},{2,6},{6,2},{3,7},{7,3},{8,12},{12,8},{9,1... | collective-permute-start | bytes 2555912 | tf_op jit(solution)/shard_map/ppermute | solution.py:461
  108.9 36.1 %collective-permute-start.7 = (bf16[16,208,128]{2,1,0:T(8,128)(2,1)}, bf16[16,208,128]{2,1,0:T(8,128)(2,1)S(1)}, u32[]{:S(2)}, u32[]{:S(2)}) collective-permute-start(bf16[16,208,128]{2,1,0:T(8,128)(2,1)} %collective-permute-done.3.p2), channel_id=1, source_target_pairs={{0,4},{4,0},{1,5},{5,1},{2,6},{6,2},{3,7},{7,3},{8,12},{12,8},{9,1... | collective-permute-start | bytes 2555912 | tf_op jit(solution)/shard_map/ppermute | solution.py:461
  110.9 34.0 %collective-permute-start.8 = (bf16[16,208,128]{2,1,0:T(8,128)(2,1)}, bf16[16,208,128]{2,1,0:T(8,128)(2,1)S(1)}, u32[]{:S(2)}, u32[]{:S(2)}) collective-permute-start(bf16[16,208,128]{2,1,0:T(8,128)(2,1)} %collective-permute-done.4.p3), channel_id=1, source_target_pairs={{0,4},{4,0},{1,5},{5,1},{2,6},{6,2},{3,7},{7,3},{8,12},{12,8},{9,1... | collective-permute-start | bytes 2555912 | tf_op jit(solution)/shard_map/ppermute | solution.py:461
  140.1 15.8 %all-to-all-start.4 = ((bf16[8,32,256]{2,1,0:T(8,128)(2,1)}), bf16[8,32,256]{2,1,0:T(8,128)(2,1)S(1)}, u32[]{:S(2)}, u32[]{:S(2)}) async-start(bf16[8,32,256]{2,1,0:T(8,128)(2,1)} %shard_map.204), calls=%async_computation.4 | async-start | bytes 262144 | tf_op jit(solution)/shard_map/all_to_all | solution.py:450
  144.9 9.9 %copy-start.4 = (f32[512,256]{1,0:T(8,128)S(1)}, f32[512,256]{1,0:T(8,128)}, u32[]{:S(2)}) copy-start(f32[512,256]{1,0:T(8,128)} %get-tuple-element.42.seq_input) | copy-start | bytes 1572868
  144.9 9.9 %copy-start.5 = (bf16[512,256]{1,0:T(8,128)(2,1)S(1)}, bf16[512,256]{1,0:T(8,128)(2,1)}, u32[]{:S(2)}) copy-start(bf16[512,256]{1,0:T(8,128)(2,1)} %get-tuple-element.41.weighted) | copy-start | bytes 786436
  144.9 9.9 %copy-start.6 = (bf16[4,128,256]{2,1,0:T(8,128)(2,1)S(1)}, bf16[4,128,256]{2,1,0:T(8,128)(2,1)}, u32[]{:S(2)}) copy-start(bf16[4,128,256]{2,1,0:T(8,128)(2,1)} %get-tuple-element.44.local) | copy-start | bytes 786436
  144.9 10.0 %copy-start.9 = (bf16[512,128]{1,0:T(8,128)(2,1)S(1)}, bf16[512,128]{1,0:T(8,128)(2,1)}, u32[]{:S(2)}) copy-start(bf16[512,128]{1,0:T(8,128)(2,1)} %get-tuple-element.43.seq_write) | copy-start | bytes 393220
  153.4 0.8 copy-start.2
  154.1 0.7 copy-start.7
  154.8 1.0 copy-start.3
  154.8 1.1 copy-start.8
  158.5 12.3 %collective-permute-start.10 = (bf16[128,2048]{1,0:T(8,128)(2,1)S(1)}, bf16[128,2048]{1,0:T(8,128)(2,1)S(1)}, u32[]{:S(2)}, u32[]{:S(2)}) collective-permute-start(bf16[128,2048]{1,0:T(8,128)(2,1)S(1)} %get-tuple-element.54), channel_id=1, source_target_pairs={{0,1},{4,7},{1,2},{5,4},{2,3},{6,5},{3,0},{7,6},{8,9},{12,15},{9,1... | collective-permute-start | bytes 1572872 | tf_op jit(solution)/shard_map/ppermute | solution.py:457
  164.6 11.8 %collective-permute-start.9 = (bf16[128,2048]{1,0:T(8,128)(2,1)S(1)}, bf16[128,2048]{1,0:T(8,128)(2,1)S(1)}, u32[]{:S(2)}, u32[]{:S(2)}) collective-permute-start(bf16[128,2048]{1,0:T(8,128)(2,1)S(1)} %get-tuple-element.52), channel_id=1, source_target_pairs={{0,3},{4,5},{1,0},{5,6},{2,1},{6,7},{3,2},{7,4},{8,11},{12,13},{9,... | collective-permute-start | bytes 1572872 | tf_op jit(solution)/shard_map/ppermute | solution.py:457
  171.0 12.9 %collective-permute-start.11 = (bf16[128,2048]{1,0:T(8,128)(2,1)S(1)}, bf16[128,2048]{1,0:T(8,128)(2,1)S(1)}, u32[]{:S(2)}, u32[]{:S(2)}) collective-permute-start(bf16[128,2048]{1,0:T(8,128)(2,1)S(1)} %shard_map.209), channel_id=1, source_target_pairs={{0,1},{4,7},{1,2},{5,4},{2,3},{6,5},{3,0},{7,6},{8,9},{12,15},{9,1... | collective-permute-start | bytes 1572872 | tf_op jit(solution)/shard_map/ppermute | solution.py:457

commit v7 on v6

--- a/solution.py
+++ b/solution.py
@@ -201,16 +201,18 @@
         ring[z, 192:208, :] = jnp.concatenate([v, v[0:2]], axis=0).astype(BF16)
 
 
-def cum_body(tok, ws, small, spikes, dt, cum, cum_t, edge, square):
+def cum_body(tok, ws, small, spikes, dt_t, cum_t, edge, square):
     edge[...] = tok[3, 112:128, :]
     n = tok[...].reshape(ROWS, 2048)
     square[...] = jnp.zeros(square.shape, F32)
-    square[0, 0:2, :] = small[17:19, 0:128]
-    columns = square[0].T[0:4, :]
+    square[0:2, :] = small[17:19, 0:128]
+    columns = square[...].T[0:4, :]
     raw = dot_nt(ws[...], n) + columns[:, 0:1]
     step = jnp.maximum(raw, 0.0) + jnp.log1p(jnp.exp(-jnp.abs(raw)))
     logs = -step * jnp.exp(columns[:, 1:2]) + spikes[...]
-    square[0] = jnp.zeros((BLK, BLK), F32)
+    dt_t[...] = jnp.zeros(dt_t.shape, F32)
+    cum_t[...] = jnp.zeros(cum_t.shape, F32)
+    dt_t[0:4, :] = step
     r = lax.broadcasted_iota(jnp.int32, (BLK, BLK), 0)
     s = lax.broadcasted_iota(jnp.int32, (BLK, BLK), 1)
     upper = jnp.where(r <= s, 1.0, 0.0).astype(F32)
@@ -227,11 +229,12 @@
             + carry
         )
         cum_t[0:4, rows] = part
-        square[0, 0:4, :] = part
-        square[1, 0:4, :] = step[:, rows]
-        cum[rows, :] = square[0].T
-        dt[rows, :] = square[1].T
         carry = part[:, BLK - 1 : BLK]
+
+
+def by_position(ref, start):
+    part = ref[:, start : start + BLK]
+    return jnp.concatenate([part, jnp.zeros((BLK - 8, BLK), F32)], axis=0).T
 
 
 def fetches(tok, normed, sem):
@@ -245,29 +248,30 @@
 
 
 def first_body(
-    tok, halo, own, other, dt, cum, small,
+    tok, halo, own, other, dt_t, cum_t, small,
     weighted, seq_input, seq_write, local, pieces,
-    whole, normed, fields, sem,
+    whole, normed, fields,
 ):
-    fetch = fetches(tok, normed, sem)
     normed[0:HALO, :] = halo[...]
+    normed[HALO:, :] = tok[...].reshape(ROWS, 2048)
     lay_out(first_pieces(own, other), ((whole, 0, 48),))
-    wait_for(fetch)
     projected = dot(normed[...], blocks(whole, 0, 3))
     fields[...] = projected.astype(BF16).astype(F32)
     xin = silu(taps(fields, small[3:7, :], slice(0, 256), 4))
     write = silu(taps(fields, small[7:11, 0:128], slice(256, 384), 4))
     seq_input[...] = xin
     seq_write[...] = write.astype(BF16)
-    scaled = xin * per_head(dt[:, 0:128])
+    step = jnp.concatenate([by_position(dt_t, b * BLK) for b in range(NB)], axis=0)
+    scaled = xin * per_head(step)
     weighted[...] = scaled.astype(BF16)
     state = jnp.zeros((128, 256), F32)
     before = jnp.zeros((1, 128), F32)
     for b in range(NB):
         rows = slice(b * BLK, (b + 1) * BLK)
-        end = cum[(b + 1) * BLK - 1 : (b + 1) * BLK, :]
+        here = by_position(cum_t, b * BLK)
+        end = here[BLK - 1 : BLK, :]
         local[b] = state.astype(BF16)
-        to_end = per_head(jnp.exp(end - cum[rows, :]))
+        to_end = per_head(jnp.exp(end - here))
         added = dot(write[rows].T.astype(BF16), (scaled[rows] * to_end).astype(BF16))
         state = state * per_head(jnp.exp(end - before)) + added
         before = end
@@ -359,19 +363,32 @@
 
 
 def within_body(
-    read, weighted, seq_input, seq_write, local, cum, cum_t, small, partly
+    read, far_weighted, far_input, far_write, far_local, cum_t, small, partly,
+    weighted, seq_input, seq_write, local, sem,
 ):
+    pairs = (
+        (far_write, seq_write),
+        (far_local, local),
+        (far_weighted, weighted),
+        (far_input, seq_input),
+    )
+    fetch = [
+        pltpu.make_async_copy(far, here, sem.at[i]) for i, (far, here) in enumerate(pairs)
+    ]
+    for copy in fetch:
+        copy.start()
     weight = per_head(small[16:17, 0:128])
     r = lax.broadcasted_iota(jnp.int32, (BLK, BLK), 0)
     s = lax.broadcasted_iota(jnp.int32, (BLK, BLK), 1)
     causal = r >= s
     low = s < 64
     before = jnp.zeros((1, 128), F32)
+    wait_for(fetch)
     for b in range(NB):
         rows = slice(b * BLK, (b + 1) * BLK)
         rb = read[rows, :]
         scores = dot_nt(rb, seq_write[rows, :])
-        here = cum[rows, :]
+        here = by_position(cum_t, b * BLK)
         from_local = dot(rb, local[b]) * per_head(jnp.exp(here - before))
         before = here[BLK - 1 : BLK, :]
         halves = []
@@ -399,8 +416,8 @@
             wide[z, j // 2, j % 2, 48:64, :] = tile.astype(BF16)
 
 
-def project_out(act, at, wide, out):
-    a = act[pl.ds(pl.multiple_of(at * 128, 128), 128), :]
+def project_out(act, wide, out):
+    a = act[...]
     for q in range(4):
         zs = slice(4 * q, 4 * (q + 1))
         w = [wide[zs, :, :, 16 * k : 16 * (k + 1), :].reshape(512, 128) for k in range(4)]
@@ -408,15 +425,13 @@
         out[:, 512 * q : 512 * (q + 1)] = dot_nt(a, w).astype(out.dtype)
 
 
-def tail_body(
-    arriving, partly, read, gate, cum, mixer, small, stored, act, far, wide, sem
-):
-    fetch = pltpu.make_async_copy(stored, wide, sem)
-    fetch.start()
-    act[:, 0:256] = mixer[...]
+def finish_rows(at, arriving, partly, read, gate, cum_t, mixer, small, act):
+    rows = pl.ds(pl.multiple_of(at * 128, 128), 128)
     state = jnp.concatenate([arriving[j, 0:16, :] for j in range(8)], axis=0)
-    head = partly[...] + dot(read[...], state) * per_head(jnp.exp(cum[...]))
-    gated = head * gate[...]
+    part = cum_t[:, rows]
+    here = jnp.concatenate([part, jnp.zeros((BLK - 8, BLK), F32)], axis=0).T
+    head = partly[rows, :] + dot(read[rows, :], state) * per_head(jnp.exp(here))
+    gated = head * gate[rows, :]
     square = gated * gated
     r = lax.broadcasted_iota(jnp.int32, (256, 256), 0) // 64
     s = lax.broadcasted_iota(jnp.int32, (256, 256), 1) // 64
@@ -424,17 +439,29 @@
     high = square.astype(BF16)
     rest = (square - high.astype(F32)).astype(BF16)
     mean = dot(high, same) + dot(rest, same)
+    act[:, 0:256] = mixer[rows, :]
     act[:, 256:512] = (gated * lax.rsqrt(mean + EPS) * small[15:16, :]).astype(BF16)
+
+
+def tail_body(
+    arriving, partly, read, gate, cum_t, mixer, small, stored, far, wide, act, sem
+):
+    fetch = pltpu.make_async_copy(stored, wide, sem)
+    fetch.start()
+    at = (lax.axis_index("tp") + 2) % 4
+    finish_rows(at, arriving, partly, read, gate, cum_t, mixer, small, act)
     fetch.wait()
     patch(wide, arriving)
-    project_out(act, (lax.axis_index("tp") + 2) % 4, wide, far)
-
-
-def near_body(act, wide, beside, near, mine):
+    project_out(act, wide, far)
+
+
+def near_body(
+    arriving, partly, read, gate, cum_t, mixer, small, wide, beside, near, mine, act
+):
     y, c = lax.axis_index("tp"), lax.axis_index("c")
-    project_out(act, (y + 3 + 2 * c) % 4, wide, beside)
-    project_out(act, (y + 1 + 2 * c) % 4, wide, near)
-    project_out(act, y, wide, mine)
+    for at, out in (((y + 3 + 2 * c) % 4, beside), ((y + 1 + 2 * c) % 4, near), (y, mine)):
+        finish_rows(at, arriving, partly, read, gate, cum_t, mixer, small, act)
+        project_out(act, wide, out)
 
 
 def add_body(near, got, out):
@@ -529,16 +556,15 @@
     ring.append(two_way(ring[0], "x", -1))
     ring.append(two_way(ring[1], "x", 1))
     ring += [swapped(part) for part in ring]
-    dt, cum, cum_t, edge = call(
+    dt_t, cum_t, edge = call(
         cum_body,
         (
-            shape((ROWS, 128), F32),
-            shape((ROWS, 128), F32),
+            shape((8, ROWS), F32),
             shape((8, ROWS), F32),
             shape((HALO, 2048), BF16),
         ),
         (tok, step_size_weight.T, small, decay_spikes),
-        scratch=(pltpu.VMEM((2, BLK, BLK), F32),),
+        scratch=(pltpu.VMEM((BLK, BLK), F32),),
     )
     halo = lax.ppermute(edge, SP, [(i, i + 1) for i in range(127)])
     weighted, seq_input, seq_write, local, pieces = call(
@@ -550,15 +576,13 @@
             main_memory((NB, 128, 256), BF16),
             main_memory((8, 24, 256), BF16),
         ),
-        (tok, halo, first, first_other, dt, cum, small),
+        (tok, halo, first, first_other, dt_t, cum_t, small),
         (
             pltpu.VMEM((16, 4, 2, 48, 128), BF16),
             pltpu.VMEM((HALO + ROWS, 2048), BF16),
             pltpu.VMEM((HALO + ROWS, 384), F32),
-            pltpu.SemaphoreType.DMA((4,)),
         ),
         mib=16,
-        far_in=(0,),
     )
     got = exchanged(pieces, ("x", "c"))
     send = call(plane_body, shape((16, 24, 256), BF16), (got, left))
@@ -570,8 +594,8 @@
         rest_body,
         (
             on_chip((ROWS, 128), BF16),
-            on_chip((ROWS, 256), F32),
-            on_chip((ROWS, 256), BF16),
+            main_memory((ROWS, 256), F32),
+            main_memory((ROWS, 256), BF16),
             main_memory((16, 4, 2, 64, 128), BF16),
         ),
         (tok, halo, *ring, small),
@@ -592,23 +616,34 @@
     partly = call(
         within_body,
         shape((ROWS, 256), F32),
-        (read, weighted, seq_input, seq_write, local, cum, cum_t, small),
-    )
-    act, far, wide = call(
+        (read, weighted, seq_input, seq_write, local, cum_t, small),
+        scratch=(
+            pltpu.VMEM((ROWS, 256), BF16),
+            pltpu.VMEM((ROWS, 256), F32),
+            pltpu.VMEM((ROWS, 128), BF16),
+            pltpu.VMEM((NB, 128, 256), BF16),
+            pltpu.SemaphoreType.DMA((4,)),
+        ),
+        far_in=(1, 2, 3, 4),
+    )
+    block_ = shape((128, 2048), BF16)
+    rows_ = (arriving, partly, read, gate, cum_t, mixer, small)
+    far, wide = call(
         tail_body,
-        (
-            on_chip((ROWS, 512), BF16),
-            shape((128, 2048), BF16),
-            on_chip((16, 4, 2, 64, 128), BF16),
-        ),
-        (arriving, partly, read, gate, cum, mixer, small, wide),
-        scratch=(pltpu.SemaphoreType.DMA,),
+        (block_, on_chip((16, 4, 2, 64, 128), BF16)),
+        (*rows_, wide),
+        scratch=(pltpu.VMEM((128, 512), BF16), pltpu.SemaphoreType.DMA),
         mib=16,
         far_in=(7,),
     )
     got_far = two_way(far, "tp", 1)
-    block_ = shape((128, 2048), BF16)
-    beside, near, mine = call(near_body, (block_, block_, block_), (act, wide), mib=12)
+    beside, near, mine = call(
+        near_body,
+        (block_, block_, block_),
+        (*rows_, wide),
+        scratch=(pltpu.VMEM((128, 512), BF16),),
+        mib=12,
+    )
     got_beside = two_way(beside, "tp", -1)
     both = call(add_body, shape((128, 2048), BF16), (near, got_far))
     got_near = two_way(both, "tp", 1)

time: 186 us -> 187 us (level)
  no operation moved by 1% of the time
where the time goes in v7:
time: 187 us; the launch traced here: 186 us
  blocking collectives  78.6 us (42%)
  starting transfers between devices  47.4 us (25%)
  Pallas kernels  29.2 us (16%)
  waiting for transfers between devices  28.5 us (15%)
  local copies, waits for them, and re-layouts  1.91 us (1%)
    all_gather x1, blocking collectives, per_device(): column = lax.all_gather(own, 'z', axis=0, tiled=False)  39.7 us
    all_to_all x2, blocking collectives, exchanged(): return lax.all_to_all(tiles, axis, 0, 0, tiled=True)  38.9 us
    pallas_call x12, Pallas kernels, call(): pl.pallas_call(body, out_shape=outs, in_specs=[hbm if i in far_in else vm...  29.2 us
    all_to_all x3, starting transfers between devices, exchanged(): return lax.all_to_all(tiles, axis, 0, 0, tiled=True)  16.6 us
    ppermute x3, waiting for transfers between devices, two_way(): lax.ppermute(shard, ('x', 'c'), [(2 * i + c, 2 * j + c) for i, c, j in st...  12.6 us
    ppermute x3, waiting for transfers between devices, two_way(): lax.ppermute(shard, ('c', 'tp'), [(4 * c + i, 4 * c + j) for i, c, j in s...  11.6 us
    ppermute x5, starting transfers between devices, swapped(): return lax.ppermute(shard, 'c', [(0, 1), (1, 0)])  10.6 us
    ppermute x3, starting transfers between devices, two_way(): lax.ppermute(shard, ('c', 'tp'), [(4 * c + i, 4 * c + j) for i, c, j in s...  10.4 us
  transfers between devices with their start and end apart: 15, of which 5 were waited for; matrix products, arithmetic and copies ran while one was open for 0% of the time, Pallas kernels for 11%

profile of v7, /device:TPU:34, one launch (start us, length us, event | category | flops | bytes accessed | tf_op | source)
XLA Modules:
  0.0 186.0 jit_solution(16995903558031902463)
XLA Ops:
  0.0 3.2 %shard_map.199 = (bf16[4,128,2048]{2,1,0:T(8,128)(2,1)}, bf16[254,128]{1,0:T(8,128)(2,1)}, f32[1,256]{1,0:T(1,128)}, f32[24,256]{1,0:T(8,128)}) custom-call(bf16[128,2048]{1,0:T(8,128)(2,1)} %tok.1, bf16[16,128]{1,0:T(8,128)(2,1)} %bitcast.13, bf16[16,256]{1,0:T(8,128)(2,1)} %w0.1, bf16[16,128]{1,0:T(8,128)(2,1)} %w1.1, bf16[16,128]{1,0:T(8,128)(2,1)} %w2.1, ...), custom_call_target="tpu_custom_call" | custom-call | tf_op jit(solution)/shard_map/pallas_call | solution.py:28
  3.2 39.7 %all-gather.1.column = bf16[16,254,128]{2,1,0:T(8,128)(2,1)S(1)} all-gather(bf16[1,254,128]{2,1,0:T(8,128)(2,1)} %bitcast.10), channel_id=2, replica_groups=mesh['z'=16,'x'=4,'c'=2,'tp'=4] {'z'}, dimensions={0}, use_global_device_ids=true | all-gather | bytes 1105408 | tf_op jit(solution)/shard_map/all_gather | solution.py:546
  42.9 1.3 shard_map.201
  44.2 12.9 %all_to_all.25.own = bf16[4,16,48,128]{3,2,1,0:T(8,128)(2,1)S(1)} all-to-all(bf16[4,16,48,128]{3,2,1,0:T(8,128)(2,1)} %get-tuple-element.32), channel_id=1, replica_groups=mesh['z'=16,'x'=4,'c'=2,'tp'=4] {'x'}, dimensions={0} | all-to-all | bytes 1572864 | tf_op jit(solution)/shard_map/all_to_all | solution.py:477
  57.1 0.0 copy-start.4
  57.1 0.0 copy-start.5
  57.1 0.0 copy-start.6
  57.1 4.6 %all-to-all-start = ((bf16[4,128,2048]{2,1,0:T(8,128)(2,1)}), bf16[4,128,2048]{2,1,0:T(8,128)(2,1)S(1)}, u32[]{:S(2)}, u32[]{:S(2)}) async-start(bf16[4,128,2048]{2,1,0:T(8,128)(2,1)} %get-tuple-element.28), calls=%async_computation | async-start | bytes 4194304 | tf_op jit(solution)/shard_map/all_to_all | solution.py:477
  61.7 2.1 %collective-permute-start.2 = (bf16[16,208,128]{2,1,0:T(8,128)(2,1)}, bf16[16,208,128]{2,1,0:T(8,128)(2,1)}, u32[]{:S(2)}, u32[]{:S(2)}) collective-permute-start(bf16[16,208,128]{2,1,0:T(8,128)(2,1)} %get-tuple-element.37.p0), channel_id=1, source_target_pairs={{0,8},{4,28},{8,16},{12,4},{16,24},{20,12},{24,0},{28,20},{1,9},{5... | collective-permute-start | bytes 2555912 | tf_op jit(solution)/shard_map/ppermute | solution.py:483
  63.8 1.9 %collective-permute-start.1 = (bf16[4,16,48,128]{3,2,1,0:T(8,128)(2,1)S(1)}, bf16[4,16,48,128]{3,2,1,0:T(8,128)(2,1)}, u32[]{:S(2)}, u32[]{:S(2)}) collective-permute-start(bf16[4,16,48,128]{3,2,1,0:T(8,128)(2,1)S(1)} %all_to_all.25.own), channel_id=1, source_target_pairs={{0,4},{4,0},{1,5},{5,1},{2,6},{6,2},{3,7},{7,3},{8,12},{12,8},{9,1... | collective-permute-start | bytes 2359304 | tf_op jit(solution)/shard_map/ppermute | solution.py:488
  65.7 3.7 %collective-permute-start.3 = (bf16[16,208,128]{2,1,0:T(8,128)(2,1)}, bf16[16,208,128]{2,1,0:T(8,128)(2,1)}, u32[]{:S(2)}, u32[]{:S(2)}) collective-permute-start(bf16[16,208,128]{2,1,0:T(8,128)(2,1)} %get-tuple-element.37.p0), channel_id=1, source_target_pairs={{0,24},{4,12},{8,0},{12,20},{16,8},{20,28},{24,16},{28,4},{1,25},{... | collective-permute-start | bytes 2555912 | tf_op jit(solution)/shard_map/ppermute | solution.py:483
  69.4 12.6 %collective-permute-done.2.p1 = bf16[16,208,128]{2,1,0:T(8,128)(2,1)} collective-permute-done((bf16[16,208,128]{2,1,0:T(8,128)(2,1)}, bf16[16,208,128]{2,1,0:T(8,128)(2,1)}, u32[]{:S(2)}, u32[]{:S(2)}) %collective-permute-start.2) | collective-permute-done | bytes 852000 | tf_op jit(solution)/shard_map/ppermute | solution.py:483
  82.0 1.9 %collective-permute-start.4 = (bf16[16,208,128]{2,1,0:T(8,128)(2,1)}, bf16[16,208,128]{2,1,0:T(8,128)(2,1)}, u32[]{:S(2)}, u32[]{:S(2)}) collective-permute-start(bf16[16,208,128]{2,1,0:T(8,128)(2,1)} %collective-permute-done.2.p1), channel_id=1, source_target_pairs={{0,8},{4,28},{8,16},{12,4},{16,24},{20,12},{24,0},{28,20},{1,9},{5... | collective-permute-start | bytes 2555912 | tf_op jit(solution)/shard_map/ppermute | solution.py:483
  83.9 0.0 all-to-all-done.tok
  83.9 0.0 copy-start
  83.9 0.0 copy-done.4
  84.0 0.0 copy-done.5
  84.0 0.0 copy-done.6
  84.0 1.1 shard_map.200
  85.0 0.0 copy-start.7
  85.0 2.1 %collective-permute-start = (bf16[16,2048]{1,0:T(8,128)(2,1)S(1)}, bf16[16,2048]{1,0:T(8,128)(2,1)S(1)}, u32[]{:S(2)}, u32[]{:S(2)}) collective-permute-start(bf16[16,2048]{1,0:T(8,128)(2,1)S(1)} %get-tuple-element.30), channel_id=1, source_target_pairs={{0,4},{4,8},{8,12},{12,16},{16,20},{20,24},{24,28},{28,32},{32,36}... | collective-permute-start | bytes 196616 | tf_op jit(solution)/shard_map/ppermute | solution.py:569
  87.1 0.0 collective-permute-done.1.other
  87.1 4.3 %collective-permute-done.halo = bf16[16,2048]{1,0:T(8,128)(2,1)S(1)} collective-permute-done((bf16[16,2048]{1,0:T(8,128)(2,1)S(1)}, bf16[16,2048]{1,0:T(8,128)(2,1)S(1)}, u32[]{:S(2)}, u32[]{:S(2)}) %collective-permute-start) | collective-permute-done | bytes 65568 | tf_op jit(solution)/shard_map/ppermute | solution.py:569
  91.5 4.7 %shard_map.202 = (bf16[512,256]{1,0:T(8,128)(2,1)}, f32[512,256]{1,0:T(8,128)}, bf16[512,128]{1,0:T(8,128)(2,1)}, bf16[4,128,256]{2,1,0:T(8,128)(2,1)}, bf16[8,24,256]{2,1,0:T(8,128)(2,1)}) custom-call(bf16[4,128,2048]{2,1,0:T(8,128)(2,1)S(1)} %all-to-all-done.tok, bf16[16,2048]{1,0:T(8,128)(2,1)S(1)} %collective-permute-done.halo, ...), custom_call_target="tpu_custom_call" | custom-call | tf_op jit(solution)/shard_map/pallas_call | solution.py:28
  96.2 0.0 copy-done
  96.2 7.2 %all-to-all-start.2 = ((bf16[8,24,256]{2,1,0:T(8,128)(2,1)}), bf16[8,24,256]{2,1,0:T(8,128)(2,1)S(1)}, u32[]{:S(2)}, u32[]{:S(2)}) async-start(bf16[8,24,256]{2,1,0:T(8,128)(2,1)} %get-tuple-element.35), calls=%async_computation.2 | async-start | bytes 196608 | tf_op jit(solution)/shard_map/all_to_all | solution.py:477
  103.3 2.0 %collective-permute-start.5 = (bf16[16,208,128]{2,1,0:T(8,128)(2,1)}, bf16[16,208,128]{2,1,0:T(8,128)(2,1)S(1)}, u32[]{:S(2)}, u32[]{:S(2)}) collective-permute-start(bf16[16,208,128]{2,1,0:T(8,128)(2,1)} %get-tuple-element.37.p0), channel_id=1, source_target_pairs={{0,4},{4,0},{1,5},{5,1},{2,6},{6,2},{3,7},{7,3},{8,12},{12,8},{9,1... | collective-permute-start | bytes 2555912 | tf_op jit(solution)/shard_map/ppermute | solution.py:488
  105.4 2.3 %collective-permute-start.6 = (bf16[16,208,128]{2,1,0:T(8,128)(2,1)}, bf16[16,208,128]{2,1,0:T(8,128)(2,1)S(1)}, u32[]{:S(2)}, u32[]{:S(2)}) collective-permute-start(bf16[16,208,128]{2,1,0:T(8,128)(2,1)} %collective-permute-done.2.p1), channel_id=1, source_target_pairs={{0,4},{4,0},{1,5},{5,1},{2,6},{6,2},{3,7},{7,3},{8,12},{12,8},{9,1... | collective-permute-start | bytes 2555912 | tf_op jit(solution)/shard_map/ppermute | solution.py:488
  107.7 0.0 collective-permute-done.3.p2
  107.7 2.0 %collective-permute-start.7 = (bf16[16,208,128]{2,1,0:T(8,128)(2,1)}, bf16[16,208,128]{2,1,0:T(8,128)(2,1)S(1)}, u32[]{:S(2)}, u32[]{:S(2)}) collective-permute-start(bf16[16,208,128]{2,1,0:T(8,128)(2,1)} %collective-permute-done.3.p2), channel_id=1, source_target_pairs={{0,4},{4,0},{1,5},{5,1},{2,6},{6,2},{3,7},{7,3},{8,12},{12,8},{9,1... | collective-permute-start | bytes 2555912 | tf_op jit(solution)/shard_map/ppermute | solution.py:488
  109.7 0.0 collective-permute-done.4.p3
  109.7 2.3 %collective-permute-start.8 = (bf16[16,208,128]{2,1,0:T(8,128)(2,1)}, bf16[16,208,128]{2,1,0:T(8,128)(2,1)}, u32[]{:S(2)}, u32[]{:S(2)}) collective-permute-start(bf16[16,208,128]{2,1,0:T(8,128)(2,1)} %collective-permute-done.4.p3), channel_id=1, source_target_pairs={{0,4},{4,0},{1,5},{5,1},{2,6},{6,2},{3,7},{7,3},{8,12},{12,8},{9,1... | collective-permute-start | bytes 2555912 | tf_op jit(solution)/shard_map/ppermute | solution.py:488
  112.0 0.0 all-to-all-done.2.got
  112.0 0.0 copy-done.7
  112.1 26.0 %all_to_all.26.planes = bf16[16,24,256]{2,1,0:T(8,128)(2,1)S(1)} all-to-all(bf16[16,24,256]{2,1,0:T(8,128)(2,1)S(1)} %shard_map.203), channel_id=1, replica_groups=mesh['z'=16,'x'=4,'c'=2,'tp'=4] {'z'}, dimensions={0} | all-to-all | bytes 393216 | tf_op jit(solution)/shard_map/all_to_all | solution.py:477
  138.1 0.8 shard_map.204
  138.9 4.8 %all-to-all-start.4 = ((bf16[8,32,256]{2,1,0:T(8,128)(2,1)}), bf16[8,32,256]{2,1,0:T(8,128)(2,1)S(1)}, u32[]{:S(2)}, u32[]{:S(2)}) async-start(bf16[8,32,256]{2,1,0:T(8,128)(2,1)} %shard_map.204), calls=%async_computation.4 | async-start | bytes 262144 | tf_op jit(solution)/shard_map/all_to_all | solution.py:477
  143.7 0.0 collective-permute-done.5.p4
  143.7 0.0 copy-start.8
  143.7 0.0 collective-permute-done.6.p5
  143.7 0.0 collective-permute-done.7.p6
  143.7 0.0 collective-permute-done.8.p7
  143.7 0.9 copy-done.8
  144.7 9.4 %shard_map.205 = (bf16[512,128]{1,0:T(8,128)(2,1)S(1)}, f32[512,256]{1,0:T(8,128)}, bf16[512,256]{1,0:T(8,128)(2,1)}, bf16[16,4,2,64,128]{4,3,2,1,0:T(8,128)(2,1)}) custom-call(bf16[4,128,2048]{2,1,0:T(8,128)(2,1)} %copy-done, bf16[16,2048]{1,0:T(8,128)(2,1)S(1)} %collective-permute-done.halo, bf16[16,208,128]{2,1,0:T(8,128)(2,1)} %get-tuple-element.37.p0, ...), custom_call_target="tpu_custom_call" | custom-call | tf_op jit(solution)/shard_map/pallas_call | solution.py:28
  154.1 0.0 copy-start.1
  154.1 0.0 copy-start.3
  154.1 2.6 %shard_map.206.partly = f32[512,256]{1,0:T(8,128)S(1)} custom-call(bf16[512,128]{1,0:T(8,128)(2,1)S(1)} %get-tuple-element.38.read, bf16[512,256]{1,0:T(8,128)(2,1)} %get-tuple-element.39.far_weighted, f32[512,256]{1,0:T(8,128)} %get-tuple-element.40.far_input, bf16[512,128]{1,0:T(8,128)(2,1)} %get-tuple-element.41.far_write, ...), custom_call_target="tpu_custom_call" | custom-call | tf_op jit(solution)/shard_map/pallas_call | solution.py:28
  156.8 0.0 all-to-all-done.4.arriving
  156.8 0.0 copy-done.1
  156.8 0.0 copy-start.2
  156.8 0.9 copy-done.2
  157.7 2.4 %shard_map.207 = (bf16[128,2048]{1,0:T(8,128)(2,1)S(1)}, bf16[16,4,2,64,128]{4,3,2,1,0:T(8,128)(2,1)S(1)}) custom-call(bf16[8,32,256]{2,1,0:T(8,128)(2,1)S(1)} %all-to-all-done.4.arriving, f32[512,256]{1,0:T(8,128)S(1)} %shard_map.206.partly, bf16[512,128]{1,0:T(8,128)(2,1)S(1)} %get-tuple-element.38.read, f32[512,256]{1,0:T(8,128)S(1)} %copy-done.1, ...), custom_call_target="tpu_custom_call" | custom-call | tf_op jit(solution)/shard_map/pallas_call | solution.py:28
  160.2 3.9 %collective-permute-start.10 = (bf16[128,2048]{1,0:T(8,128)(2,1)S(1)}, bf16[128,2048]{1,0:T(8,128)(2,1)S(1)}, u32[]{:S(2)}, u32[]{:S(2)}) collective-permute-start(bf16[128,2048]{1,0:T(8,128)(2,1)S(1)} %get-tuple-element.50), channel_id=1, source_target_pairs={{0,1},{4,7},{1,2},{5,4},{2,3},{6,5},{3,0},{7,6},{8,9},{12,15},{9,1... | collective-permute-start | bytes 1572872 | tf_op jit(solution)/shard_map/ppermute | solution.py:484
  164.1 0.0 copy-done.3
  164.1 2.6 %shard_map.208 = (bf16[128,2048]{1,0:T(8,128)(2,1)S(1)}, bf16[128,2048]{1,0:T(8,128)(2,1)S(1)}, bf16[128,2048]{1,0:T(8,128)(2,1)S(1)}) custom-call(bf16[8,32,256]{2,1,0:T(8,128)(2,1)S(1)} %all-to-all-done.4.arriving, f32[512,256]{1,0:T(8,128)S(1)} %shard_map.206.partly, bf16[512,128]{1,0:T(8,128)(2,1)S(1)} %get-tuple-element.38.read, ...), custom_call_target="tpu_custom_call" | custom-call | tf_op jit(solution)/shard_map/pallas_call | solution.py:28
  166.8 3.1 %collective-permute-start.9 = (bf16[128,2048]{1,0:T(8,128)(2,1)S(1)}, bf16[128,2048]{1,0:T(8,128)(2,1)S(1)}, u32[]{:S(2)}, u32[]{:S(2)}) collective-permute-start(bf16[128,2048]{1,0:T(8,128)(2,1)S(1)} %get-tuple-element.48), channel_id=1, source_target_pairs={{0,3},{4,5},{1,0},{5,6},{2,1},{6,7},{3,2},{7,4},{8,11},{12,13},{9,... | collective-permute-start | bytes 1572872 | tf_op jit(solution)/shard_map/ppermute | solution.py:484
  169.9 2.6 %collective-permute-done.10.got = bf16[128,2048]{1,0:T(8,128)(2,1)S(1)} collective-permute-done((bf16[128,2048]{1,0:T(8,128)(2,1)S(1)}, bf16[128,2048]{1,0:T(8,128)(2,1)S(1)}, u32[]{:S(2)}, u32[]{:S(2)}) %collective-permute-start.10) | collective-permute-done | bytes 524320 | tf_op jit(solution)/shard_map/ppermute | solution.py:484
  172.5 0.1 shard_map.209
  172.6 3.4 %collective-permute-start.11 = (bf16[128,2048]{1,0:T(8,128)(2,1)S(1)}, bf16[128,2048]{1,0:T(8,128)(2,1)S(1)}, u32[]{:S(2)}, u32[]{:S(2)}) collective-permute-start(bf16[128,2048]{1,0:T(8,128)(2,1)S(1)} %shard_map.209), channel_id=1, source_target_pairs={{0,1},{4,7},{1,2},{5,4},{2,3},{6,5},{3,0},{7,6},{8,9},{12,15},{9,1... | collective-permute-start | bytes 1572872 | tf_op jit(solution)/shard_map/ppermute | solution.py:484
  176.0 3.8 %collective-permute-done.9.a = bf16[128,2048]{1,0:T(8,128)(2,1)S(1)} collective-permute-done((bf16[128,2048]{1,0:T(8,128)(2,1)S(1)}, bf16[128,2048]{1,0:T(8,128)(2,1)S(1)}, u32[]{:S(2)}, u32[]{:S(2)}) %collective-permute-start.9) | collective-permute-done | bytes 524320 | tf_op jit(solution)/shard_map/ppermute | solution.py:484
  179.8 5.2 %collective-permute-done.11.b = bf16[128,2048]{1,0:T(8,128)(2,1)S(1)} collective-permute-done((bf16[128,2048]{1,0:T(8,128)(2,1)S(1)}, bf16[128,2048]{1,0:T(8,128)(2,1)S(1)}, u32[]{:S(2)}, u32[]{:S(2)}) %collective-permute-start.11) | collective-permute-done | bytes 524320 | tf_op jit(solution)/shard_map/ppermute | solution.py:484
  185.0 1.0 shard_map.210
  (1 shorter events, 0.0 us)
Async XLA Ops:
  57.1 26.9 %copy-start.4 = (f32[24,256]{1,0:T(8,128)S(1)}, f32[24,256]{1,0:T(8,128)}, u32[]{:S(2)}) copy-start(f32[24,256]{1,0:T(8,128)} %get-tuple-element.29.small) | copy-start | bytes 73732
  57.1 26.9 %copy-start.5 = (bf16[2048,4]{0,1:T(4,128)(2,1)S(1)}, bf16[2048,4]{0,1:T(4,128)(2,1)}, u32[]{:S(2)}) copy-start(bf16[2048,4]{0,1:T(4,128)(2,1)} %param.30) | copy-start | bytes 49156
  57.1 26.9 %copy-start.6 = (f32[4,512]{1,0:T(4,128)S(1)}, f32[4,512]{1,0:T(4,128)}, u32[]{:S(2)}) copy-start(f32[4,512]{1,0:T(4,128)} %spikes.1) | copy-start | bytes 24580
  57.1 26.9 %all-to-all-start = ((bf16[4,128,2048]{2,1,0:T(8,128)(2,1)}), bf16[4,128,2048]{2,1,0:T(8,128)(2,1)S(1)}, u32[]{:S(2)}, u32[]{:S(2)}) async-start(bf16[4,128,2048]{2,1,0:T(8,128)(2,1)} %get-tuple-element.28), calls=%async_computation | async-start | bytes 4194304 | tf_op jit(solution)/shard_map/all_to_all | solution.py:477
  61.7 20.3 %collective-permute-start.2 = (bf16[16,208,128]{2,1,0:T(8,128)(2,1)}, bf16[16,208,128]{2,1,0:T(8,128)(2,1)}, u32[]{:S(2)}, u32[]{:S(2)}) collective-permute-start(bf16[16,208,128]{2,1,0:T(8,128)(2,1)} %get-tuple-element.37.p0), channel_id=1, source_target_pairs={{0,8},{4,28},{8,16},{12,4},{16,24},{20,12},{24,0},{28,20},{1,9},{5... | collective-permute-start | bytes 2555912 | tf_op jit(solution)/shard_map/ppermute | solution.py:483
  63.8 23.3 %collective-permute-start.1 = (bf16[4,16,48,128]{3,2,1,0:T(8,128)(2,1)S(1)}, bf16[4,16,48,128]{3,2,1,0:T(8,128)(2,1)}, u32[]{:S(2)}, u32[]{:S(2)}) collective-permute-start(bf16[4,16,48,128]{3,2,1,0:T(8,128)(2,1)S(1)} %all_to_all.25.own), channel_id=1, source_target_pairs={{0,4},{4,0},{1,5},{5,1},{2,6},{6,2},{3,7},{7,3},{8,12},{12,8},{9,1... | collective-permute-start | bytes 2359304 | tf_op jit(solution)/shard_map/ppermute | solution.py:488
  65.7 42.0 %collective-permute-start.3 = (bf16[16,208,128]{2,1,0:T(8,128)(2,1)}, bf16[16,208,128]{2,1,0:T(8,128)(2,1)}, u32[]{:S(2)}, u32[]{:S(2)}) collective-permute-start(bf16[16,208,128]{2,1,0:T(8,128)(2,1)} %get-tuple-element.37.p0), channel_id=1, source_target_pairs={{0,24},{4,12},{8,0},{12,20},{16,8},{20,28},{24,16},{28,4},{1,25},{... | collective-permute-start | bytes 2555912 | tf_op jit(solution)/shard_map/ppermute | solution.py:483
  82.0 27.7 %collective-permute-start.4 = (bf16[16,208,128]{2,1,0:T(8,128)(2,1)}, bf16[16,208,128]{2,1,0:T(8,128)(2,1)}, u32[]{:S(2)}, u32[]{:S(2)}) collective-permute-start(bf16[16,208,128]{2,1,0:T(8,128)(2,1)} %collective-permute-done.2.p1), channel_id=1, source_target_pairs={{0,8},{4,28},{8,16},{12,4},{16,24},{20,12},{24,0},{28,20},{1,9},{5... | collective-permute-start | bytes 2555912 | tf_op jit(solution)/shard_map/ppermute | solution.py:483
  83.9 12.2 %copy-start = (bf16[4,128,2048]{2,1,0:T(8,128)(2,1)}, bf16[4,128,2048]{2,1,0:T(8,128)(2,1)S(1)}, u32[]{:S(2)}) copy-start(bf16[4,128,2048]{2,1,0:T(8,128)(2,1)S(1)} %all-to-all-done.tok) | copy-start | bytes 6291460
  85.0 27.0 %copy-start.7 = (f32[1,256]{1,0:T(1,128)S(1)}, f32[1,256]{1,0:T(1,128)}, u32[]{:S(2)}) copy-start(f32[1,256]{1,0:T(1,128)} %get-tuple-element.36.left) | copy-start | bytes 3076
  85.0 6.4 %collective-permute-start = (bf16[16,2048]{1,0:T(8,128)(2,1)S(1)}, bf16[16,2048]{1,0:T(8,128)(2,1)S(1)}, u32[]{:S(2)}, u32[]{:S(2)}) collective-permute-start(bf16[16,2048]{1,0:T(8,128)(2,1)S(1)} %get-tuple-element.30), channel_id=1, source_target_pairs={{0,4},{4,8},{8,12},{12,16},{16,20},{20,24},{24,28},{28,32},{32,36}... | collective-permute-start | bytes 196616 | tf_op jit(solution)/shard_map/ppermute | solution.py:569
  96.2 15.9 %all-to-all-start.2 = ((bf16[8,24,256]{2,1,0:T(8,128)(2,1)}), bf16[8,24,256]{2,1,0:T(8,128)(2,1)S(1)}, u32[]{:S(2)}, u32[]{:S(2)}) async-start(bf16[8,24,256]{2,1,0:T(8,128)(2,1)} %get-tuple-element.35), calls=%async_computation.2 | async-start | bytes 196608 | tf_op jit(solution)/shard_map/all_to_all | solution.py:477
  103.3 40.4 %collective-permute-start.5 = (bf16[16,208,128]{2,1,0:T(8,128)(2,1)}, bf16[16,208,128]{2,1,0:T(8,128)(2,1)S(1)}, u32[]{:S(2)}, u32[]{:S(2)}) collective-permute-start(bf16[16,208,128]{2,1,0:T(8,128)(2,1)} %get-tuple-element.37.p0), channel_id=1, source_target_pairs={{0,4},{4,0},{1,5},{5,1},{2,6},{6,2},{3,7},{7,3},{8,12},{12,8},{9,1... | collective-permute-start | bytes 2555912 | tf_op jit(solution)/shard_map/ppermute | solution.py:488
  105.4 38.3 %collective-permute-start.6 = (bf16[16,208,128]{2,1,0:T(8,128)(2,1)}, bf16[16,208,128]{2,1,0:T(8,128)(2,1)S(1)}, u32[]{:S(2)}, u32[]{:S(2)}) collective-permute-start(bf16[16,208,128]{2,1,0:T(8,128)(2,1)} %collective-permute-done.2.p1), channel_id=1, source_target_pairs={{0,4},{4,0},{1,5},{5,1},{2,6},{6,2},{3,7},{7,3},{8,12},{12,8},{9,1... | collective-permute-start | bytes 2555912 | tf_op jit(solution)/shard_map/ppermute | solution.py:488
  107.7 36.0 %collective-permute-start.7 = (bf16[16,208,128]{2,1,0:T(8,128)(2,1)}, bf16[16,208,128]{2,1,0:T(8,128)(2,1)S(1)}, u32[]{:S(2)}, u32[]{:S(2)}) collective-permute-start(bf16[16,208,128]{2,1,0:T(8,128)(2,1)} %collective-permute-done.3.p2), channel_id=1, source_target_pairs={{0,4},{4,0},{1,5},{5,1},{2,6},{6,2},{3,7},{7,3},{8,12},{12,8},{9,1... | collective-permute-start | bytes 2555912 | tf_op jit(solution)/shard_map/ppermute | solution.py:488
  109.7 34.0 %collective-permute-start.8 = (bf16[16,208,128]{2,1,0:T(8,128)(2,1)}, bf16[16,208,128]{2,1,0:T(8,128)(2,1)}, u32[]{:S(2)}, u32[]{:S(2)}) collective-permute-start(bf16[16,208,128]{2,1,0:T(8,128)(2,1)} %collective-permute-done.4.p3), channel_id=1, source_target_pairs={{0,4},{4,0},{1,5},{5,1},{2,6},{6,2},{3,7},{7,3},{8,12},{12,8},{9,1... | collective-permute-start | bytes 2555912 | tf_op jit(solution)/shard_map/ppermute | solution.py:488
  138.9 17.9 %all-to-all-start.4 = ((bf16[8,32,256]{2,1,0:T(8,128)(2,1)}), bf16[8,32,256]{2,1,0:T(8,128)(2,1)S(1)}, u32[]{:S(2)}, u32[]{:S(2)}) async-start(bf16[8,32,256]{2,1,0:T(8,128)(2,1)} %shard_map.204), calls=%async_computation.4 | async-start | bytes 262144 | tf_op jit(solution)/shard_map/all_to_all | solution.py:477
  143.7 1.0 copy-start.8
  154.1 2.7 %copy-start.1 = (f32[512,256]{1,0:T(8,128)S(1)}, f32[512,256]{1,0:T(8,128)}, u32[]{:S(2)}) copy-start(f32[512,256]{1,0:T(8,128)} %get-tuple-element.43.gate) | copy-start | bytes 1572868
  154.1 10.0 %copy-start.3 = (bf16[512,256]{1,0:T(8,128)(2,1)S(1)}, bf16[512,256]{1,0:T(8,128)(2,1)}, u32[]{:S(2)}) copy-start(bf16[512,256]{1,0:T(8,128)(2,1)} %get-tuple-element.44.mixer) | copy-start | bytes 786436
  156.8 1.0 copy-start.2
  160.2 12.3 %collective-permute-start.10 = (bf16[128,2048]{1,0:T(8,128)(2,1)S(1)}, bf16[128,2048]{1,0:T(8,128)(2,1)S(1)}, u32[]{:S(2)}, u32[]{:S(2)}) collective-permute-start(bf16[128,2048]{1,0:T(8,128)(2,1)S(1)} %get-tuple-element.50), channel_id=1, source_target_pairs={{0,1},{4,7},{1,2},{5,4},{2,3},{6,5},{3,0},{7,6},{8,9},{12,15},{9,1... | collective-permute-start | bytes 1572872 | tf_op jit(solution)/shard_map/ppermute | solution.py:484
  166.8 13.0 %collective-permute-start.9 = (bf16[128,2048]{1,0:T(8,128)(2,1)S(1)}, bf16[128,2048]{1,0:T(8,128)(2,1)S(1)}, u32[]{:S(2)}, u32[]{:S(2)}) collective-permute-start(bf16[128,2048]{1,0:T(8,128)(2,1)S(1)} %get-tuple-element.48), channel_id=1, source_target_pairs={{0,3},{4,5},{1,0},{5,6},{2,1},{6,7},{3,2},{7,4},{8,11},{12,13},{9,... | collective-permute-start | bytes 1572872 | tf_op jit(solution)/shard_map/ppermute | solution.py:484
  172.6 12.4 %collective-permute-start.11 = (bf16[128,2048]{1,0:T(8,128)(2,1)S(1)}, bf16[128,2048]{1,0:T(8,128)(2,1)S(1)}, u32[]{:S(2)}, u32[]{:S(2)}) collective-permute-start(bf16[128,2048]{1,0:T(8,128)(2,1)S(1)} %shard_map.209), channel_id=1, source_target_pairs={{0,1},{4,7},{1,2},{5,4},{2,3},{6,5},{3,0},{7,6},{8,9},{12,15},{9,1... | collective-permute-start | bytes 1572872 | tf_op jit(solution)/shard_map/ppermute | solution.py:484
